TPU v7x, 32 devices: a whole 2x2x4 slice. The times are simulated.
32 devices in a mesh: sp: 4 (over z), fs: 4 (over y, x), tp: 2 (over core).
Axes of the slice: x: 2, y: 2, z: 4, core: 2. Of those that a mesh axis runs over, the one named last changes fastest.
Arguments:
- tokens: bfloat16 [512, 2048], P(('sp', 'fs', 'tp')), may hold values from -16 to 16
- in_gain: float32 [2048], replicated, may hold values from 0.1 to 1.9
- ret_query: bfloat16 [2048, 1024], P(None, ('fs', 'tp')), may hold values from -0.125 to 0.125
- ret_key: bfloat16 [2048, 1024], P(None, ('fs', 'tp')), may hold values from -0.125 to 0.125
- ret_value: bfloat16 [2048, 1024], P(None, ('fs', 'tp')), may hold values from -0.125 to 0.125
- decay_log: float32 [8, 512], P(('fs', 'tp'), 'sp'), may hold values from -1 to 0
- init_state: bfloat16 [8, 128, 128], P(('fs', 'tp')), may hold values from -24 to 24
- ret_gain: float32 [1024], P(('fs', 'tp')), may hold values from 0.1 to 1.9
- diff_query: bfloat16 [2, 2048, 512], P(None, None, ('fs', 'tp')), may hold values from -1 to 1
- diff_key: bfloat16 [2, 2048, 512], P(None, None, ('fs', 'tp')), may hold values from -1 to 1
- diff_value: bfloat16 [2048, 1024], P(None, ('fs', 'tp')), may hold values from -0.125 to 0.125
- diff_lambda: float32 [8], P(('fs', 'tp')), may hold values from 0.3 to 0.8
- diff_gain: float32 [1024], P(('fs', 'tp')), may hold values from 0.1 to 1.9
- out_weight: bfloat16 [2, 1024, 2048], P(None, ('fs', 'tp'), 'sp'), may hold values from -0.125 to 0.125
Outputs:
- mixed: bfloat16 [512, 2048], P(('sp', 'fs', 'tp'))
All inputs are finite; a program needn't handle non-finite values.
Results may differ from a plain program's by a relative error of at most 0.017.
Values may be sent and summed in bfloat16 or wider, within the bound.
No kernel may reach another device: no remote copies, remote signals or barrier semaphores. Data moves between devices by JAX's collectives and lax.ppermute only.
A program may use at most 64 MiB of HBM per device.

v0:
```python
import jax
import jax.numpy as jnp
from jax import lax
from jax.experimental import pallas as pl
from jax.experimental.pallas import tpu as pltpu
from jax.sharding import PartitionSpec as P


EPS = 1e-06
HUGE = 1e30
HIGHEST = lax.Precision.HIGHEST
F32 = jnp.float32
BF16 = jnp.bfloat16


def dot(a, b, dims, **kw):
    return lax.dot_general(a, b, (dims, ((), ())), preferred_element_type=F32, **kw)


def nn(a, b, **kw):
    return dot(a, b, ((1,), (0,)), **kw)


def nt(a, b, **kw):
    return dot(a, b, ((1,), (1,)), **kw)


def tn(a, b, **kw):
    return dot(a, b, ((0,), (0,)), **kw)


def few(count):
    return count in (2, 4)


def at_or_before(n):
    return lax.broadcasted_iota(jnp.int32, (n, n), 1) <= lax.broadcasted_iota(jnp.int32, (n, n), 0)


def cumulated(decay_row):
    n = decay_row.shape[1]
    row = lax.broadcasted_iota(jnp.int32, (n, n), 0)
    col = lax.broadcasted_iota(jnp.int32, (n, n), 1)
    wide = jnp.broadcast_to(decay_row, (n, n))
    down = jnp.sum(jnp.where(col <= row, wide, 0.0), axis=1, keepdims=True)
    decay_col = jnp.sum(jnp.where(col == row, wide, 0.0), axis=1, keepdims=True)
    along = jnp.sum(jnp.where(row <= col, decay_col, 0.0), axis=0, keepdims=True)
    return down, along


def project_kernel(x, gain, wk, wv, dk, dv, decay, normed, packed, ret_k, ret_v):
    rows, head = ret_k.shape
    wide = x[...].astype(F32)
    scale = lax.rsqrt(jnp.mean(wide * wide, axis=-1, keepdims=True) + EPS)
    rounded = (wide * scale * gain[...]).astype(BF16)
    normed[...] = rounded
    k = nn(rounded, wk[...]).astype(BF16)
    v = nn(rounded, wv[...]).astype(BF16)
    ret_k[...] = k
    ret_v[...] = v
    cumul, _ = cumulated(decay[...])
    last = cumul[rows - 1 :, :]
    weighted = k.astype(F32) * (jnp.exp(last - cumul) * head ** (-0.5))
    state = tn(weighted, v.astype(F32), precision=HIGHEST)
    keys = nt(rounded, dk[...].reshape(-1, dk.shape[2]))
    packed[0:rows, :] = keys.astype(BF16)
    packed[rows : 2 * rows, :] = nn(rounded, dv[...]).astype(BF16)
    packed[2 * rows : 2 * rows + head, :] = state.astype(BF16)
    factor = jnp.broadcast_to(jnp.exp(last), (8, head))
    packed[2 * rows + head :, :] = factor.astype(BF16)


def own_kernel(normed, wq, dq, packed, ret_k, ret_v, decay, lam, init, queries, scaled, inner, sums, stats):
    rows, head = ret_k.shape
    x = normed[...]
    q = nn(x, wq[...]).astype(BF16)
    cumul, along = cumulated(decay[...])
    lower = at_or_before(rows)
    weights = nt(q, ret_k[...]) * head ** (-0.5) * jnp.exp(jnp.where(lower, cumul - along, -HUGE))
    inner[...] = nn(weights.astype(BF16), ret_v[...])
    scaled[...] = q.astype(F32) * jnp.exp(cumul)
    both = nt(x, dq[...].reshape(-1, dq.shape[2])).astype(BF16)
    queries[...] = both
    half = head // 2
    keys = packed[0:rows, :]
    values = packed[rows : 2 * rows, :]
    for m in range(2):
        s = nt(both[:, m * half : (m + 1) * half], keys[:, m * half : (m + 1) * half]) * half ** (-0.5)
        s = jnp.where(lower, s, -HUGE)
        top = jnp.max(s, axis=-1, keepdims=True)
        e = jnp.exp(s - top)
        sums[m] = nn(e.astype(BF16), values)
        stats[m] = jnp.concatenate([jnp.broadcast_to(top, (rows, half)), jnp.broadcast_to(jnp.sum(e, axis=-1, keepdims=True), (rows, half))], axis=1)


def finish_kernel(count, *refs):
    queries, scaled, inner, sums, stats, lam, init, ret_gain, diff_gain = refs[:9]
    blocks = refs[9 : 8 + count]
    weights = refs[8 + count : 8 + 2 * count]
    partial = refs[8 + 2 * count]
    rows, head = inner.shape
    half = head // 2
    place = lax.axis_index("sp")
    entering = jnp.zeros((head, head), F32)
    carry = jnp.ones((1, head), F32)
    for d, block in enumerate(blocks, 1):
        entering = entering + carry * block[2 * rows : 2 * rows + head, :].astype(F32)
        factor = block[2 * rows + head : 2 * rows + head + 8, :].astype(F32)[0:1, :]
        carry = jnp.where(place >= d, carry * factor, carry)
    entering = entering + carry * init[0].astype(F32)
    ret_out = inner[...] + nn(scaled[...], entering, precision=HIGHEST)
    centre = ret_out - jnp.mean(ret_out, axis=-1, keepdims=True)
    spread = lax.rsqrt(jnp.mean(centre * centre, axis=-1, keepdims=True) + EPS)
    ret_mix = (centre * spread * ret_gain[...]).astype(BF16)

    keys = jnp.concatenate([b[0:rows, :] for b in blocks], axis=0)
    values = jnp.concatenate([b[rows : 2 * rows, :] for b in blocks], axis=0)
    distance = 1 + lax.broadcasted_iota(jnp.int32, (1, keys.shape[0]), 1) // rows
    allowed = distance <= place
    maps = []
    for m in range(2):
        s = nt(queries[:, m * half : (m + 1) * half], keys[:, m * half : (m + 1) * half]) * half ** (-0.5)
        s = jnp.where(allowed, s, -HUGE)
        old_top = stats[m][:, 0:1]
        old_total = stats[m][:, half : half + 1]
        top = jnp.maximum(old_top, jnp.max(s, axis=-1, keepdims=True))
        e = jnp.exp(s - top)
        keep = jnp.exp(old_top - top)
        total = old_total * keep + jnp.sum(e, axis=-1, keepdims=True)
        maps.append((sums[m] * keep + nn(e.astype(BF16), values)) / total)
    diff_out = maps[0] - lam[0] * maps[1]
    level = lax.rsqrt(jnp.mean(diff_out * diff_out, axis=-1, keepdims=True) + EPS)
    diff_mix = (diff_out * level * diff_gain[...]).astype(BF16)

    mixed = jnp.concatenate([ret_mix, diff_mix], axis=1)
    for k, w in enumerate(weights):
        cols = w.shape[2]
        at = pl.multiple_of((place ^ k) * cols, cols)
        partial[:, pl.ds(at, cols)] = nn(mixed, w[...].reshape(2 * head, cols)).astype(BF16)


def call(kernel, outs, flops, smem=(), n=0):
    specs = [pl.BlockSpec(memory_space=pltpu.SMEM if i in smem else pltpu.VMEM) for i in range(n)]
    return pl.pallas_call(
        kernel,
        out_shape=outs,
        in_specs=specs,
        out_specs=[pl.BlockSpec(memory_space=pltpu.VMEM)] * len(outs),
        compiler_params=pltpu.CompilerParams(vmem_limit_bytes=24 * 1024 * 1024),
        cost_estimate=pl.CostEstimate(flops=flops, bytes_accessed=1 << 20, transcendentals=1 << 16),
    )


def shape(dims, kind):
    return jax.ShapeDtypeStruct(dims, kind)


def local_few(
    tokens, in_gain, ret_query, ret_key, ret_value, decay_log, init_state, ret_gain,
    diff_query, diff_key, diff_value, diff_lambda, diff_gain, out_weight,
):
    head = ret_query.shape[1]
    width = tokens.shape[1]
    count = lax.axis_size("sp")
    group = lax.axis_size(("fs", "tp"))
    own_rows = tokens.shape[0]
    rows = own_rows * group

    def swapped(array, k):
        return lax.ppermute(array, "sp", [(i, i ^ k) for i in range(count)])

    weights = [out_weight] * count
    weights[1] = swapped(out_weight, 1)
    if count == 4:
        weights[2] = swapped(out_weight, 2)
        weights[3] = swapped(weights[2], 1)
    gathered = lax.all_gather(tokens, ("fs", "tp"), axis=0, tiled=True)
    square = shape((rows, head), BF16)
    normed, packed, ret_k, ret_v = call(
        project_kernel, [shape((rows, width), BF16), shape((2 * rows + head + 8, head), BF16), square, square],
        flops=2 * rows * width * head * 4, n=7,
    )(gathered, in_gain[None, :], ret_key, ret_value, jnp.swapaxes(diff_key, 1, 2), diff_value, decay_log)
    blocks = []
    for d in range(1, count):
        blocks.append(lax.ppermute(packed, "sp", [(i, i + d) for i in range(count - d)]))
    wide = shape((rows, head), F32)
    pair = shape((2, rows, head), F32)
    mine = call(
        own_kernel, [square, wide, wide, pair, pair], flops=2 * rows * width * head * 2, smem=(7,), n=9,
    )(normed, ret_query, jnp.swapaxes(diff_query, 1, 2), packed, ret_k, ret_v, decay_log, diff_lambda, init_state)
    (partial,) = call(
        lambda *refs: finish_kernel(count, *refs), [shape((rows, width), BF16)],
        flops=2 * rows * width * head * 2, smem=(5,), n=8 + 2 * count,
    )(*mine, diff_lambda, init_state, ret_gain[None, :], diff_gain[None, :], *blocks, *weights)
    shares = lax.all_to_all(partial, ("fs", "tp"), 0, 0, tiled=True)
    return shares.reshape(group, own_rows, width).astype(F32).sum(axis=0).astype(BF16)


def local_many(
    tokens, in_gain, ret_query, ret_key, ret_value, decay_log, init_state, ret_gain,
    diff_query, diff_key, diff_value, diff_lambda, diff_gain, out_weight,
):
    head = ret_query.shape[1]
    width = tokens.shape[1]
    count = lax.axis_size("sp")
    place = lax.axis_index("sp")
    group = lax.axis_size(("fs", "tp"))
    own_rows = tokens.shape[0]
    rows = own_rows * group

    full_weight = lax.all_gather(out_weight, "sp", axis=2, tiled=True).reshape(2 * head, width)
    wide = lax.all_gather(tokens, ("fs", "tp"), axis=0, tiled=True).astype(F32)
    normed = (wide * lax.rsqrt(jnp.mean(wide * wide, axis=-1, keepdims=True) + EPS) * in_gain).astype(BF16)
    ret_q, ret_k, ret_v, diff_v = (nn(normed, w).astype(BF16) for w in (ret_query, ret_key, ret_value, diff_value))
    queries = [nn(normed, diff_query[m]).astype(BF16) for m in range(2)]
    keys = [nn(normed, diff_key[m]).astype(BF16) for m in range(2)]
    lower = at_or_before(rows)
    cumul, along = cumulated(decay_log)
    last = cumul[-1:, :]
    weighted = ret_k.astype(F32) * (jnp.exp(last - cumul) * head ** (-0.5))
    state = tn(weighted, ret_v.astype(F32), precision=HIGHEST)
    factor = jnp.broadcast_to(jnp.exp(last), (8, head))
    packed = jnp.concatenate([jnp.concatenate(keys, axis=1), diff_v, state.astype(BF16), factor.astype(BF16)], axis=0)
    every = lax.all_gather(packed, "sp")
    all_keys = every[:, :rows].reshape(count * rows, -1)
    all_values = every[:, rows : 2 * rows].reshape(count * rows, -1)

    def step(b, carried):
        block = lax.dynamic_index_in_dim(every, b, 0, False).astype(F32)
        return block[2 * rows + head, 0] * carried + block[2 * rows : 2 * rows + head]

    entering = lax.fori_loop(0, place, step, init_state[0].astype(F32))
    scores = nt(ret_q, ret_k) * head ** (-0.5) * jnp.exp(jnp.where(lower, cumul - along, -HUGE))
    ret_out = nn(scores.astype(BF16), ret_v) + nn(ret_q.astype(F32) * jnp.exp(cumul), entering, precision=HIGHEST)
    centre = ret_out - jnp.mean(ret_out, axis=-1, keepdims=True)
    ret_mix = (centre * lax.rsqrt(jnp.mean(centre * centre, axis=-1, keepdims=True) + EPS) * ret_gain).astype(BF16)

    maps = []
    half = head // 2
    allowed = jnp.arange(count * rows)[None, :] <= (place * rows + jnp.arange(rows))[:, None]
    for m in range(2):
        s = nt(queries[m], all_keys[:, m * half : (m + 1) * half]) * half ** (-0.5)
        s = jnp.where(allowed, s, -HUGE)
        e = jnp.exp(s - s.max(axis=-1, keepdims=True))
        maps.append(nn(e.astype(BF16), all_values) / e.sum(axis=-1, keepdims=True))
    diff_out = maps[0] - diff_lambda[0] * maps[1]
    level = lax.rsqrt(jnp.mean(diff_out * diff_out, axis=-1, keepdims=True) + EPS)
    diff_mix = (diff_out * level * diff_gain).astype(BF16)

    mixed = jnp.concatenate([ret_mix, diff_mix], axis=1)
    partial = nn(mixed, full_weight).astype(BF16)
    shares = lax.all_to_all(partial, ("fs", "tp"), 0, 0, tiled=True)
    return shares.reshape(group, own_rows, width).astype(F32).sum(axis=0).astype(BF16)


def solution(mesh):
    count = mesh.shape["sp"]
    in_specs = (
        P(("sp", "fs", "tp"), None),
        P(),
        P(None, ("fs", "tp")),
        P(None, ("fs", "tp")),
        P(None, ("fs", "tp")),
        P(("fs", "tp"), "sp"),
        P(("fs", "tp"), None, None),
        P(("fs", "tp")),
        P(None, None, ("fs", "tp")),
        P(None, None, ("fs", "tp")),
        P(None, ("fs", "tp")),
        P(("fs", "tp")),
        P(("fs", "tp")),
        P(None, ("fs", "tp"), "sp"),
    )
    out_specs = P(("sp", "fs", "tp"), None)
    local = local_few if few(count) else local_many
    return jax.shard_map(local, mesh=mesh, in_specs=in_specs, out_specs=out_specs, check_vma=False)
```

profile of v0, /device:TPU:16, one launch (start us, length us, event | category | flops | bytes accessed | tf_op | source)
XLA Modules:
  0.0 60.1 jit_solution(8799871836189928001)
XLA Ops:
  0.0 0.0 copy-start
  0.0 0.0 collective-permute-start.4
  0.0 1.9 %collective-permute-start.3 = (bf16[2,128,512]{2,1,0:T(8,128)(2,1)}, bf16[2,128,512]{2,1,0:T(8,128)(2,1)S(1)}, u32[]{:S(2)}, u32[]{:S(2)}) collective-permute-start(bf16[2,128,512]{2,1,0:T(8,128)(2,1)} %refs_12_.1), channel_id=1, source_target_pairs={{0,8},{8,0},{16,24},{24,16},{1,9},{9,1},{17,25},{25,17},{2,10},{10... | collective-permute-start | bytes 786440 | tf_op jit(solution)/shard_map/ppermute | solution.py:170
  1.9 9.9 %collective-permute-done.4.refs_14_ = bf16[2,128,512]{2,1,0:T(8,128)(2,1)S(1)} collective-permute-done((bf16[2,128,512]{2,1,0:T(8,128)(2,1)}, bf16[2,128,512]{2,1,0:T(8,128)(2,1)S(1)}, u32[]{:S(2)}, u32[]{:S(2)}) %collective-permute-start.4) | collective-permute-done | bytes 262176 | tf_op jit(solution)/shard_map/ppermute | solution.py:170
  11.8 4.4 %collective-permute-start.5 = (bf16[2,128,512]{2,1,0:T(8,128)(2,1)S(1)}, bf16[2,128,512]{2,1,0:T(8,128)(2,1)S(1)}, u32[]{:S(2)}, u32[]{:S(2)}) collective-permute-start(bf16[2,128,512]{2,1,0:T(8,128)(2,1)S(1)} %collective-permute-done.4.refs_14_), channel_id=1, source_target_pairs={{0,8},{8,0},{16,24},{24,16},{1,9},{9,1},{17,25},{25,17},{2,10},{10... | collective-permute-start | bytes 786440 | tf_op jit(solution)/shard_map/ppermute | solution.py:170
  16.2 0.0 copy-start.8
  16.2 10.3 %all_gather.3.x = bf16[128,2048]{1,0:T(8,128)(2,1)S(1)} all-gather(bf16[16,2048]{1,0:T(8,128)(2,1)} %param.14), channel_id=1, replica_groups=mesh['sp'=4,'fs'=4,'tp'=2] {'fs','tp'}, dimensions={0}, use_global_device_ids=true | all-gather | bytes 589824 | tf_op jit(solution)/shard_map/all_gather | solution.py:177
  26.5 0.0 copy-start.9
  26.5 0.0 copy-done
  26.5 0.0 copy-done.8
  26.5 0.6 %copy-done.9 = f32[1,128]{1,0:T(1,128)S(1)} copy-done((f32[1,128]{1,0:T(1,128)S(1)}, f32[1,128]{1,0:T(1,128)}, u32[]{:S(2)}) %copy-start.9) | copy-done | bytes 536
  27.2 0.0 copy-start.1
  27.2 1.0 %copy-done.1 = bf16[2048,128]{1,0:T(8,128)(2,1)S(1)} copy-done((bf16[2048,128]{1,0:T(8,128)(2,1)S(1)}, bf16[2048,128]{1,0:T(8,128)(2,1)}, u32[]{:S(2)}) %copy-start.1) | copy-done | bytes 524312
  28.2 0.0 copy-start.2
  28.2 1.0 %copy-done.2 = bf16[2,2048,64]{1,2,0:T(8,128)(2,1)S(1)} copy-done((bf16[2,2048,64]{1,2,0:T(8,128)(2,1)S(1)}, bf16[2,2048,64]{1,2,0:T(8,128)(2,1)}, u32[]{:S(2)}) %copy-start.2) | copy-done | bytes 524312
  29.3 0.0 copy-start.3
  29.3 1.0 %copy-done.3 = bf16[2048,128]{1,0:T(8,128)(2,1)S(1)} copy-done((bf16[2048,128]{1,0:T(8,128)(2,1)S(1)}, bf16[2048,128]{1,0:T(8,128)(2,1)}, u32[]{:S(2)}) %copy-start.3) | copy-done | bytes 524312
  30.3 0.0 copy-start.4
  30.3 0.0 copy-start.5
  30.3 0.0 copy-start.7
  30.3 1.1 %shard_map.136 = (bf16[128,2048]{1,0:T(8,128)(2,1)S(1)}, bf16[392,128]{1,0:T(8,128)(2,1)S(1)}, bf16[128,128]{1,0:T(8,128)(2,1)S(1)}, bf16[128,128]{1,0:T(8,128)(2,1)S(1)}) custom-call(bf16[128,2048]{1,0:T(8,128)(2,1)S(1)} %all_gather.3.x, f32[1,2048]{1,0:T(1,128)S(1)} %bitcast.9, bf16[2048,128]{1,0:T(8,128)(2,1)S(1)} %copy-done, ...), custom_call_target="tpu_custom_call" | custom-call | flops 268435456 | bytes 1048576 | tf_op jit(solution)/shard_map/pallas_call | solution.py:179
  31.4 0.7 %collective-permute-start.2 = (bf16[392,128]{1,0:T(8,128)(2,1)S(1)}, bf16[392,128]{1,0:T(8,128)(2,1)S(1)}, u32[]{:S(2)}, u32[]{:S(2)}) collective-permute-start(bf16[392,128]{1,0:T(8,128)(2,1)S(1)} %get-tuple-element.15.packed), channel_id=1, source_target_pairs={{0,24},{1,25},{2,26},{3,27},{4,28},{5,29},{6,30},{7,31}} | collective-permute-start | bytes 301064 | tf_op jit(solution)/shard_map/ppermute | solution.py:185
  32.0 1.3 %collective-permute-start.1 = (bf16[392,128]{1,0:T(8,128)(2,1)S(1)}, bf16[392,128]{1,0:T(8,128)(2,1)S(1)}, u32[]{:S(2)}, u32[]{:S(2)}) collective-permute-start(bf16[392,128]{1,0:T(8,128)(2,1)S(1)} %get-tuple-element.15.packed), channel_id=1, source_target_pairs={{0,16},{8,24},{1,17},{9,25},{2,18},{10,26},{3,19},{11,27},{4,20},{... | collective-permute-start | bytes 301064 | tf_op jit(solution)/shard_map/ppermute | solution.py:185
  33.3 2.5 %collective-permute-start = (bf16[392,128]{1,0:T(8,128)(2,1)S(1)}, bf16[392,128]{1,0:T(8,128)(2,1)S(1)}, u32[]{:S(2)}, u32[]{:S(2)}) collective-permute-start(bf16[392,128]{1,0:T(8,128)(2,1)S(1)} %get-tuple-element.15.packed), channel_id=1, source_target_pairs={{0,8},{8,16},{16,24},{1,9},{9,17},{17,25},{2,10},{10,18},{18,26},{... | collective-permute-start | bytes 301064 | tf_op jit(solution)/shard_map/ppermute | solution.py:185
  36.5 0.0 copy-done.4
  36.5 0.0 copy-done.5
  36.6 0.0 copy-done.7
  36.6 0.0 copy-start.6
  36.6 1.1 %shard_map.137 = (bf16[128,128]{1,0:T(8,128)(2,1)S(1)}, f32[128,128]{1,0:T(8,128)S(1)}, f32[128,128]{1,0:T(8,128)S(1)}, f32[2,128,128]{2,1,0:T(8,128)S(1)}, f32[2,128,128]{2,1,0:T(8,128)S(1)}) custom-call(bf16[128,2048]{1,0:T(8,128)(2,1)S(1)} %get-tuple-element.14.normed, bf16[2048,128]{1,0:T(8,128)(2,1)S(1)} %copy-done.4, bf16[2,64,2048]{2,1,0:T(8,128)(2,1)S(1)} %bitcast.8, ...), custom_call_target="tpu_custom_call" | custom-call | flops 134217728 | bytes 1048576 | tf_op jit(solution)/shard_map/pallas_call | solution.py:188
  37.7 0.0 collective-permute-done.2.refs_11_
  37.7 3.8 %collective-permute-done.1.refs_10_ = bf16[392,128]{1,0:T(8,128)(2,1)S(1)} collective-permute-done((bf16[392,128]{1,0:T(8,128)(2,1)S(1)}, bf16[392,128]{1,0:T(8,128)(2,1)S(1)}, u32[]{:S(2)}, u32[]{:S(2)}) %collective-permute-start.1) | collective-permute-done | bytes 100384 | tf_op jit(solution)/shard_map/ppermute | solution.py:185
  41.5 3.6 %collective-permute-done.refs_9_ = bf16[392,128]{1,0:T(8,128)(2,1)S(1)} collective-permute-done((bf16[392,128]{1,0:T(8,128)(2,1)S(1)}, bf16[392,128]{1,0:T(8,128)(2,1)S(1)}, u32[]{:S(2)}, u32[]{:S(2)}) %collective-permute-start) | collective-permute-done | bytes 100384 | tf_op jit(solution)/shard_map/ppermute | solution.py:185
  45.2 0.0 collective-permute-done.3.refs_13_
  45.2 0.0 collective-permute-done.5.refs_15_
  45.2 0.0 copy-start.10
  45.2 0.0 copy-start.11
  45.2 0.0 copy-done.6
  45.2 0.6 %copy-done.10 = f32[128]{0:T(128)S(1)} copy-done((f32[128]{0:T(128)S(1)}, f32[128]{0:T(128)}, u32[]{:S(2)}) %copy-start.10) | copy-done | bytes 536
  45.8 0.0 copy-done.11
  45.8 1.3 %shard_map.138 = bf16[128,2048]{1,0:T(8,128)(2,1)S(1)} custom-call(bf16[128,128]{1,0:T(8,128)(2,1)S(1)} %get-tuple-element.18.refs_0_, f32[128,128]{1,0:T(8,128)S(1)} %get-tuple-element.19.refs_1_, f32[128,128]{1,0:T(8,128)S(1)} %get-tuple-element.20.refs_2_, f32[2,128,128]{2,1,0:T(8,128)S(1)} %get-tuple-element.21.refs_3_, ...), custom_call_target="tpu_custom_call" | custom-call | flops 134217728 | bytes 1048576 | tf_op jit(solution)/shard_map/pallas_call | solution.py:191
  47.2 12.2 %all_to_all.9 = bf16[8,16,2048]{2,1,0:T(8,128)(2,1)S(1)} all-to-all(bf16[8,16,2048]{2,1,0:T(8,128)(2,1)S(1)} %bitcast.6), channel_id=1, replica_groups=mesh['sp'=4,'fs'=4,'tp'=2] {'fs','tp'}, dimensions={0} | all-to-all | bytes 1048576 | tf_op jit(solution)/shard_map/all_to_all | solution.py:195
  59.4 0.7 %reduce_sum.12 = bf16[16,2048]{1,0:T(8,128)(2,1)} reduce(bf16[8,16,2048]{2,1,0:T(8,128)(2,1)S(1)} %all_to_all.9, bf16[]{:T(256)} %constant.2.clone.1), dimensions={0}, to_apply=%region_0.0 | reduce | flops 229376 | bytes 589826 | tf_op jit(solution)/shard_map/reduce_sum | solution.py:196
Async XLA Ops:
  0.0 26.5 %copy-start = (bf16[2048,128]{1,0:T(8,128)(2,1)S(1)}, bf16[2048,128]{1,0:T(8,128)(2,1)}, u32[]{:S(2)}) copy-start(bf16[2048,128]{1,0:T(8,128)(2,1)} %wk.1) | copy-start | bytes 1572868
  0.0 11.8 %collective-permute-start.4 = (bf16[2,128,512]{2,1,0:T(8,128)(2,1)}, bf16[2,128,512]{2,1,0:T(8,128)(2,1)S(1)}, u32[]{:S(2)}, u32[]{:S(2)}) collective-permute-start(bf16[2,128,512]{2,1,0:T(8,128)(2,1)} %refs_12_.1), channel_id=1, source_target_pairs={{0,16},{8,24},{16,0},{24,8},{1,17},{9,25},{17,1},{25,9},{2,18},{10... | collective-permute-start | bytes 786440 | tf_op jit(solution)/shard_map/ppermute | solution.py:170
  0.0 45.2 %collective-permute-start.3 = (bf16[2,128,512]{2,1,0:T(8,128)(2,1)}, bf16[2,128,512]{2,1,0:T(8,128)(2,1)S(1)}, u32[]{:S(2)}, u32[]{:S(2)}) collective-permute-start(bf16[2,128,512]{2,1,0:T(8,128)(2,1)} %refs_12_.1), channel_id=1, source_target_pairs={{0,8},{8,0},{16,24},{24,16},{1,9},{9,1},{17,25},{25,17},{2,10},{10... | collective-permute-start | bytes 786440 | tf_op jit(solution)/shard_map/ppermute | solution.py:170
  11.8 33.3 %collective-permute-start.5 = (bf16[2,128,512]{2,1,0:T(8,128)(2,1)S(1)}, bf16[2,128,512]{2,1,0:T(8,128)(2,1)S(1)}, u32[]{:S(2)}, u32[]{:S(2)}) collective-permute-start(bf16[2,128,512]{2,1,0:T(8,128)(2,1)S(1)} %collective-permute-done.4.refs_14_), channel_id=1, source_target_pairs={{0,8},{8,0},{16,24},{24,16},{1,9},{9,1},{17,25},{25,17},{2,10},{10... | collective-permute-start | bytes 786440 | tf_op jit(solution)/shard_map/ppermute | solution.py:170
  16.2 10.3 %copy-start.8 = (f32[2048]{0:T(1024)S(1)}, f32[2048]{0:T(1024)}, u32[]{:S(2)}) copy-start(f32[2048]{0:T(1024)} %param.15) | copy-start | bytes 24580
  26.5 0.7 %copy-start.9 = (f32[1,128]{1,0:T(1,128)S(1)}, f32[1,128]{1,0:T(1,128)}, u32[]{:S(2)}) copy-start(f32[1,128]{1,0:T(1,128)} %decay.3) | copy-start | bytes 1540
  27.2 1.0 %copy-start.1 = (bf16[2048,128]{1,0:T(8,128)(2,1)S(1)}, bf16[2048,128]{1,0:T(8,128)(2,1)}, u32[]{:S(2)}) copy-start(bf16[2048,128]{1,0:T(8,128)(2,1)} %wv.1) | copy-start | bytes 1572868
  28.2 1.0 %copy-start.2 = (bf16[2,2048,64]{1,2,0:T(8,128)(2,1)S(1)}, bf16[2,2048,64]{1,2,0:T(8,128)(2,1)}, u32[]{:S(2)}) copy-start(bf16[2,2048,64]{1,2,0:T(8,128)(2,1)} %param.23) | copy-start | bytes 1572868
  29.3 1.0 %copy-start.3 = (bf16[2048,128]{1,0:T(8,128)(2,1)S(1)}, bf16[2048,128]{1,0:T(8,128)(2,1)}, u32[]{:S(2)}) copy-start(bf16[2048,128]{1,0:T(8,128)(2,1)} %dv.1) | copy-start | bytes 1572868
  30.3 6.2 %copy-start.4 = (bf16[2048,128]{1,0:T(8,128)(2,1)S(1)}, bf16[2048,128]{1,0:T(8,128)(2,1)}, u32[]{:S(2)}) copy-start(bf16[2048,128]{1,0:T(8,128)(2,1)} %wq.1) | copy-start | bytes 1572868
  30.3 6.3 %copy-start.5 = (bf16[2,2048,64]{1,2,0:T(8,128)(2,1)S(1)}, bf16[2,2048,64]{1,2,0:T(8,128)(2,1)}, u32[]{:S(2)}) copy-start(bf16[2,2048,64]{1,2,0:T(8,128)(2,1)} %param.22) | copy-start | bytes 1572868
  30.3 6.3 %copy-start.7 = (bf16[1,128,128]{2,1,0:T(8,128)(2,1)S(1)}, bf16[1,128,128]{2,1,0:T(8,128)(2,1)}, u32[]{:S(2)}) copy-start(bf16[1,128,128]{2,1,0:T(8,128)(2,1)} %refs_6_.1) | copy-start | bytes 98308
  31.4 6.3 %collective-permute-start.2 = (bf16[392,128]{1,0:T(8,128)(2,1)S(1)}, bf16[392,128]{1,0:T(8,128)(2,1)S(1)}, u32[]{:S(2)}, u32[]{:S(2)}) collective-permute-start(bf16[392,128]{1,0:T(8,128)(2,1)S(1)} %get-tuple-element.15.packed), channel_id=1, source_target_pairs={{0,24},{1,25},{2,26},{3,27},{4,28},{5,29},{6,30},{7,31}} | collective-permute-start | bytes 301064 | tf_op jit(solution)/shard_map/ppermute | solution.py:185
  32.0 9.5 %collective-permute-start.1 = (bf16[392,128]{1,0:T(8,128)(2,1)S(1)}, bf16[392,128]{1,0:T(8,128)(2,1)S(1)}, u32[]{:S(2)}, u32[]{:S(2)}) collective-permute-start(bf16[392,128]{1,0:T(8,128)(2,1)S(1)} %get-tuple-element.15.packed), channel_id=1, source_target_pairs={{0,16},{8,24},{1,17},{9,25},{2,18},{10,26},{3,19},{11,27},{4,20},{... | collective-permute-start | bytes 301064 | tf_op jit(solution)/shard_map/ppermute | solution.py:185
  33.3 11.8 %collective-permute-start = (bf16[392,128]{1,0:T(8,128)(2,1)S(1)}, bf16[392,128]{1,0:T(8,128)(2,1)S(1)}, u32[]{:S(2)}, u32[]{:S(2)}) collective-permute-start(bf16[392,128]{1,0:T(8,128)(2,1)S(1)} %get-tuple-element.15.packed), channel_id=1, source_target_pairs={{0,8},{8,16},{16,24},{1,9},{9,17},{17,25},{2,10},{10,18},{18,26},{... | collective-permute-start | bytes 301064 | tf_op jit(solution)/shard_map/ppermute | solution.py:185
  36.6 8.6 %copy-start.6 = (bf16[2,128,512]{2,1,0:T(8,128)(2,1)S(1)}, bf16[2,128,512]{2,1,0:T(8,128)(2,1)}, u32[]{:S(2)}) copy-start(bf16[2,128,512]{2,1,0:T(8,128)(2,1)} %refs_12_.1) | copy-start | bytes 786436
  45.2 0.7 %copy-start.10 = (f32[128]{0:T(128)S(1)}, f32[128]{0:T(128)}, u32[]{:S(2)}) copy-start(f32[128]{0:T(128)} %param.21) | copy-start | bytes 1540
  45.2 0.7 %copy-start.11 = (f32[128]{0:T(128)S(1)}, f32[128]{0:T(128)}, u32[]{:S(2)}) copy-start(f32[128]{0:T(128)} %param.26) | copy-start | bytes 1540
where the time goes:
time: 60.6 us; the launch traced here: 60.1 us
  blocking collectives  22.5 us (37%)
  waiting for transfers between devices  17.4 us (29%)
  starting transfers between devices  10.8 us (18%)
  local copies, waits for them, and re-layouts  4.45 us (7%)
  Pallas kernels  3.48 us (6%)
  between operations  0.76 us (1%)
  other arithmetic  0.7 us (1%)
    all_to_all x1, blocking collectives, local_few(): shares = lax.all_to_all(partial, ('fs', 'tp'), 0, 0, tiled=True)  12.2 us
    all_gather x1, blocking collectives, local_few(): gathered = lax.all_gather(tokens, ('fs', 'tp'), axis=0, tiled=True)  10.3 us
    ppermute x3, waiting for transfers between devices, swapped(): return lax.ppermute(array, 'sp', [(i, i ^ k) for i in range(count)])  9.92 us
    ppermute x3, waiting for transfers between devices, local_few(): lax.ppermute(packed, 'sp', [(i, i + d) for i in range(count - d)])  7.49 us
    ppermute x3, starting transfers between devices, swapped(): return lax.ppermute(array, 'sp', [(i, i ^ k) for i in range(count)])  6.32 us
    ppermute x3, starting transfers between devices, local_few(): lax.ppermute(packed, 'sp', [(i, i + d) for i in range(count - d)])  4.5 us
    unnamed x24, local copies, waits for them, and re-layouts  4.45 us
    pallas_call x1, Pallas kernels, local_few(): call(lambda *refs: finish_kernel(count, *refs), [shape((rows, width), BF1...  1.34 us
  transfers between devices with their start and end apart: 6, of which 3 were waited for; matrix products, arithmetic and copies ran while one was open for 0% of the time, Pallas kernels for 4%

commit v1 on v0

--- a/solution.py
+++ b/solution.py
@@ -1,3 +1,5 @@
+import functools
+
 import jax
 import jax.numpy as jnp
 from jax import lax
@@ -12,6 +14,8 @@
 F32 = jnp.float32
 BF16 = jnp.bfloat16
 
+GATHER_FLOPS = 10**10
+
 
 def dot(a, b, dims, **kw):
     return lax.dot_general(a, b, (dims, ((), ())), preferred_element_type=F32, **kw)
@@ -27,6 +31,10 @@
 
 def tn(a, b, **kw):
     return dot(a, b, ((0,), (0,)), **kw)
+
+
+def route(d, count):
+    return [(i, i + d) for i in range(count - d)], lambda at: at - d
 
 
 def few(count):
@@ -48,40 +56,66 @@
     return down, along
 
 
-def project_kernel(x, gain, wk, wv, dk, dv, decay, normed, packed, ret_k, ret_v):
+def fetch(pairs, sems):
+    copies = [pltpu.make_async_copy(src, dst, sems.at[i]) for i, (src, dst) in enumerate(pairs)]
+    for copy in copies:
+        copy.start()
+    return copies
+
+
+def prepare_kernel(
+    tokens_h, decay_h, in_gain_h, ret_gain_h, diff_gain_h, init_h,
+    tokens, key_scale, query_scale, fade, factor, in_gain, small, init, decay, ret_gain, diff_gain, start, sems,
+):
+    head = fade.shape[0]
+    copies = fetch(
+        [(decay_h, decay), (tokens_h, tokens), (in_gain_h, in_gain), (ret_gain_h, ret_gain), (diff_gain_h, diff_gain), (init_h, start)],
+        sems,
+    )
+    copies[0].wait()
+    cumul, along = cumulated(decay[...])
+    rows = cumul.shape[0]
+    last = cumul[rows - 1 :, :]
+    key_scale[...] = jnp.broadcast_to(jnp.exp(last - cumul) * head ** (-0.5), (rows, head))
+    query_scale[...] = jnp.broadcast_to(jnp.exp(cumul), (rows, head))
+    fade[...] = jnp.exp(jnp.where(at_or_before(rows), cumul - along, -HUGE)) * head ** (-0.5)
+    factor[...] = jnp.broadcast_to(jnp.exp(last), (8, head))
+    for copy in copies[1:]:
+        copy.wait()
+    small[0:8, :] = jnp.broadcast_to(ret_gain[...], (8, head))
+    small[8:16, :] = jnp.broadcast_to(diff_gain[...], (8, head))
+    init[...] = start[0].astype(F32)
+
+
+def project_kernel(x, gain, key_scale, factor, dk, dv, wk, wv, normed, packed, ret_k, ret_v):
     rows, head = ret_k.shape
     wide = x[...].astype(F32)
     scale = lax.rsqrt(jnp.mean(wide * wide, axis=-1, keepdims=True) + EPS)
     rounded = (wide * scale * gain[...]).astype(BF16)
     normed[...] = rounded
+    packed[0:rows, :] = nt(rounded, dk[...].reshape(-1, dk.shape[2])).astype(BF16)
+    packed[rows : 2 * rows, :] = nn(rounded, dv[...]).astype(BF16)
     k = nn(rounded, wk[...]).astype(BF16)
     v = nn(rounded, wv[...]).astype(BF16)
     ret_k[...] = k
     ret_v[...] = v
-    cumul, _ = cumulated(decay[...])
-    last = cumul[rows - 1 :, :]
-    weighted = k.astype(F32) * (jnp.exp(last - cumul) * head ** (-0.5))
-    state = tn(weighted, v.astype(F32), precision=HIGHEST)
-    keys = nt(rounded, dk[...].reshape(-1, dk.shape[2]))
-    packed[0:rows, :] = keys.astype(BF16)
-    packed[rows : 2 * rows, :] = nn(rounded, dv[...]).astype(BF16)
+    state = tn(k.astype(F32) * key_scale[...], v.astype(F32), precision=HIGHEST)
     packed[2 * rows : 2 * rows + head, :] = state.astype(BF16)
-    factor = jnp.broadcast_to(jnp.exp(last), (8, head))
-    packed[2 * rows + head :, :] = factor.astype(BF16)
-
-
-def own_kernel(normed, wq, dq, packed, ret_k, ret_v, decay, lam, init, queries, scaled, inner, sums, stats):
+    packed[2 * rows + head :, :] = factor[...].astype(BF16)
+
+
+def own_kernel(lam, normed, packed, ret_k, ret_v, query_scale, fade, wq, dq, queries, scaled, inner, sums, stats, second):
     rows, head = ret_k.shape
+    second[...] = jnp.full(second.shape, lam[0])
     x = normed[...]
     q = nn(x, wq[...]).astype(BF16)
-    cumul, along = cumulated(decay[...])
-    lower = at_or_before(rows)
-    weights = nt(q, ret_k[...]) * head ** (-0.5) * jnp.exp(jnp.where(lower, cumul - along, -HUGE))
+    weights = nt(q, ret_k[...]) * fade[...]
     inner[...] = nn(weights.astype(BF16), ret_v[...])
-    scaled[...] = q.astype(F32) * jnp.exp(cumul)
+    scaled[...] = q.astype(F32) * query_scale[...]
     both = nt(x, dq[...].reshape(-1, dq.shape[2])).astype(BF16)
     queries[...] = both
     half = head // 2
+    lower = at_or_before(rows)
     keys = packed[0:rows, :]
     values = packed[rows : 2 * rows, :]
     for m in range(2):
@@ -93,30 +127,36 @@
         stats[m] = jnp.concatenate([jnp.broadcast_to(top, (rows, half)), jnp.broadcast_to(jnp.sum(e, axis=-1, keepdims=True), (rows, half))], axis=1)
 
 
-def finish_kernel(count, *refs):
-    queries, scaled, inner, sums, stats, lam, init, ret_gain, diff_gain = refs[:9]
-    blocks = refs[9 : 8 + count]
-    weights = refs[8 + count : 8 + 2 * count]
-    partial = refs[8 + 2 * count]
+def finish_kernel(sources, *refs):
+    count = len(sources) + 1
+    queries, scaled, inner, sums, stats, second, small, init = refs[:8]
+    blocks = refs[8 : 7 + count]
+    weights = refs[7 + count : 7 + 2 * count]
+    keep, send, mixed = refs[7 + 2 * count :]
     rows, head = inner.shape
     half = head // 2
     place = lax.axis_index("sp")
-    entering = jnp.zeros((head, head), F32)
-    carry = jnp.ones((1, head), F32)
-    for d, block in enumerate(blocks, 1):
+    core = lax.axis_index("tp")
+    source = [f(place) for f in sources]
+    before = [jnp.logical_and(at >= 0, at < place) for at in source]
+    factors = [b[2 * rows + head : 2 * rows + head + 8, :].astype(F32)[0:1, :] for b in blocks]
+    entering = init[...]
+    for factor, here in zip(factors, before):
+        entering = entering * jnp.where(here, factor, 1.0)
+    for j, block in enumerate(blocks):
+        carry = jnp.where(before[j], 1.0, 0.0) * jnp.ones((1, head), F32)
+        for i, factor in enumerate(factors):
+            if i != j:
+                carry = carry * jnp.where(jnp.logical_and(source[i] > source[j], before[i]), factor, 1.0)
         entering = entering + carry * block[2 * rows : 2 * rows + head, :].astype(F32)
-        factor = block[2 * rows + head : 2 * rows + head + 8, :].astype(F32)[0:1, :]
-        carry = jnp.where(place >= d, carry * factor, carry)
-    entering = entering + carry * init[0].astype(F32)
     ret_out = inner[...] + nn(scaled[...], entering, precision=HIGHEST)
     centre = ret_out - jnp.mean(ret_out, axis=-1, keepdims=True)
     spread = lax.rsqrt(jnp.mean(centre * centre, axis=-1, keepdims=True) + EPS)
-    ret_mix = (centre * spread * ret_gain[...]).astype(BF16)
+    ret_mix = (centre * spread * small[0:1, :]).astype(BF16)
 
     keys = jnp.concatenate([b[0:rows, :] for b in blocks], axis=0)
     values = jnp.concatenate([b[rows : 2 * rows, :] for b in blocks], axis=0)
-    distance = 1 + lax.broadcasted_iota(jnp.int32, (1, keys.shape[0]), 1) // rows
-    allowed = distance <= place
+    allowed = jnp.concatenate([jnp.full((1, rows), jnp.where(here, 1, 0)) for here in before], axis=1) > 0
     maps = []
     for m in range(2):
         s = nt(queries[:, m * half : (m + 1) * half], keys[:, m * half : (m + 1) * half]) * half ** (-0.5)
@@ -125,34 +165,44 @@
         old_total = stats[m][:, half : half + 1]
         top = jnp.maximum(old_top, jnp.max(s, axis=-1, keepdims=True))
         e = jnp.exp(s - top)
-        keep = jnp.exp(old_top - top)
-        total = old_total * keep + jnp.sum(e, axis=-1, keepdims=True)
-        maps.append((sums[m] * keep + nn(e.astype(BF16), values)) / total)
-    diff_out = maps[0] - lam[0] * maps[1]
+        kept = jnp.exp(old_top - top)
+        total = old_total * kept + jnp.sum(e, axis=-1, keepdims=True)
+        maps.append((sums[m] * kept + nn(e.astype(BF16), values)) / total)
+    diff_out = maps[0] - second[0:1, :] * maps[1]
     level = lax.rsqrt(jnp.mean(diff_out * diff_out, axis=-1, keepdims=True) + EPS)
-    diff_mix = (diff_out * level * diff_gain[...]).astype(BF16)
-
-    mixed = jnp.concatenate([ret_mix, diff_mix], axis=1)
+    diff_mix = (diff_out * level * small[8:9, :]).astype(BF16)
+
+    mixed[:, :, :, :head] = ret_mix.reshape(mixed.shape[:3] + (head,))
+    mixed[:, :, :, head:] = diff_mix.reshape(mixed.shape[:3] + (head,))
+    ordered = jnp.concatenate([mixed[:, core].reshape(-1, 2 * head), mixed[:, 1 - core].reshape(-1, 2 * head)], axis=0)
     for k, w in enumerate(weights):
         cols = w.shape[2]
-        at = pl.multiple_of((place ^ k) * cols, cols)
-        partial[:, pl.ds(at, cols)] = nn(mixed, w[...].reshape(2 * head, cols)).astype(BF16)
-
-
-def call(kernel, outs, flops, smem=(), n=0):
-    specs = [pl.BlockSpec(memory_space=pltpu.SMEM if i in smem else pltpu.VMEM) for i in range(n)]
-    return pl.pallas_call(
+        at = pl.ds(pl.multiple_of((place ^ k) * cols, cols), cols)
+        result = nn(ordered, w[...].reshape(2 * head, cols))
+        keep[:, at] = result[: rows // 2]
+        send[:, at] = result[rows // 2 :].astype(BF16)
+
+
+def call(kernel, outs, flops, here, away=0, scratch=(), scalars=0):
+    spots = [pltpu.SMEM] * scalars + [pltpu.VMEM] * here + [pltpu.HBM] * away
+    run = pl.pallas_call(
         kernel,
         out_shape=outs,
-        in_specs=specs,
+        in_specs=[pl.BlockSpec(memory_space=spot) for spot in spots],
         out_specs=[pl.BlockSpec(memory_space=pltpu.VMEM)] * len(outs),
+        scratch_shapes=list(scratch) + ([pltpu.SemaphoreType.DMA((away,))] if away else []),
         compiler_params=pltpu.CompilerParams(vmem_limit_bytes=24 * 1024 * 1024),
         cost_estimate=pl.CostEstimate(flops=flops, bytes_accessed=1 << 20, transcendentals=1 << 16),
     )
 
+    def placed(*args):
+        return run(*[a if spot is pltpu.SMEM else pltpu.with_memory_space_constraint(a, spot) for a, spot in zip(args, spots)])
+
+    return placed
+
 
 def shape(dims, kind):
-    return jax.ShapeDtypeStruct(dims, kind)
+    return pltpu.VMEM(dims, kind)
 
 
 def local_few(
@@ -174,26 +224,39 @@
     if count == 4:
         weights[2] = swapped(out_weight, 2)
         weights[3] = swapped(weights[2], 1)
-    gathered = lax.all_gather(tokens, ("fs", "tp"), axis=0, tiled=True)
     square = shape((rows, head), BF16)
+    wide = shape((rows, head), F32)
+    line = pltpu.VMEM((1, head), F32)
+    staged, key_scale, query_scale, fade, factor, gain, small, init = call(
+        prepare_kernel,
+        [shape(tokens.shape, BF16), wide, wide, shape((rows, rows), F32), shape((8, head), F32),
+         shape((1, width), F32), shape((16, head), F32), shape((head, head), F32)],
+        GATHER_FLOPS, 0, 6, [line, line, line, pltpu.VMEM((1, head, head), BF16)],
+    )(tokens, decay_log, in_gain[None, :], ret_gain[None, :], diff_gain[None, :], init_state)
+    gathered = lax.all_gather(staged, ("fs", "tp"), axis=0, tiled=True)
     normed, packed, ret_k, ret_v = call(
         project_kernel, [shape((rows, width), BF16), shape((2 * rows + head + 8, head), BF16), square, square],
-        flops=2 * rows * width * head * 4, n=7,
-    )(gathered, in_gain[None, :], ret_key, ret_value, jnp.swapaxes(diff_key, 1, 2), diff_value, decay_log)
-    blocks = []
+        2 * rows * width * head * 4, 8,
+    )(gathered, gain, key_scale, factor, jnp.swapaxes(diff_key, 1, 2), diff_value, ret_key, ret_value)
+    blocks, sources = [], []
     for d in range(1, count):
-        blocks.append(lax.ppermute(packed, "sp", [(i, i + d) for i in range(count - d)]))
-    wide = shape((rows, head), F32)
+        pairs, source = route(d, count)
+        sources.append(source)
+        blocks.append(lax.ppermute(packed, "sp", pairs))
     pair = shape((2, rows, head), F32)
-    mine = call(
-        own_kernel, [square, wide, wide, pair, pair], flops=2 * rows * width * head * 2, smem=(7,), n=9,
-    )(normed, ret_query, jnp.swapaxes(diff_query, 1, 2), packed, ret_k, ret_v, decay_log, diff_lambda, init_state)
-    (partial,) = call(
-        lambda *refs: finish_kernel(count, *refs), [shape((rows, width), BF16)],
-        flops=2 * rows * width * head * 2, smem=(5,), n=8 + 2 * count,
-    )(*mine, diff_lambda, init_state, ret_gain[None, :], diff_gain[None, :], *blocks, *weights)
-    shares = lax.all_to_all(partial, ("fs", "tp"), 0, 0, tiled=True)
-    return shares.reshape(group, own_rows, width).astype(F32).sum(axis=0).astype(BF16)
+    mine = call(own_kernel, [square, wide, wide, pair, pair, shape((8, head), F32)], 2 * rows * width * head * 2, 8, scalars=1)(
+        diff_lambda, normed, packed, ret_k, ret_v, query_scale, fade, ret_query, jnp.swapaxes(diff_query, 1, 2)
+    )
+    cores = lax.axis_size("tp")
+    keep, send = call(
+        functools.partial(finish_kernel, sources), [shape((rows // 2, width), F32), shape((rows // 2, width), BF16)],
+        2 * rows * width * head * 2, 7 + 2 * count,
+        scratch=[pltpu.VMEM((group // cores, cores, own_rows, 2 * head), BF16)],
+    )(*mine, small, init, *blocks, *weights)
+    other = lax.ppermute(send, "tp", [(0, 1), (1, 0)])
+    both = (keep + other.astype(F32)).astype(BF16)
+    shares = lax.all_to_all(both, "fs", 0, 0, tiled=True)
+    return shares.reshape(group // cores, own_rows, width).astype(F32).sum(axis=0).astype(BF16)
 
 
 def local_many(
@@ -272,5 +335,5 @@
         P(None, ("fs", "tp"), "sp"),
     )
     out_specs = P(("sp", "fs", "tp"), None)
-    local = local_few if few(count) else local_many
+    local = local_few if few(count) and mesh.shape["tp"] == 2 else local_many
     return jax.shard_map(local, mesh=mesh, in_specs=in_specs, out_specs=out_specs, check_vma=False)

time: 60.6 us -> 54.8 us (0.904)
  local copies, waits for them, and re-layouts: 4.45 us -> 0.04 us
  blocking collectives: 22.5 us -> 18.7 us
  waiting for transfers between devices: 17.4 us -> 18.9 us
  Pallas kernels: 3.48 us -> 4.53 us
    unnamed x24 -> x14, local copies, waits for them, and re-layouts: 4.45 us -> 0.04 us
    all_to_all x1, blocking collectives: 12.2 us -> 8.68 us  [local_few(): shares = lax.all_to_all(both, 'fs', 0, 0, tiled=True)]
    ppermute x3 -> x4, waiting for transfers between devices: 7.49 us -> 9 us  [the longest x3 7.51 us: local_few(): blocks.append(lax.ppermute(packed, 'sp', pairs))]
    pallas_call x3 -> x4, Pallas kernels: 3.48 us -> 4.53 us  [placed(): run(*[a if spot is pltpu.SMEM else pltpu.with_memory_space_constraint(a,...]
    ppermute x3 -> x4, starting transfers between devices: 4.5 us -> 4.62 us  [the longest x3 4.5 us: local_few(): blocks.append(lax.ppermute(packed, 'sp', pairs))]
  transfers between devices with their start and end apart: 6 -> 7, of which waited for: 3 -> 4; matrix products, arithmetic and copies ran while one was open for 0% -> 0% of each run, Pallas kernels for 4% -> 6%
where the time goes in v1:
time: 54.8 us; the launch traced here: 54.6 us
  waiting for transfers between devices  18.9 us (34%)
  blocking collectives  18.7 us (34%)
  starting transfers between devices  10.9 us (20%)
  Pallas kernels  4.53 us (8%)
  between operations  0.78 us (1%)
  other arithmetic  0.72 us (1%)
    all_gather x1, blocking collectives, local_few(): gathered = lax.all_gather(staged, ('fs', 'tp'), axis=0, tiled=True)  9.99 us
    ppermute x3, waiting for transfers between devices, swapped(): return lax.ppermute(array, 'sp', [(i, i ^ k) for i in range(count)])  9.92 us
    all_to_all x1, blocking collectives, local_few(): shares = lax.all_to_all(both, 'fs', 0, 0, tiled=True)  8.68 us
    ppermute x3, waiting for transfers between devices, local_few(): blocks.append(lax.ppermute(packed, 'sp', pairs))  7.51 us
    ppermute x3, starting transfers between devices, swapped(): return lax.ppermute(array, 'sp', [(i, i ^ k) for i in range(count)])  6.32 us
    pallas_call x4, Pallas kernels, placed(): run(*[a if spot is pltpu.SMEM else pltpu.with_memory_space_constraint(a,...  4.53 us
    ppermute x3, starting transfers between devices, local_few(): blocks.append(lax.ppermute(packed, 'sp', pairs))  4.5 us
    ppermute x1, waiting for transfers between devices, local_few(): other = lax.ppermute(send, 'tp', [(0, 1), (1, 0)])  1.49 us
  transfers between devices with their start and end apart: 7, of which 4 were waited for; matrix products, arithmetic and copies ran while one was open for 0% of the time, Pallas kernels for 6%

profile of v1, /device:TPU:16, one launch (start us, length us, event | category | flops | bytes accessed | tf_op | source)
XLA Modules:
  0.0 54.6 jit_solution(5687539579372545872)
XLA Ops:
  0.0 0.0 collective-permute-start.4
  0.0 1.9 %collective-permute-start.3 = (bf16[2,128,512]{2,1,0:T(8,128)(2,1)}, bf16[2,128,512]{2,1,0:T(8,128)(2,1)S(1)}, u32[]{:S(2)}, u32[]{:S(2)}) collective-permute-start(bf16[2,128,512]{2,1,0:T(8,128)(2,1)} %refs_11_.1), channel_id=1, source_target_pairs={{0,8},{8,0},{16,24},{24,16},{1,9},{9,1},{17,25},{25,17},{2,10},{10... | collective-permute-start | bytes 786440 | tf_op jit(solution)/shard_map/ppermute | solution.py:220
  1.9 9.9 %collective-permute-done.4.refs_13_ = bf16[2,128,512]{2,1,0:T(8,128)(2,1)S(1)} collective-permute-done((bf16[2,128,512]{2,1,0:T(8,128)(2,1)}, bf16[2,128,512]{2,1,0:T(8,128)(2,1)S(1)}, u32[]{:S(2)}, u32[]{:S(2)}) %collective-permute-start.4) | collective-permute-done | bytes 262176 | tf_op jit(solution)/shard_map/ppermute | solution.py:220
  11.8 4.4 %collective-permute-start.5 = (bf16[2,128,512]{2,1,0:T(8,128)(2,1)S(1)}, bf16[2,128,512]{2,1,0:T(8,128)(2,1)S(1)}, u32[]{:S(2)}, u32[]{:S(2)}) collective-permute-start(bf16[2,128,512]{2,1,0:T(8,128)(2,1)S(1)} %collective-permute-done.4.refs_13_), channel_id=1, source_target_pairs={{0,8},{8,0},{16,24},{24,16},{1,9},{9,1},{17,25},{25,17},{2,10},{10... | collective-permute-start | bytes 786440 | tf_op jit(solution)/shard_map/ppermute | solution.py:220
  16.2 0.0 copy-start.3
  16.2 0.0 copy-start.4
  16.2 0.0 copy-start.5
  16.2 1.0 %shard_map.136 = (bf16[16,2048]{1,0:T(8,128)(2,1)S(1)}, f32[128,128]{1,0:T(8,128)S(1)}, f32[128,128]{1,0:T(8,128)S(1)}, f32[128,128]{1,0:T(8,128)S(1)}, f32[8,12...) custom-call(bf16[16,2048]{1,0:T(8,128)(2,1)} %tokens_h.1, ...), custom_call_target="tpu_custom_call" | custom-call | flops 10000000000 | bytes 1048576 | tf_op jit(solution)/shard_map/pallas_call | solution.py:199
  17.3 0.0 copy-start.2
  17.3 10.0 %all_gather.3.x = bf16[128,2048]{1,0:T(8,128)(2,1)S(1)} all-gather(bf16[16,2048]{1,0:T(8,128)(2,1)S(1)} %get-tuple-element.25), channel_id=1, replica_groups=mesh['sp'=4,'fs'=4,'tp'=2] {'fs','tp'}, dimensions={0}, use_global_device_ids=true | all-gather | bytes 589824 | tf_op jit(solution)/shard_map/all_gather | solution.py:236
  27.3 0.0 copy-done.3
  27.3 0.0 copy-done.4
  27.3 0.0 copy-done.5
  27.3 0.0 copy-done.2
  27.3 0.0 copy-start
  27.3 0.0 copy-start.1
  27.3 1.1 %shard_map.137 = (bf16[128,2048]{1,0:T(8,128)(2,1)S(1)}, bf16[392,128]{1,0:T(8,128)(2,1)S(1)}, bf16[128,128]{1,0:T(8,128)(2,1)S(1)}, bf16[128,128]{1,0:T(8,128)(2,1)S(1)}) custom-call(bf16[128,2048]{1,0:T(8,128)(2,1)S(1)} %all_gather.3.x, f32[1,2048]{1,0:T(1,128)S(1)} %get-tuple-element.26.gain, f32[128,128]{1,0:T(8,128)S(1)} %get-tuple-element.27.key_scale, ...), custom_call_target="tpu_custom_call" | custom-call | flops 268435456 | bytes 1048576 | tf_op jit(solution)/shard_map/pallas_call | solution.py:199
  28.5 0.7 %collective-permute-start.2 = (bf16[392,128]{1,0:T(8,128)(2,1)S(1)}, bf16[392,128]{1,0:T(8,128)(2,1)S(1)}, u32[]{:S(2)}, u32[]{:S(2)}) collective-permute-start(bf16[392,128]{1,0:T(8,128)(2,1)S(1)} %get-tuple-element.30.packed), channel_id=1, source_target_pairs={{0,24},{1,25},{2,26},{3,27},{4,28},{5,29},{6,30},{7,31}} | collective-permute-start | bytes 301064 | tf_op jit(solution)/shard_map/ppermute | solution.py:245
  29.1 1.3 %collective-permute-start.1 = (bf16[392,128]{1,0:T(8,128)(2,1)S(1)}, bf16[392,128]{1,0:T(8,128)(2,1)S(1)}, u32[]{:S(2)}, u32[]{:S(2)}) collective-permute-start(bf16[392,128]{1,0:T(8,128)(2,1)S(1)} %get-tuple-element.30.packed), channel_id=1, source_target_pairs={{0,16},{8,24},{1,17},{9,25},{2,18},{10,26},{3,19},{11,27},{4,20},{... | collective-permute-start | bytes 301064 | tf_op jit(solution)/shard_map/ppermute | solution.py:245
  30.4 2.5 %collective-permute-start = (bf16[392,128]{1,0:T(8,128)(2,1)S(1)}, bf16[392,128]{1,0:T(8,128)(2,1)S(1)}, u32[]{:S(2)}, u32[]{:S(2)}) collective-permute-start(bf16[392,128]{1,0:T(8,128)(2,1)S(1)} %get-tuple-element.30.packed), channel_id=1, source_target_pairs={{0,8},{8,16},{16,24},{1,9},{9,17},{17,25},{2,10},{10,18},{18,26},{... | collective-permute-start | bytes 301064 | tf_op jit(solution)/shard_map/ppermute | solution.py:245
  33.6 0.0 copy-done
  33.6 0.0 copy-done.1
  33.6 0.0 copy-start.6
  33.7 1.1 %shard_map.138 = (bf16[128,128]{1,0:T(8,128)(2,1)S(1)}, f32[128,128]{1,0:T(8,128)S(1)}, f32[128,128]{1,0:T(8,128)S(1)}, f32[2,128,128]{2,1,0:T(8,128)S(1)}, f32[...) custom-call(f32[1]{0:T(128)S(6)} %copy.15.lam, bf16[128,2048]{1,0:T(8,128)(2,1)S(1)} %get-tuple-element.29.normed, ...), custom_call_target="tpu_custom_call" | custom-call | flops 134217728 | bytes 1048576 | tf_op jit(solution)/shard_map/pallas_call | solution.py:199
  34.7 0.0 collective-permute-done.2.refs_10_
  34.7 3.9 %collective-permute-done.1.refs_9_ = bf16[392,128]{1,0:T(8,128)(2,1)S(1)} collective-permute-done((bf16[392,128]{1,0:T(8,128)(2,1)S(1)}, bf16[392,128]{1,0:T(8,128)(2,1)S(1)}, u32[]{:S(2)}, u32[]{:S(2)}) %collective-permute-start.1) | collective-permute-done | bytes 100384 | tf_op jit(solution)/shard_map/ppermute | solution.py:245
  38.6 3.7 %collective-permute-done.refs_8_ = bf16[392,128]{1,0:T(8,128)(2,1)S(1)} collective-permute-done((bf16[392,128]{1,0:T(8,128)(2,1)S(1)}, bf16[392,128]{1,0:T(8,128)(2,1)S(1)}, u32[]{:S(2)}, u32[]{:S(2)}) %collective-permute-start) | collective-permute-done | bytes 100384 | tf_op jit(solution)/shard_map/ppermute | solution.py:245
  42.3 0.0 collective-permute-done.3.refs_12_
  42.3 0.0 collective-permute-done.5.refs_14_
  42.3 0.0 copy-done.6
  42.3 1.3 %shard_map.139 = (f32[64,2048]{1,0:T(8,128)S(1)}, bf16[64,2048]{1,0:T(8,128)(2,1)S(1)}) custom-call(bf16[128,128]{1,0:T(8,128)(2,1)S(1)} %get-tuple-element.35.refs_0_, f32[128,128]{1,0:T(8,128)S(1)} %get-tuple-element.36.refs_1_, f32[128,128]{1,0:T(8,128)S(1)} %get-tuple-element.37.refs_2_, f32[2,128,128]{2,1,0:T(8,128)S(1)} %get-tuple-element.38.refs_3_, ...), custom_call_target="tpu_custom_call" | custom-call | flops 134217728 | bytes 1048576 | tf_op jit(solution)/shard_map/pallas_call | solution.py:199
  43.6 0.1 collective-permute-start.6
  43.7 1.5 %collective-permute-done.6 = bf16[64,2048]{1,0:T(8,128)(2,1)S(1)} collective-permute-done((bf16[64,2048]{1,0:T(8,128)(2,1)S(1)}, bf16[64,2048]{1,0:T(8,128)(2,1)S(1)}, u32[]{:S(2)}, u32[]{:S(2)}) %collective-permute-start.6) | collective-permute-done | bytes 262176 | tf_op jit(solution)/shard_map/ppermute | solution.py:256
  45.2 8.7 %all_to_all.9 = bf16[4,16,2048]{2,1,0:T(8,128)(2,1)S(1)} all-to-all(bf16[4,16,2048]{2,1,0:T(8,128)(2,1)S(1)} %bitcast.8), channel_id=1, replica_groups=mesh['sp'=4,'fs'=4,'tp'=2] {'fs'}, dimensions={0} | all-to-all | bytes 524288 | tf_op jit(solution)/shard_map/all_to_all | solution.py:258
  53.9 0.7 %reduce_sum.12 = bf16[16,2048]{1,0:T(8,128)(2,1)} reduce(bf16[4,16,2048]{2,1,0:T(8,128)(2,1)S(1)} %all_to_all.9, bf16[]{:T(256)} %constant.2.clone.1), dimensions={0}, to_apply=%region_0.0 | reduce | flops 98304 | bytes 327682 | tf_op jit(solution)/shard_map/reduce_sum | solution.py:259
  (1 shorter events, 0.0 us)
Async XLA Ops:
  0.0 11.8 %collective-permute-start.4 = (bf16[2,128,512]{2,1,0:T(8,128)(2,1)}, bf16[2,128,512]{2,1,0:T(8,128)(2,1)S(1)}, u32[]{:S(2)}, u32[]{:S(2)}) collective-permute-start(bf16[2,128,512]{2,1,0:T(8,128)(2,1)} %refs_11_.1), channel_id=1, source_target_pairs={{0,16},{8,24},{16,0},{24,8},{1,17},{9,25},{17,1},{25,9},{2,18},{10... | collective-permute-start | bytes 786440 | tf_op jit(solution)/shard_map/ppermute | solution.py:220
  0.0 42.3 %collective-permute-start.3 = (bf16[2,128,512]{2,1,0:T(8,128)(2,1)}, bf16[2,128,512]{2,1,0:T(8,128)(2,1)S(1)}, u32[]{:S(2)}, u32[]{:S(2)}) collective-permute-start(bf16[2,128,512]{2,1,0:T(8,128)(2,1)} %refs_11_.1), channel_id=1, source_target_pairs={{0,8},{8,0},{16,24},{24,16},{1,9},{9,1},{17,25},{25,17},{2,10},{10... | collective-permute-start | bytes 786440 | tf_op jit(solution)/shard_map/ppermute | solution.py:220
  11.8 30.4 %collective-permute-start.5 = (bf16[2,128,512]{2,1,0:T(8,128)(2,1)S(1)}, bf16[2,128,512]{2,1,0:T(8,128)(2,1)S(1)}, u32[]{:S(2)}, u32[]{:S(2)}) collective-permute-start(bf16[2,128,512]{2,1,0:T(8,128)(2,1)S(1)} %collective-permute-done.4.refs_13_), channel_id=1, source_target_pairs={{0,8},{8,0},{16,24},{24,16},{1,9},{9,1},{17,25},{25,17},{2,10},{10... | collective-permute-start | bytes 786440 | tf_op jit(solution)/shard_map/ppermute | solution.py:220
  16.2 11.1 %copy-start.3 = (bf16[2048,128]{1,0:T(8,128)(2,1)S(1)}, bf16[2048,128]{1,0:T(8,128)(2,1)}, u32[]{:S(2)}) copy-start(bf16[2048,128]{1,0:T(8,128)(2,1)} %dv.1) | copy-start | bytes 1572868
  16.2 11.1 %copy-start.4 = (bf16[2048,128]{1,0:T(8,128)(2,1)S(1)}, bf16[2048,128]{1,0:T(8,128)(2,1)}, u32[]{:S(2)}) copy-start(bf16[2048,128]{1,0:T(8,128)(2,1)} %wk.1) | copy-start | bytes 1572868
  16.2 11.1 %copy-start.5 = (bf16[2048,128]{1,0:T(8,128)(2,1)S(1)}, bf16[2048,128]{1,0:T(8,128)(2,1)}, u32[]{:S(2)}) copy-start(bf16[2048,128]{1,0:T(8,128)(2,1)} %wv.1) | copy-start | bytes 1572868
  17.3 10.0 %copy-start.2 = (bf16[2,2048,64]{1,2,0:T(8,128)(2,1)S(1)}, bf16[2,2048,64]{1,2,0:T(8,128)(2,1)}, u32[]{:S(2)}) copy-start(bf16[2,2048,64]{1,2,0:T(8,128)(2,1)} %param.23) | copy-start | bytes 1572868
  27.3 6.3 %copy-start = (bf16[2048,128]{1,0:T(8,128)(2,1)S(1)}, bf16[2048,128]{1,0:T(8,128)(2,1)}, u32[]{:S(2)}) copy-start(bf16[2048,128]{1,0:T(8,128)(2,1)} %wq.1) | copy-start | bytes 1572868
  27.3 6.3 %copy-start.1 = (bf16[2,2048,64]{1,2,0:T(8,128)(2,1)S(1)}, bf16[2,2048,64]{1,2,0:T(8,128)(2,1)}, u32[]{:S(2)}) copy-start(bf16[2,2048,64]{1,2,0:T(8,128)(2,1)} %param.22) | copy-start | bytes 1572868
  28.5 6.3 %collective-permute-start.2 = (bf16[392,128]{1,0:T(8,128)(2,1)S(1)}, bf16[392,128]{1,0:T(8,128)(2,1)S(1)}, u32[]{:S(2)}, u32[]{:S(2)}) collective-permute-start(bf16[392,128]{1,0:T(8,128)(2,1)S(1)} %get-tuple-element.30.packed), channel_id=1, source_target_pairs={{0,24},{1,25},{2,26},{3,27},{4,28},{5,29},{6,30},{7,31}} | collective-permute-start | bytes 301064 | tf_op jit(solution)/shard_map/ppermute | solution.py:245
  29.1 9.5 %collective-permute-start.1 = (bf16[392,128]{1,0:T(8,128)(2,1)S(1)}, bf16[392,128]{1,0:T(8,128)(2,1)S(1)}, u32[]{:S(2)}, u32[]{:S(2)}) collective-permute-start(bf16[392,128]{1,0:T(8,128)(2,1)S(1)} %get-tuple-element.30.packed), channel_id=1, source_target_pairs={{0,16},{8,24},{1,17},{9,25},{2,18},{10,26},{3,19},{11,27},{4,20},{... | collective-permute-start | bytes 301064 | tf_op jit(solution)/shard_map/ppermute | solution.py:245
  30.4 11.8 %collective-permute-start = (bf16[392,128]{1,0:T(8,128)(2,1)S(1)}, bf16[392,128]{1,0:T(8,128)(2,1)S(1)}, u32[]{:S(2)}, u32[]{:S(2)}) collective-permute-start(bf16[392,128]{1,0:T(8,128)(2,1)S(1)} %get-tuple-element.30.packed), channel_id=1, source_target_pairs={{0,8},{8,16},{16,24},{1,9},{9,17},{17,25},{2,10},{10,18},{18,26},{... | collective-permute-start | bytes 301064 | tf_op jit(solution)/shard_map/ppermute | solution.py:245
  33.6 8.6 %copy-start.6 = (bf16[2,128,512]{2,1,0:T(8,128)(2,1)S(1)}, bf16[2,128,512]{2,1,0:T(8,128)(2,1)}, u32[]{:S(2)}) copy-start(bf16[2,128,512]{2,1,0:T(8,128)(2,1)} %refs_11_.1) | copy-start | bytes 786436
  43.6 1.6 %collective-permute-start.6 = (bf16[64,2048]{1,0:T(8,128)(2,1)S(1)}, bf16[64,2048]{1,0:T(8,128)(2,1)S(1)}, u32[]{:S(2)}, u32[]{:S(2)}) collective-permute-start(bf16[64,2048]{1,0:T(8,128)(2,1)S(1)} %get-tuple-element.44), channel_id=1, source_target_pairs={{0,1},{1,0},{2,3},{3,2},{4,5},{5,4},{6,7},{7,6},{8,9},{9,8},{10,11... | collective-permute-start | bytes 786440 | tf_op jit(solution)/shard_map/ppermute | solution.py:256

commit v2 on v1

--- a/solution.py
+++ b/solution.py
@@ -14,7 +14,7 @@
 F32 = jnp.float32
 BF16 = jnp.bfloat16
 
-GATHER_FLOPS = 10**10
+GATHER_FLOPS = 3 * 10**10
 
 
 def dot(a, b, dims, **kw):
@@ -56,66 +56,56 @@
     return down, along
 
 
-def fetch(pairs, sems):
-    copies = [pltpu.make_async_copy(src, dst, sems.at[i]) for i, (src, dst) in enumerate(pairs)]
-    for copy in copies:
-        copy.start()
-    return copies
-
-
-def prepare_kernel(
-    tokens_h, decay_h, in_gain_h, ret_gain_h, diff_gain_h, init_h,
-    tokens, key_scale, query_scale, fade, factor, in_gain, small, init, decay, ret_gain, diff_gain, start, sems,
+def mark_kernel(done):
+    done[...] = jnp.zeros_like(done)
+
+
+def project_kernel(
+    x0, x1, x2, x3, y0, y1, y2, y3, gain, decay, dk, dv, wk, wv, done, normed, packed, ret_k, ret_v
 ):
-    head = fade.shape[0]
-    copies = fetch(
-        [(decay_h, decay), (tokens_h, tokens), (in_gain_h, in_gain), (ret_gain_h, ret_gain), (diff_gain_h, diff_gain), (init_h, start)],
-        sems,
-    )
-    copies[0].wait()
-    cumul, along = cumulated(decay[...])
-    rows = cumul.shape[0]
-    last = cumul[rows - 1 :, :]
-    key_scale[...] = jnp.broadcast_to(jnp.exp(last - cumul) * head ** (-0.5), (rows, head))
-    query_scale[...] = jnp.broadcast_to(jnp.exp(cumul), (rows, head))
-    fade[...] = jnp.exp(jnp.where(at_or_before(rows), cumul - along, -HUGE)) * head ** (-0.5)
-    factor[...] = jnp.broadcast_to(jnp.exp(last), (8, head))
-    for copy in copies[1:]:
-        copy.wait()
-    small[0:8, :] = jnp.broadcast_to(ret_gain[...], (8, head))
-    small[8:16, :] = jnp.broadcast_to(diff_gain[...], (8, head))
-    init[...] = start[0].astype(F32)
-
-
-def project_kernel(x, gain, key_scale, factor, dk, dv, wk, wv, normed, packed, ret_k, ret_v):
     rows, head = ret_k.shape
-    wide = x[...].astype(F32)
-    scale = lax.rsqrt(jnp.mean(wide * wide, axis=-1, keepdims=True) + EPS)
-    rounded = (wide * scale * gain[...]).astype(BF16)
-    normed[...] = rounded
+    chip = lax.axis_index("fs")
+    core = lax.axis_index("tp")
+    for j, side in enumerate(((x0, x1, x2, x3), (y0, y1, y2, y3))):
+        for k, piece in enumerate(side):
+            own = piece.shape[0]
+            wide = piece[...].astype(F32)
+            scale = lax.rsqrt(jnp.mean(wide * wide, axis=-1, keepdims=True) + EPS)
+            at = pl.multiple_of(((chip ^ k) * 2 + (core ^ j)) * own, own)
+            normed[pl.ds(at, own), :] = (wide * scale * gain[...]).astype(BF16)
+    rounded = normed[...]
     packed[0:rows, :] = nt(rounded, dk[...].reshape(-1, dk.shape[2])).astype(BF16)
     packed[rows : 2 * rows, :] = nn(rounded, dv[...]).astype(BF16)
     k = nn(rounded, wk[...]).astype(BF16)
     v = nn(rounded, wv[...]).astype(BF16)
     ret_k[...] = k
     ret_v[...] = v
-    state = tn(k.astype(F32) * key_scale[...], v.astype(F32), precision=HIGHEST)
+    cumul, _ = cumulated(decay[...])
+    last = cumul[rows - 1 :, :]
+    state = tn(k.astype(F32) * (jnp.exp(last - cumul) * head ** (-0.5)), v.astype(F32), precision=HIGHEST)
     packed[2 * rows : 2 * rows + head, :] = state.astype(BF16)
-    packed[2 * rows + head :, :] = factor[...].astype(BF16)
-
-
-def own_kernel(lam, normed, packed, ret_k, ret_v, query_scale, fade, wq, dq, queries, scaled, inner, sums, stats, second):
+    packed[2 * rows + head :, :] = jnp.broadcast_to(jnp.exp(last), (8, head)).astype(BF16)
+
+
+def own_kernel(
+    lam, normed, packed, ret_k, ret_v, decay, wq, dq, ret_gain, diff_gain, start,
+    queries, scaled, inner, sums, stats, small, init,
+):
     rows, head = ret_k.shape
-    second[...] = jnp.full(second.shape, lam[0])
+    small[0:8, :] = jnp.broadcast_to(ret_gain[...], (8, head))
+    small[8:16, :] = jnp.broadcast_to(diff_gain[...], (8, head))
+    small[16:24, :] = jnp.full((8, head), lam[0])
+    init[...] = start[0].astype(F32)
     x = normed[...]
+    cumul, along = cumulated(decay[...])
+    lower = at_or_before(rows)
     q = nn(x, wq[...]).astype(BF16)
-    weights = nt(q, ret_k[...]) * fade[...]
+    weights = nt(q, ret_k[...]) * head ** (-0.5) * jnp.exp(jnp.where(lower, cumul - along, -HUGE))
     inner[...] = nn(weights.astype(BF16), ret_v[...])
-    scaled[...] = q.astype(F32) * query_scale[...]
+    scaled[...] = q.astype(F32) * jnp.exp(cumul)
     both = nt(x, dq[...].reshape(-1, dq.shape[2])).astype(BF16)
     queries[...] = both
     half = head // 2
-    lower = at_or_before(rows)
     keys = packed[0:rows, :]
     values = packed[rows : 2 * rows, :]
     for m in range(2):
@@ -129,14 +119,16 @@
 
 def finish_kernel(sources, *refs):
     count = len(sources) + 1
-    queries, scaled, inner, sums, stats, second, small, init = refs[:8]
-    blocks = refs[8 : 7 + count]
-    weights = refs[7 + count : 7 + 2 * count]
-    keep, send, mixed = refs[7 + 2 * count :]
+    queries, scaled, inner, sums, stats, small, init = refs[:7]
+    blocks = refs[7 : 6 + count]
+    weights = refs[6 + count : 6 + 2 * count]
+    *outs, mixed = refs[6 + 2 * count :]
+    keeps, sends = outs[: len(outs) // 2], outs[len(outs) // 2 :]
     rows, head = inner.shape
     half = head // 2
     place = lax.axis_index("sp")
     core = lax.axis_index("tp")
+    chip = lax.axis_index("fs")
     source = [f(place) for f in sources]
     before = [jnp.logical_and(at >= 0, at < place) for at in source]
     factors = [b[2 * rows + head : 2 * rows + head + 8, :].astype(F32)[0:1, :] for b in blocks]
@@ -168,19 +160,21 @@
         kept = jnp.exp(old_top - top)
         total = old_total * kept + jnp.sum(e, axis=-1, keepdims=True)
         maps.append((sums[m] * kept + nn(e.astype(BF16), values)) / total)
-    diff_out = maps[0] - second[0:1, :] * maps[1]
+    diff_out = maps[0] - small[16:17, :] * maps[1]
     level = lax.rsqrt(jnp.mean(diff_out * diff_out, axis=-1, keepdims=True) + EPS)
     diff_mix = (diff_out * level * small[8:9, :]).astype(BF16)
 
     mixed[:, :, :, :head] = ret_mix.reshape(mixed.shape[:3] + (head,))
     mixed[:, :, :, head:] = diff_mix.reshape(mixed.shape[:3] + (head,))
-    ordered = jnp.concatenate([mixed[:, core].reshape(-1, 2 * head), mixed[:, 1 - core].reshape(-1, 2 * head)], axis=0)
+    ordered = jnp.concatenate([mixed[chip ^ k, core ^ j] for j in range(2) for k in range(mixed.shape[0])], axis=0)
     for k, w in enumerate(weights):
         cols = w.shape[2]
         at = pl.ds(pl.multiple_of((place ^ k) * cols, cols), cols)
         result = nn(ordered, w[...].reshape(2 * head, cols))
-        keep[:, at] = result[: rows // 2]
-        send[:, at] = result[rows // 2 :].astype(BF16)
+        own = keeps[0].shape[0]
+        for i, (keep, send) in enumerate(zip(keeps, sends)):
+            keep[:, at] = result[i * own : (i + 1) * own]
+            send[:, at] = result[rows // 2 + i * own : rows // 2 + (i + 1) * own].astype(BF16)
 
 
 def call(kernel, outs, flops, here, away=0, scratch=(), scalars=0):
@@ -225,38 +219,54 @@
         weights[2] = swapped(out_weight, 2)
         weights[3] = swapped(weights[2], 1)
     square = shape((rows, head), BF16)
-    wide = shape((rows, head), F32)
-    line = pltpu.VMEM((1, head), F32)
-    staged, key_scale, query_scale, fade, factor, gain, small, init = call(
-        prepare_kernel,
-        [shape(tokens.shape, BF16), wide, wide, shape((rows, rows), F32), shape((8, head), F32),
-         shape((1, width), F32), shape((16, head), F32), shape((head, head), F32)],
-        GATHER_FLOPS, 0, 6, [line, line, line, pltpu.VMEM((1, head, head), BF16)],
-    )(tokens, decay_log, in_gain[None, :], ret_gain[None, :], diff_gain[None, :], init_state)
-    gathered = lax.all_gather(staged, ("fs", "tp"), axis=0, tiled=True)
+    chips = lax.axis_size("fs")
+
+    def across(array, k):
+        return lax.ppermute(array, "fs", [(i, i ^ k) for i in range(chips)])
+
+    def paired(array):
+        return lax.ppermute(array, "tp", [(0, 1), (1, 0)])
+
+    (done,) = call(mark_kernel, [shape((8, head), F32)], GATHER_FLOPS, 0)()
+    near_rows, far_rows = [tokens], []
+    for k in range(1, chips):
+        near_rows.append(across(tokens, k))
+    for k in range(chips):
+        far_rows.append(paired(near_rows[k]))
     normed, packed, ret_k, ret_v = call(
         project_kernel, [shape((rows, width), BF16), shape((2 * rows + head + 8, head), BF16), square, square],
-        2 * rows * width * head * 4, 8,
-    )(gathered, gain, key_scale, factor, jnp.swapaxes(diff_key, 1, 2), diff_value, ret_key, ret_value)
+        2 * rows * width * head * 4, 15,
+    )(
+        *near_rows, *far_rows, in_gain[None, :], decay_log, jnp.swapaxes(diff_key, 1, 2), diff_value,
+        ret_key, ret_value, done,
+    )
     blocks, sources = [], []
     for d in range(1, count):
         pairs, source = route(d, count)
         sources.append(source)
         blocks.append(lax.ppermute(packed, "sp", pairs))
+    wide = shape((rows, head), F32)
     pair = shape((2, rows, head), F32)
-    mine = call(own_kernel, [square, wide, wide, pair, pair, shape((8, head), F32)], 2 * rows * width * head * 2, 8, scalars=1)(
-        diff_lambda, normed, packed, ret_k, ret_v, query_scale, fade, ret_query, jnp.swapaxes(diff_query, 1, 2)
+    mine = call(
+        own_kernel, [square, wide, wide, pair, pair, shape((24, head), F32), shape((head, head), F32)],
+        2 * rows * width * head * 2, 10, scalars=1,
+    )(
+        diff_lambda, normed, packed, ret_k, ret_v, decay_log, ret_query, jnp.swapaxes(diff_query, 1, 2),
+        ret_gain[None, :], diff_gain[None, :], init_state,
     )
-    cores = lax.axis_size("tp")
-    keep, send = call(
-        functools.partial(finish_kernel, sources), [shape((rows // 2, width), F32), shape((rows // 2, width), BF16)],
-        2 * rows * width * head * 2, 7 + 2 * count,
-        scratch=[pltpu.VMEM((group // cores, cores, own_rows, 2 * head), BF16)],
-    )(*mine, small, init, *blocks, *weights)
-    other = lax.ppermute(send, "tp", [(0, 1), (1, 0)])
-    both = (keep + other.astype(F32)).astype(BF16)
-    shares = lax.all_to_all(both, "fs", 0, 0, tiled=True)
-    return shares.reshape(group // cores, own_rows, width).astype(F32).sum(axis=0).astype(BF16)
+    part = (own_rows, width)
+    outs = call(
+        functools.partial(finish_kernel, sources), [shape(part, F32)] * chips + [shape(part, BF16)] * chips,
+        2 * rows * width * head * 2, 6 + 2 * count, scratch=[pltpu.VMEM((chips, 2, own_rows, 2 * head), BF16)],
+    )(*mine, *blocks, *weights)
+    sums = []
+    for k in range(chips):
+        other = paired(outs[chips + k])
+        sums.append(outs[k] + other.astype(F32))
+    total = sums[0]
+    for k in range(1, chips):
+        total = total + across(sums[k].astype(BF16), k).astype(F32)
+    return total.astype(BF16)
 
 
 def local_many(
@@ -335,5 +345,8 @@
         P(None, ("fs", "tp"), "sp"),
     )
     out_specs = P(("sp", "fs", "tp"), None)
-    local = local_few if few(count) and mesh.shape["tp"] == 2 else local_many
-    return jax.shard_map(local, mesh=mesh, in_specs=in_specs, out_specs=out_specs, check_vma=False)
+    local = local_few if few(count) and mesh.shape["fs"] == 4 and mesh.shape["tp"] == 2 else local_many
+    step = jax.shard_map(local, mesh=mesh, in_specs=in_specs, out_specs=out_specs, check_vma=False)
+    if local is local_many or count != 4:
+        return step
+    return step

time: 54.8 us -> 43.8 us (0.80)
  blocking collectives: 18.7 us -> 0 us
  starting transfers between devices: 10.9 us -> 19.8 us
  waiting for transfers between devices: 18.9 us -> 17.4 us
  local copies, waits for them, and re-layouts: 0.04 us -> 1.28 us
  Pallas kernels: 4.53 us -> 3.51 us
    all_gather x1 -> x0, blocking collectives: 9.99 us -> none  [local_few(): gathered = lax.all_gather(staged, ('fs', 'tp'), axis=0, tiled=True)]
    ppermute x1 -> x14, starting transfers between devices: 0.11 us -> 8.84 us  [the longest x6 7.24 us: across(): return lax.ppermute(array, 'fs', [(i, i ^ k) for i in range(chips)])]
    all_to_all x1 -> x0, blocking collectives: 8.68 us -> none  [local_few(): shares = lax.all_to_all(both, 'fs', 0, 0, tiled=True)]
    ppermute x3, waiting for transfers between devices: 9.92 us -> 3.56 us  [swapped(): return lax.ppermute(array, 'sp', [(i, i ^ k) for i in range(count)])]
    ppermute x1 -> x14, waiting for transfers between devices: 1.49 us -> 7.25 us  [the longest x6 7 us: across(): return lax.ppermute(array, 'fs', [(i, i ^ k) for i in range(chips)])]
    unnamed x14 -> x26, local copies, waits for them, and re-layouts: 0.04 us -> 1.28 us
    pallas_call x4, Pallas kernels: 4.53 us -> 3.51 us  [placed(): run(*[a if spot is pltpu.SMEM else pltpu.with_memory_space_constraint(a,...]
    ppermute x3, waiting for transfers between devices: 7.51 us -> 6.55 us  [local_few(): blocks.append(lax.ppermute(packed, 'sp', pairs))]
  transfers between devices with their start and end apart: 7 -> 20, of which waited for: 4 -> 9; matrix products, arithmetic and copies ran while one was open for 0% -> 0% of each run, Pallas kernels for 6% -> 5%
where the time goes in v2:
time: 43.8 us; the launch traced here: 43.5 us
  starting transfers between devices  19.8 us (45%)
  waiting for transfers between devices  17.4 us (40%)
  Pallas kernels  3.51 us (8%)
  local copies, waits for them, and re-layouts  1.28 us (3%)
  between operations  0.86 us (2%)
  other arithmetic  0.74 us (2%)
    ppermute x6, starting transfers between devices, across(): return lax.ppermute(array, 'fs', [(i, i ^ k) for i in range(chips)])  7.24 us
    ppermute x6, waiting for transfers between devices, across(): return lax.ppermute(array, 'fs', [(i, i ^ k) for i in range(chips)])  7 us
    ppermute x3, waiting for transfers between devices, local_few(): blocks.append(lax.ppermute(packed, 'sp', pairs))  6.55 us
    ppermute x3, starting transfers between devices, swapped(): return lax.ppermute(array, 'sp', [(i, i ^ k) for i in range(count)])  6.45 us
    ppermute x3, starting transfers between devices, local_few(): blocks.append(lax.ppermute(packed, 'sp', pairs))  4.5 us
    ppermute x3, waiting for transfers between devices, swapped(): return lax.ppermute(array, 'sp', [(i, i ^ k) for i in range(count)])  3.56 us
    pallas_call x4, Pallas kernels, placed(): run(*[a if spot is pltpu.SMEM else pltpu.with_memory_space_constraint(a,...  3.51 us
    ppermute x8, starting transfers between devices, paired(): return lax.ppermute(array, 'tp', [(0, 1), (1, 0)])  1.6 us
  transfers between devices with their start and end apart: 20, of which 9 were waited for; matrix products, arithmetic and copies ran while one was open for 0% of the time, Pallas kernels for 5%

profile of v2, /device:TPU:16, one launch (start us, length us, event | category | flops | bytes accessed | tf_op | source)
XLA Modules:
  0.0 43.5 jit_solution(3505051489296810894)
XLA Ops:
  0.0 0.1 collective-permute-start.11
  0.1 2.8 %collective-permute-start.2 = (bf16[16,2048]{1,0:T(8,128)(2,1)}, bf16[16,2048]{1,0:T(8,128)(2,1)S(1)}, u32[]{:S(2)}, u32[]{:S(2)}) collective-permute-start(bf16[16,2048]{1,0:T(8,128)(2,1)} %x0.1), channel_id=1, source_target_pairs={{0,6},{2,4},{4,2},{6,0},{1,7},{3,5},{5,3},{7,1},{8,14},{10,12},{12... | collective-permute-start | bytes 196616 | tf_op jit(solution)/shard_map/ppermute | solution.py:225
  2.9 0.5 %collective-permute-start.1 = (bf16[16,2048]{1,0:T(8,128)(2,1)}, bf16[16,2048]{1,0:T(8,128)(2,1)S(1)}, u32[]{:S(2)}, u32[]{:S(2)}) collective-permute-start(bf16[16,2048]{1,0:T(8,128)(2,1)} %x0.1), channel_id=1, source_target_pairs={{0,4},{2,6},{4,0},{6,2},{1,5},{3,7},{5,1},{7,3},{8,12},{10,14},{12... | collective-permute-start | bytes 196616 | tf_op jit(solution)/shard_map/ppermute | solution.py:225
  3.4 0.3 collective-permute-start
  3.7 0.0 collective-permute-start.3
  3.7 1.9 %collective-permute-done.2.x3 = bf16[16,2048]{1,0:T(8,128)(2,1)S(1)} collective-permute-done((bf16[16,2048]{1,0:T(8,128)(2,1)}, bf16[16,2048]{1,0:T(8,128)(2,1)S(1)}, u32[]{:S(2)}, u32[]{:S(2)}) %collective-permute-start.2) | collective-permute-done | bytes 65568 | tf_op jit(solution)/shard_map/ppermute | solution.py:225
  5.6 1.9 %collective-permute-start.10 = (bf16[2,128,512]{2,1,0:T(8,128)(2,1)}, bf16[2,128,512]{2,1,0:T(8,128)(2,1)S(1)}, u32[]{:S(2)}, u32[]{:S(2)}) collective-permute-start(bf16[2,128,512]{2,1,0:T(8,128)(2,1)} %refs_10_.1), channel_id=1, source_target_pairs={{0,8},{8,0},{16,24},{24,16},{1,9},{9,1},{17,25},{25,17},{2,10},{10... | collective-permute-start | bytes 786440 | tf_op jit(solution)/shard_map/ppermute | solution.py:214
  7.5 0.0 collective-permute-done.1.x2
  7.5 0.0 collective-permute-start.6
  7.5 0.4 collective-permute-done.x1
  7.9 0.1 collective-permute-start.5
  8.0 0.0 collective-permute-done.3.y0
  8.0 0.4 collective-permute-start.4
  8.4 3.6 %collective-permute-done.11.refs_12_ = bf16[2,128,512]{2,1,0:T(8,128)(2,1)S(1)} collective-permute-done((bf16[2,128,512]{2,1,0:T(8,128)(2,1)}, bf16[2,128,512]{2,1,0:T(8,128)(2,1)S(1)}, u32[]{:S(2)}, u32[]{:S(2)}) %collective-permute-start.11) | collective-permute-done | bytes 262176 | tf_op jit(solution)/shard_map/ppermute | solution.py:214
  11.9 4.5 %collective-permute-start.12 = (bf16[2,128,512]{2,1,0:T(8,128)(2,1)S(1)}, bf16[2,128,512]{2,1,0:T(8,128)(2,1)S(1)}, u32[]{:S(2)}, u32[]{:S(2)}) collective-permute-start(bf16[2,128,512]{2,1,0:T(8,128)(2,1)S(1)} %collective-permute-done.11.refs_12_), channel_id=1, source_target_pairs={{0,8},{8,0},{16,24},{24,16},{1,9},{9,1},{17,25},{25,17},{2,10},{10... | collective-permute-start | bytes 786440 | tf_op jit(solution)/shard_map/ppermute | solution.py:214
  16.4 0.0 collective-permute-done.6.y3
  16.4 0.0 collective-permute-done.5.y2
  16.4 0.0 collective-permute-done.4.y1
  16.5 0.0 copy-start.10
  16.5 0.6 %copy-done.9 = f32[2048]{0:T(1024)S(1)} copy-done((f32[2048]{0:T(1024)S(1)}, f32[2048]{0:T(1024)}, u32[]{:S(2)}) %copy-start.9) | copy-done | bytes 8216
  17.1 1.1 %shard_map.137 = (bf16[128,2048]{1,0:T(8,128)(2,1)S(1)}, bf16[392,128]{1,0:T(8,128)(2,1)S(1)}, bf16[128,128]{1,0:T(8,128)(2,1)S(1)}, bf16[128,128]{1,0:T(8,128)(2,1)S(1)}) custom-call(bf16[16,2048]{1,0:T(8,128)(2,1)S(1)} %copy-done.7, bf16[16,2048]{1,0:T(8,128)(2,1)S(1)} %collective-permute-done.x1, bf16[16,2048]{1,0:T(8,128)(2,1)S(1)} %collective-permute-done.1.x2, ...), custom_call_target="tpu_custom_call" | custom-call | flops 268435456 | bytes 1048576 | tf_op jit(solution)/shard_map/pallas_call | solution.py:193
  18.3 0.7 %collective-permute-start.9 = (bf16[392,128]{1,0:T(8,128)(2,1)S(1)}, bf16[392,128]{1,0:T(8,128)(2,1)S(1)}, u32[]{:S(2)}, u32[]{:S(2)}) collective-permute-start(bf16[392,128]{1,0:T(8,128)(2,1)S(1)} %get-tuple-element.25.packed), channel_id=1, source_target_pairs={{0,24},{1,25},{2,26},{3,27},{4,28},{5,29},{6,30},{7,31}} | collective-permute-start | bytes 301064 | tf_op jit(solution)/shard_map/ppermute | solution.py:247
  19.0 1.3 %collective-permute-start.8 = (bf16[392,128]{1,0:T(8,128)(2,1)S(1)}, bf16[392,128]{1,0:T(8,128)(2,1)S(1)}, u32[]{:S(2)}, u32[]{:S(2)}) collective-permute-start(bf16[392,128]{1,0:T(8,128)(2,1)S(1)} %get-tuple-element.25.packed), channel_id=1, source_target_pairs={{0,16},{8,24},{1,17},{9,25},{2,18},{10,26},{3,19},{11,27},{4,20},{... | collective-permute-start | bytes 301064 | tf_op jit(solution)/shard_map/ppermute | solution.py:247
  20.3 2.5 %collective-permute-start.7 = (bf16[392,128]{1,0:T(8,128)(2,1)S(1)}, bf16[392,128]{1,0:T(8,128)(2,1)S(1)}, u32[]{:S(2)}, u32[]{:S(2)}) collective-permute-start(bf16[392,128]{1,0:T(8,128)(2,1)S(1)} %get-tuple-element.25.packed), channel_id=1, source_target_pairs={{0,8},{8,16},{16,24},{1,9},{9,17},{17,25},{2,10},{10,18},{18,26},{... | collective-permute-start | bytes 301064 | tf_op jit(solution)/shard_map/ppermute | solution.py:247
  23.5 0.0 copy-start.11
  23.5 0.0 copy-start.12
  23.5 0.6 %copy-done.11 = f32[128]{0:T(128)S(1)} copy-done((f32[128]{0:T(128)S(1)}, f32[128]{0:T(128)}, u32[]{:S(2)}) %copy-start.11) | copy-done | bytes 536
  24.1 0.0 copy-done.12
  24.1 1.1 %shard_map.138 = (bf16[128,128]{1,0:T(8,128)(2,1)S(1)}, f32[128,128]{1,0:T(8,128)S(1)}, f32[128,128]{1,0:T(8,128)S(1)}, f32[2,128,128]{2,1,0:T(8,128)S(1)}, f32[...) custom-call(f32[1]{0:T(128)S(6)} %copy.15.lam, ...), custom_call_target="tpu_custom_call" | custom-call | flops 134217728 | bytes 1048576 | tf_op jit(solution)/shard_map/pallas_call | solution.py:193
  25.2 3.1 %collective-permute-done.8.refs_8_ = bf16[392,128]{1,0:T(8,128)(2,1)S(1)} collective-permute-done((bf16[392,128]{1,0:T(8,128)(2,1)S(1)}, bf16[392,128]{1,0:T(8,128)(2,1)S(1)}, u32[]{:S(2)}, u32[]{:S(2)}) %collective-permute-start.8) | collective-permute-done | bytes 100384 | tf_op jit(solution)/shard_map/ppermute | solution.py:247
  28.3 3.5 %collective-permute-done.7.refs_7_ = bf16[392,128]{1,0:T(8,128)(2,1)S(1)} collective-permute-done((bf16[392,128]{1,0:T(8,128)(2,1)S(1)}, bf16[392,128]{1,0:T(8,128)(2,1)S(1)}, u32[]{:S(2)}, u32[]{:S(2)}) %collective-permute-start.7) | collective-permute-done | bytes 100384 | tf_op jit(solution)/shard_map/ppermute | solution.py:247
  31.8 0.0 collective-permute-done.12.refs_13_
  31.8 1.3 %shard_map.139 = (f32[16,2048]{1,0:T(8,128)S(1)}, f32[16,2048]{1,0:T(8,128)S(1)}, f32[16,2048]{1,0:T(8,128)S(1)}, f32[16,2048]{1,0:T(8,128)S(1)}, bf16[16,2048]{...) custom-call(bf16[128,128]{1,0:T(8,128)(2,1)S(1)} %get-tuple-element., ...), custom_call_target="tpu_custom_call" | custom-call | flops 134217728 | bytes 1048576 | tf_op jit(solution)/shard_map/pallas_call | solution.py:193
  33.1 0.1 collective-permute-start.14
  33.2 0.5 %collective-permute-start.13 = (bf16[16,2048]{1,0:T(8,128)(2,1)S(1)}, bf16[16,2048]{1,0:T(8,128)(2,1)S(1)}, u32[]{:S(2)}, u32[]{:S(2)}) collective-permute-start(bf16[16,2048]{1,0:T(8,128)(2,1)S(1)} %get-tuple-element.36), channel_id=1, source_target_pairs={{0,1},{1,0},{2,3},{3,2},{4,5},{5,4},{6,7},{7,6},{8,9},{9,8},{10,11... | collective-permute-start | bytes 196616 | tf_op jit(solution)/shard_map/ppermute | solution.py:228
  33.7 0.1 collective-permute-start.16
  33.7 0.4 collective-permute-start.18
  34.2 0.2 collective-permute-done.14
  34.4 1.6 %collective-permute-start.15 = (bf16[16,2048]{1,0:T(8,128)(2,1)S(1)}, bf16[16,2048]{1,0:T(8,128)(2,1)S(1)}, u32[]{:S(2)}, u32[]{:S(2)}) collective-permute-start(bf16[16,2048]{1,0:T(8,128)(2,1)S(1)} %add_convert_fusion.3), channel_id=1, source_target_pairs={{0,2},{2,0},{4,6},{6,4},{1,3},{3,1},{5,7},{7,5},{8,10},{10,8},{12,... | collective-permute-start | bytes 196616 | tf_op jit(solution)/shard_map/ppermute | solution.py:225
  36.0 0.0 collective-permute-done.16
  36.0 1.6 %collective-permute-start.17 = (bf16[16,2048]{1,0:T(8,128)(2,1)S(1)}, bf16[16,2048]{1,0:T(8,128)(2,1)S(1)}, u32[]{:S(2)}, u32[]{:S(2)}) collective-permute-start(bf16[16,2048]{1,0:T(8,128)(2,1)S(1)} %add_convert_fusion.2), channel_id=1, source_target_pairs={{0,4},{2,6},{4,0},{6,2},{1,5},{3,7},{5,1},{7,3},{8,12},{10,14},{12... | collective-permute-start | bytes 196616 | tf_op jit(solution)/shard_map/ppermute | solution.py:225
  37.6 0.0 collective-permute-done.18
  37.6 0.5 %collective-permute-start.19 = (bf16[16,2048]{1,0:T(8,128)(2,1)S(1)}, bf16[16,2048]{1,0:T(8,128)(2,1)S(1)}, u32[]{:S(2)}, u32[]{:S(2)}) collective-permute-start(bf16[16,2048]{1,0:T(8,128)(2,1)S(1)} %add_convert_fusion.1), channel_id=1, source_target_pairs={{0,6},{2,4},{4,2},{6,0},{1,7},{3,5},{5,3},{7,1},{8,14},{10,12},{12... | collective-permute-start | bytes 196616 | tf_op jit(solution)/shard_map/ppermute | solution.py:225
  38.2 0.0 collective-permute-done.13
  38.2 0.6 %collective-permute-done.15 = bf16[16,2048]{1,0:T(8,128)(2,1)S(1)} collective-permute-done((bf16[16,2048]{1,0:T(8,128)(2,1)S(1)}, bf16[16,2048]{1,0:T(8,128)(2,1)S(1)}, u32[]{:S(2)}, u32[]{:S(2)}) %collective-permute-start.15) | collective-permute-done | bytes 65568 | tf_op jit(solution)/shard_map/ppermute | solution.py:225
  38.8 1.6 %collective-permute-done.17 = bf16[16,2048]{1,0:T(8,128)(2,1)S(1)} collective-permute-done((bf16[16,2048]{1,0:T(8,128)(2,1)S(1)}, bf16[16,2048]{1,0:T(8,128)(2,1)S(1)}, u32[]{:S(2)}, u32[]{:S(2)}) %collective-permute-start.17) | collective-permute-done | bytes 65568 | tf_op jit(solution)/shard_map/ppermute | solution.py:225
  40.3 2.5 %collective-permute-done.19 = bf16[16,2048]{1,0:T(8,128)(2,1)S(1)} collective-permute-done((bf16[16,2048]{1,0:T(8,128)(2,1)S(1)}, bf16[16,2048]{1,0:T(8,128)(2,1)S(1)}, u32[]{:S(2)}, u32[]{:S(2)}) %collective-permute-start.19) | collective-permute-done | bytes 65568 | tf_op jit(solution)/shard_map/ppermute | solution.py:225
  42.9 0.7 %add_convert_fusion = bf16[16,2048]{1,0:T(8,128)(2,1)} fusion(bf16[16,2048]{1,0:T(8,128)(2,1)S(1)} %collective-permute-done.19, bf16[16,2048]{1,0:T(8,128)(2,1)S(1)} %collective-permute-done.17, bf16[16,2048]{1,0:T(8,128)(2,1)S(1)} %collective-permute-done.15, f32[16,2048]{1,0:T(8,128)S(1)} %get-tuple-element.35, bf16[16,2048]{1,0:T(8,128)(2,1)S(1)} %collective-permute-done.13), kind=kLoop, calls=%fused_computation | loop fusion | flops 294912 | bytes 458752 | tf_op jit(solution)/shard_map/convert_element_type | solution.py:269
  (26 shorter events, 0.1 us)
Async XLA Ops:
  0.0 16.5 %copy-start.7 = (bf16[16,2048]{1,0:T(8,128)(2,1)S(1)}, bf16[16,2048]{1,0:T(8,128)(2,1)}, u32[]{:S(2)}) copy-start(bf16[16,2048]{1,0:T(8,128)(2,1)} %x0.1) | copy-start | bytes 196612
  0.0 16.5 %copy-start.3 = (bf16[2048,128]{1,0:T(8,128)(2,1)S(1)}, bf16[2048,128]{1,0:T(8,128)(2,1)}, u32[]{:S(2)}) copy-start(bf16[2048,128]{1,0:T(8,128)(2,1)} %dv.1) | copy-start | bytes 1572868
  0.0 16.5 %copy-start.2 = (bf16[2,2048,64]{1,2,0:T(8,128)(2,1)S(1)}, bf16[2,2048,64]{1,2,0:T(8,128)(2,1)}, u32[]{:S(2)}) copy-start(bf16[2,2048,64]{1,2,0:T(8,128)(2,1)} %param.23) | copy-start | bytes 1572868
  0.0 16.5 %copy-start.5 = (bf16[2048,128]{1,0:T(8,128)(2,1)S(1)}, bf16[2048,128]{1,0:T(8,128)(2,1)}, u32[]{:S(2)}) copy-start(bf16[2048,128]{1,0:T(8,128)(2,1)} %wv.1) | copy-start | bytes 1572868
  0.0 16.5 %copy-start.4 = (bf16[2048,128]{1,0:T(8,128)(2,1)S(1)}, bf16[2048,128]{1,0:T(8,128)(2,1)}, u32[]{:S(2)}) copy-start(bf16[2048,128]{1,0:T(8,128)(2,1)} %wk.1) | copy-start | bytes 1572868
  0.0 11.9 %collective-permute-start.11 = (bf16[2,128,512]{2,1,0:T(8,128)(2,1)}, bf16[2,128,512]{2,1,0:T(8,128)(2,1)S(1)}, u32[]{:S(2)}, u32[]{:S(2)}) collective-permute-start(bf16[2,128,512]{2,1,0:T(8,128)(2,1)} %refs_10_.1), channel_id=1, source_target_pairs={{0,16},{8,24},{16,0},{24,8},{1,17},{9,25},{17,1},{25,9},{2,18},{10... | collective-permute-start | bytes 786440 | tf_op jit(solution)/shard_map/ppermute | solution.py:214
  0.1 5.5 %collective-permute-start.2 = (bf16[16,2048]{1,0:T(8,128)(2,1)}, bf16[16,2048]{1,0:T(8,128)(2,1)S(1)}, u32[]{:S(2)}, u32[]{:S(2)}) collective-permute-start(bf16[16,2048]{1,0:T(8,128)(2,1)} %x0.1), channel_id=1, source_target_pairs={{0,6},{2,4},{4,2},{6,0},{1,7},{3,5},{5,3},{7,1},{8,14},{10,12},{12... | collective-permute-start | bytes 196616 | tf_op jit(solution)/shard_map/ppermute | solution.py:225
  2.9 4.6 %collective-permute-start.1 = (bf16[16,2048]{1,0:T(8,128)(2,1)}, bf16[16,2048]{1,0:T(8,128)(2,1)S(1)}, u32[]{:S(2)}, u32[]{:S(2)}) collective-permute-start(bf16[16,2048]{1,0:T(8,128)(2,1)} %x0.1), channel_id=1, source_target_pairs={{0,4},{2,6},{4,0},{6,2},{1,5},{3,7},{5,1},{7,3},{8,12},{10,14},{12... | collective-permute-start | bytes 196616 | tf_op jit(solution)/shard_map/ppermute | solution.py:225
  3.4 4.5 %collective-permute-start = (bf16[16,2048]{1,0:T(8,128)(2,1)}, bf16[16,2048]{1,0:T(8,128)(2,1)S(1)}, u32[]{:S(2)}, u32[]{:S(2)}) collective-permute-start(bf16[16,2048]{1,0:T(8,128)(2,1)} %x0.1), channel_id=1, source_target_pairs={{0,2},{2,0},{4,6},{6,4},{1,3},{3,1},{5,7},{7,5},{8,10},{10,8},{12,... | collective-permute-start | bytes 196616 | tf_op jit(solution)/shard_map/ppermute | solution.py:225
  3.7 4.3 %collective-permute-start.3 = (bf16[16,2048]{1,0:T(8,128)(2,1)}, bf16[16,2048]{1,0:T(8,128)(2,1)S(1)}, u32[]{:S(2)}, u32[]{:S(2)}) collective-permute-start(bf16[16,2048]{1,0:T(8,128)(2,1)} %x0.1), channel_id=1, source_target_pairs={{0,1},{1,0},{2,3},{3,2},{4,5},{5,4},{6,7},{7,6},{8,9},{9,8},{10,11... | collective-permute-start | bytes 196616 | tf_op jit(solution)/shard_map/ppermute | solution.py:228
  5.6 26.2 %collective-permute-start.10 = (bf16[2,128,512]{2,1,0:T(8,128)(2,1)}, bf16[2,128,512]{2,1,0:T(8,128)(2,1)S(1)}, u32[]{:S(2)}, u32[]{:S(2)}) collective-permute-start(bf16[2,128,512]{2,1,0:T(8,128)(2,1)} %refs_10_.1), channel_id=1, source_target_pairs={{0,8},{8,0},{16,24},{24,16},{1,9},{9,1},{17,25},{25,17},{2,10},{10... | collective-permute-start | bytes 786440 | tf_op jit(solution)/shard_map/ppermute | solution.py:214
  7.5 8.9 %collective-permute-start.6 = (bf16[16,2048]{1,0:T(8,128)(2,1)S(1)}, bf16[16,2048]{1,0:T(8,128)(2,1)S(1)}, u32[]{:S(2)}, u32[]{:S(2)}) collective-permute-start(bf16[16,2048]{1,0:T(8,128)(2,1)S(1)} %collective-permute-done.2.x3), channel_id=1, source_target_pairs={{0,1},{1,0},{2,3},{3,2},{4,5},{5,4},{6,7},{7,6},{8,9},{9,8},{10,11... | collective-permute-start | bytes 196616 | tf_op jit(solution)/shard_map/ppermute | solution.py:228
  7.9 8.6 %collective-permute-start.5 = (bf16[16,2048]{1,0:T(8,128)(2,1)S(1)}, bf16[16,2048]{1,0:T(8,128)(2,1)S(1)}, u32[]{:S(2)}, u32[]{:S(2)}) collective-permute-start(bf16[16,2048]{1,0:T(8,128)(2,1)S(1)} %collective-permute-done.1.x2), channel_id=1, source_target_pairs={{0,1},{1,0},{2,3},{3,2},{4,5},{5,4},{6,7},{7,6},{8,9},{9,8},{10,11... | collective-permute-start | bytes 196616 | tf_op jit(solution)/shard_map/ppermute | solution.py:228
  8.0 8.4 %collective-permute-start.4 = (bf16[16,2048]{1,0:T(8,128)(2,1)S(1)}, bf16[16,2048]{1,0:T(8,128)(2,1)S(1)}, u32[]{:S(2)}, u32[]{:S(2)}) collective-permute-start(bf16[16,2048]{1,0:T(8,128)(2,1)S(1)} %collective-permute-done.x1), channel_id=1, source_target_pairs={{0,1},{1,0},{2,3},{3,2},{4,5},{5,4},{6,7},{7,6},{8,9},{9,8},{10,11... | collective-permute-start | bytes 196616 | tf_op jit(solution)/shard_map/ppermute | solution.py:228
  11.9 19.8 %collective-permute-start.12 = (bf16[2,128,512]{2,1,0:T(8,128)(2,1)S(1)}, bf16[2,128,512]{2,1,0:T(8,128)(2,1)S(1)}, u32[]{:S(2)}, u32[]{:S(2)}) collective-permute-start(bf16[2,128,512]{2,1,0:T(8,128)(2,1)S(1)} %collective-permute-done.11.refs_12_), channel_id=1, source_target_pairs={{0,8},{8,0},{16,24},{24,16},{1,9},{9,1},{17,25},{25,17},{2,10},{10... | collective-permute-start | bytes 786440 | tf_op jit(solution)/shard_map/ppermute | solution.py:214
  16.4 0.7 %copy-start.9 = (f32[2048]{0:T(1024)S(1)}, f32[2048]{0:T(1024)}, u32[]{:S(2)}) copy-start(f32[2048]{0:T(1024)} %param.15) | copy-start | bytes 24580
  16.5 0.7 %copy-start.10 = (f32[1,128]{1,0:T(1,128)S(1)}, f32[1,128]{1,0:T(1,128)}, u32[]{:S(2)}) copy-start(f32[1,128]{1,0:T(1,128)} %decay.3) | copy-start | bytes 1540
  17.1 6.3 %copy-start = (bf16[2048,128]{1,0:T(8,128)(2,1)S(1)}, bf16[2048,128]{1,0:T(8,128)(2,1)}, u32[]{:S(2)}) copy-start(bf16[2048,128]{1,0:T(8,128)(2,1)} %wq.1) | copy-start | bytes 1572868
  17.1 6.4 %copy-start.1 = (bf16[2,2048,64]{1,2,0:T(8,128)(2,1)S(1)}, bf16[2,2048,64]{1,2,0:T(8,128)(2,1)}, u32[]{:S(2)}) copy-start(bf16[2,2048,64]{1,2,0:T(8,128)(2,1)} %param.22) | copy-start | bytes 1572868
  17.1 6.4 %copy-start.8 = (bf16[1,128,128]{2,1,0:T(8,128)(2,1)S(1)}, bf16[1,128,128]{2,1,0:T(8,128)(2,1)}, u32[]{:S(2)}) copy-start(bf16[1,128,128]{2,1,0:T(8,128)(2,1)} %start.1) | copy-start | bytes 98308
  18.3 6.9 %collective-permute-start.9 = (bf16[392,128]{1,0:T(8,128)(2,1)S(1)}, bf16[392,128]{1,0:T(8,128)(2,1)S(1)}, u32[]{:S(2)}, u32[]{:S(2)}) collective-permute-start(bf16[392,128]{1,0:T(8,128)(2,1)S(1)} %get-tuple-element.25.packed), channel_id=1, source_target_pairs={{0,24},{1,25},{2,26},{3,27},{4,28},{5,29},{6,30},{7,31}} | collective-permute-start | bytes 301064 | tf_op jit(solution)/shard_map/ppermute | solution.py:247
  19.0 9.3 %collective-permute-start.8 = (bf16[392,128]{1,0:T(8,128)(2,1)S(1)}, bf16[392,128]{1,0:T(8,128)(2,1)S(1)}, u32[]{:S(2)}, u32[]{:S(2)}) collective-permute-start(bf16[392,128]{1,0:T(8,128)(2,1)S(1)} %get-tuple-element.25.packed), channel_id=1, source_target_pairs={{0,16},{8,24},{1,17},{9,25},{2,18},{10,26},{3,19},{11,27},{4,20},{... | collective-permute-start | bytes 301064 | tf_op jit(solution)/shard_map/ppermute | solution.py:247
  20.3 11.5 %collective-permute-start.7 = (bf16[392,128]{1,0:T(8,128)(2,1)S(1)}, bf16[392,128]{1,0:T(8,128)(2,1)S(1)}, u32[]{:S(2)}, u32[]{:S(2)}) collective-permute-start(bf16[392,128]{1,0:T(8,128)(2,1)S(1)} %get-tuple-element.25.packed), channel_id=1, source_target_pairs={{0,8},{8,16},{16,24},{1,9},{9,17},{17,25},{2,10},{10,18},{18,26},{... | collective-permute-start | bytes 301064 | tf_op jit(solution)/shard_map/ppermute | solution.py:247
  23.5 0.7 %copy-start.11 = (f32[128]{0:T(128)S(1)}, f32[128]{0:T(128)}, u32[]{:S(2)}) copy-start(f32[128]{0:T(128)} %param.21) | copy-start | bytes 1540
  23.5 0.7 %copy-start.12 = (f32[128]{0:T(128)S(1)}, f32[128]{0:T(128)}, u32[]{:S(2)}) copy-start(f32[128]{0:T(128)} %param.26) | copy-start | bytes 1540
  24.1 7.6 %copy-start.6 = (bf16[2,128,512]{2,1,0:T(8,128)(2,1)S(1)}, bf16[2,128,512]{2,1,0:T(8,128)(2,1)}, u32[]{:S(2)}) copy-start(bf16[2,128,512]{2,1,0:T(8,128)(2,1)} %refs_10_.1) | copy-start | bytes 786436
  33.1 1.3 %collective-permute-start.14 = (bf16[16,2048]{1,0:T(8,128)(2,1)S(1)}, bf16[16,2048]{1,0:T(8,128)(2,1)S(1)}, u32[]{:S(2)}, u32[]{:S(2)}) collective-permute-start(bf16[16,2048]{1,0:T(8,128)(2,1)S(1)} %get-tuple-element.38), channel_id=1, source_target_pairs={{0,1},{1,0},{2,3},{3,2},{4,5},{5,4},{6,7},{7,6},{8,9},{9,8},{10,11... | collective-permute-start | bytes 196616 | tf_op jit(solution)/shard_map/ppermute | solution.py:228
  33.2 5.0 %collective-permute-start.13 = (bf16[16,2048]{1,0:T(8,128)(2,1)S(1)}, bf16[16,2048]{1,0:T(8,128)(2,1)S(1)}, u32[]{:S(2)}, u32[]{:S(2)}) collective-permute-start(bf16[16,2048]{1,0:T(8,128)(2,1)S(1)} %get-tuple-element.36), channel_id=1, source_target_pairs={{0,1},{1,0},{2,3},{3,2},{4,5},{5,4},{6,7},{7,6},{8,9},{9,8},{10,11... | collective-permute-start | bytes 196616 | tf_op jit(solution)/shard_map/ppermute | solution.py:228
  33.7 2.3 %collective-permute-start.16 = (bf16[16,2048]{1,0:T(8,128)(2,1)S(1)}, bf16[16,2048]{1,0:T(8,128)(2,1)S(1)}, u32[]{:S(2)}, u32[]{:S(2)}) collective-permute-start(bf16[16,2048]{1,0:T(8,128)(2,1)S(1)} %get-tuple-element.40), channel_id=1, source_target_pairs={{0,1},{1,0},{2,3},{3,2},{4,5},{5,4},{6,7},{7,6},{8,9},{9,8},{10,11... | collective-permute-start | bytes 196616 | tf_op jit(solution)/shard_map/ppermute | solution.py:228
  33.7 3.9 %collective-permute-start.18 = (bf16[16,2048]{1,0:T(8,128)(2,1)S(1)}, bf16[16,2048]{1,0:T(8,128)(2,1)S(1)}, u32[]{:S(2)}, u32[]{:S(2)}) collective-permute-start(bf16[16,2048]{1,0:T(8,128)(2,1)S(1)} %get-tuple-element.42), channel_id=1, source_target_pairs={{0,1},{1,0},{2,3},{3,2},{4,5},{5,4},{6,7},{7,6},{8,9},{9,8},{10,11... | collective-permute-start | bytes 196616 | tf_op jit(solution)/shard_map/ppermute | solution.py:228
  34.4 4.3 %collective-permute-start.15 = (bf16[16,2048]{1,0:T(8,128)(2,1)S(1)}, bf16[16,2048]{1,0:T(8,128)(2,1)S(1)}, u32[]{:S(2)}, u32[]{:S(2)}) collective-permute-start(bf16[16,2048]{1,0:T(8,128)(2,1)S(1)} %add_convert_fusion.3), channel_id=1, source_target_pairs={{0,2},{2,0},{4,6},{6,4},{1,3},{3,1},{5,7},{7,5},{8,10},{10,8},{12,... | collective-permute-start | bytes 196616 | tf_op jit(solution)/shard_map/ppermute | solution.py:225
  36.0 4.3 %collective-permute-start.17 = (bf16[16,2048]{1,0:T(8,128)(2,1)S(1)}, bf16[16,2048]{1,0:T(8,128)(2,1)S(1)}, u32[]{:S(2)}, u32[]{:S(2)}) collective-permute-start(bf16[16,2048]{1,0:T(8,128)(2,1)S(1)} %add_convert_fusion.2), channel_id=1, source_target_pairs={{0,4},{2,6},{4,0},{6,2},{1,5},{3,7},{5,1},{7,3},{8,12},{10,14},{12... | collective-permute-start | bytes 196616 | tf_op jit(solution)/shard_map/ppermute | solution.py:225
  37.6 5.2 %collective-permute-start.19 = (bf16[16,2048]{1,0:T(8,128)(2,1)S(1)}, bf16[16,2048]{1,0:T(8,128)(2,1)S(1)}, u32[]{:S(2)}, u32[]{:S(2)}) collective-permute-start(bf16[16,2048]{1,0:T(8,128)(2,1)S(1)} %add_convert_fusion.1), channel_id=1, source_target_pairs={{0,6},{2,4},{4,2},{6,0},{1,7},{3,5},{5,3},{7,1},{8,14},{10,12},{12... | collective-permute-start | bytes 196616 | tf_op jit(solution)/shard_map/ppermute | solution.py:225

commit v3 on v1

--- a/solution.py
+++ b/solution.py
@@ -14,7 +14,7 @@
 F32 = jnp.float32
 BF16 = jnp.bfloat16
 
-GATHER_FLOPS = 10**10
+GATHER_FLOPS = 3 * 10**10
 
 
 def dot(a, b, dims, **kw):
@@ -37,8 +37,12 @@
     return [(i, i + d) for i in range(count - d)], lambda at: at - d
 
 
+ROUNDS = (lambda at: lax.rem(2 * at + 1, 5), lambda at: lax.rem(3 * at + 2, 5))
+ROUND_PAIRS = (((1, 0), (3, 1), (0, 2), (2, 3)), ((2, 0), (0, 1), (3, 2), (1, 3)))
+
+
 def few(count):
-    return count in (2, 4)
+    return count == 4
 
 
 def at_or_before(n):
@@ -64,15 +68,15 @@
 
 
 def prepare_kernel(
-    tokens_h, decay_h, in_gain_h, ret_gain_h, diff_gain_h, init_h,
-    tokens, key_scale, query_scale, fade, factor, in_gain, small, init, decay, ret_gain, diff_gain, start, sems,
+    decay_h, in_gain_h, ret_gain_h, diff_gain_h, init_h,
+    key_scale, query_scale, fade, factor, gain, small, init, decay, in_gain, ret_gain, diff_gain, start, sems,
 ):
-    head = fade.shape[0]
+    head = factor.shape[1]
     copies = fetch(
-        [(decay_h, decay), (tokens_h, tokens), (in_gain_h, in_gain), (ret_gain_h, ret_gain), (diff_gain_h, diff_gain), (init_h, start)],
-        sems,
+        [(decay_h, decay), (in_gain_h, in_gain), (ret_gain_h, ret_gain), (diff_gain_h, diff_gain), (init_h, start)], sems
     )
-    copies[0].wait()
+    for copy in copies:
+        copy.wait()
     cumul, along = cumulated(decay[...])
     rows = cumul.shape[0]
     last = cumul[rows - 1 :, :]
@@ -80,19 +84,26 @@
     query_scale[...] = jnp.broadcast_to(jnp.exp(cumul), (rows, head))
     fade[...] = jnp.exp(jnp.where(at_or_before(rows), cumul - along, -HUGE)) * head ** (-0.5)
     factor[...] = jnp.broadcast_to(jnp.exp(last), (8, head))
-    for copy in copies[1:]:
-        copy.wait()
+    gain[...] = in_gain[...]
     small[0:8, :] = jnp.broadcast_to(ret_gain[...], (8, head))
     small[8:16, :] = jnp.broadcast_to(diff_gain[...], (8, head))
     init[...] = start[0].astype(F32)
 
 
-def project_kernel(x, gain, key_scale, factor, dk, dv, wk, wv, normed, packed, ret_k, ret_v):
+def project_kernel(
+    x0, x1, x2, x3, y0, y1, y2, y3, gain, key_scale, factor, dk, dv, wk, wv, normed, packed, ret_k, ret_v
+):
     rows, head = ret_k.shape
-    wide = x[...].astype(F32)
-    scale = lax.rsqrt(jnp.mean(wide * wide, axis=-1, keepdims=True) + EPS)
-    rounded = (wide * scale * gain[...]).astype(BF16)
-    normed[...] = rounded
+    chip = lax.axis_index("fs")
+    core = lax.axis_index("tp")
+    for j, side in enumerate(((x0, x1, x2, x3), (y0, y1, y2, y3))):
+        for k, piece in enumerate(side):
+            own = piece.shape[0]
+            wide = piece[...].astype(F32)
+            scale = lax.rsqrt(jnp.mean(wide * wide, axis=-1, keepdims=True) + EPS)
+            at = pl.multiple_of(((chip ^ k) * 2 + (core ^ j)) * own, own)
+            normed[pl.ds(at, own), :] = (wide * scale * gain[...]).astype(BF16)
+    rounded = normed[...]
     packed[0:rows, :] = nt(rounded, dk[...].reshape(-1, dk.shape[2])).astype(BF16)
     packed[rows : 2 * rows, :] = nn(rounded, dv[...]).astype(BF16)
     k = nn(rounded, wk[...]).astype(BF16)
@@ -131,12 +142,13 @@
     count = len(sources) + 1
     queries, scaled, inner, sums, stats, second, small, init = refs[:8]
     blocks = refs[8 : 7 + count]
-    weights = refs[7 + count : 7 + 2 * count]
-    keep, send, mixed = refs[7 + 2 * count :]
+    weights = refs[7 + count : -4]
+    keep, send, order, mixed = refs[-4:]
     rows, head = inner.shape
     half = head // 2
     place = lax.axis_index("sp")
     core = lax.axis_index("tp")
+    chip = lax.axis_index("fs")
     source = [f(place) for f in sources]
     before = [jnp.logical_and(at >= 0, at < place) for at in source]
     factors = [b[2 * rows + head : 2 * rows + head + 8, :].astype(F32)[0:1, :] for b in blocks]
@@ -174,13 +186,47 @@
 
     mixed[:, :, :, :head] = ret_mix.reshape(mixed.shape[:3] + (head,))
     mixed[:, :, :, head:] = diff_mix.reshape(mixed.shape[:3] + (head,))
-    ordered = jnp.concatenate([mixed[:, core].reshape(-1, 2 * head), mixed[:, 1 - core].reshape(-1, 2 * head)], axis=0)
+    ordered = jnp.concatenate([mixed[chip ^ k, core ^ j] for j in range(2) for k in range(mixed.shape[0])], axis=0)
+    order[...] = ordered
+    cols = weights[0].shape[2]
     for k, w in enumerate(weights):
-        cols = w.shape[2]
-        at = pl.ds(pl.multiple_of((place ^ k) * cols, cols), cols)
         result = nn(ordered, w[...].reshape(2 * head, cols))
-        keep[:, at] = result[: rows // 2]
-        send[:, at] = result[rows // 2 :].astype(BF16)
+        keep[:, k * cols : (k + 1) * cols] = result[: rows // 2]
+        send[:, k * cols : (k + 1) * cols] = result[rows // 2 :].astype(BF16)
+
+
+def pick_kernel(own, second, picked):
+    picked[...] = jnp.where(lax.axis_index("sp") == 2, own[...], second[...])
+
+
+def last_kernel(outer, inner, order, keep, send):
+    kept = keep.shape[0]
+    place = lax.axis_index("sp")
+    weight = jnp.where(jnp.logical_or(place == 1, place == 2), inner[...], outer[...])
+    result = nn(order[...], weight.reshape(-1, weight.shape[2]))
+    keep[...] = result[:kept]
+    send[...] = result[kept:].astype(BF16)
+
+
+def merge_kernel(keep, other, last_keep, last_other, mine, *sends):
+    own, _ = mine.shape
+    cut = keep.shape[1]
+    for k, target in enumerate((mine, *sends)):
+        span = slice(k * own, (k + 1) * own)
+        target[:, :cut] = (keep[span, :] + other[span, :].astype(F32)).astype(target.dtype)
+        target[:, cut:] = (last_keep[span, :] + last_other[span, :].astype(F32)).astype(target.dtype)
+
+
+def total_kernel(mine, *refs):
+    *shares, out = refs
+    total = mine[...]
+    for share in shares:
+        total = total + share[...].astype(F32)
+    place = lax.axis_index("sp")
+    cols = total.shape[1] // lax.axis_size("sp")
+    for k, to in enumerate((place, ROUNDS[0](place), ROUNDS[1](place), place ^ 3)):
+        at = pl.multiple_of(to * cols, cols)
+        out[:, pl.ds(at, cols)] = total[:, k * cols : (k + 1) * cols].astype(BF16)
 
 
 def call(kernel, outs, flops, here, away=0, scratch=(), scalars=0):
@@ -216,47 +262,68 @@
     own_rows = tokens.shape[0]
     rows = own_rows * group
 
-    def swapped(array, k):
-        return lax.ppermute(array, "sp", [(i, i ^ k) for i in range(count)])
-
-    weights = [out_weight] * count
-    weights[1] = swapped(out_weight, 1)
-    if count == 4:
-        weights[2] = swapped(out_weight, 2)
-        weights[3] = swapped(weights[2], 1)
+    weights = [out_weight]
+    for pairs in ROUND_PAIRS:
+        weights.append(lax.ppermute(out_weight, "sp", list(pairs)))
+    outer = lax.ppermute(weights[1], "sp", [(1, 0), (2, 3)])
+    (picked,) = call(pick_kernel, [shape(out_weight.shape, BF16)], 1 << 17, 2)(out_weight, weights[2])
+    inner = lax.ppermute(picked, "sp", [(2, 1), (3, 2)])
     square = shape((rows, head), BF16)
+    chips = lax.axis_size("fs")
+    line = pltpu.VMEM((1, head), F32)
+
+    def across(array, k):
+        return lax.ppermute(array, "fs", [(i, i ^ k) for i in range(chips)])
+
+    def paired(array):
+        return lax.ppermute(array, "tp", [(0, 1), (1, 0)])
+
     wide = shape((rows, head), F32)
-    line = pltpu.VMEM((1, head), F32)
-    staged, key_scale, query_scale, fade, factor, gain, small, init = call(
+    key_scale, query_scale, fade, factor, gain, small, init = call(
         prepare_kernel,
-        [shape(tokens.shape, BF16), wide, wide, shape((rows, rows), F32), shape((8, head), F32),
-         shape((1, width), F32), shape((16, head), F32), shape((head, head), F32)],
-        GATHER_FLOPS, 0, 6, [line, line, line, pltpu.VMEM((1, head, head), BF16)],
-    )(tokens, decay_log, in_gain[None, :], ret_gain[None, :], diff_gain[None, :], init_state)
-    gathered = lax.all_gather(staged, ("fs", "tp"), axis=0, tiled=True)
+        [wide, wide, shape((rows, rows), F32), shape((8, head), F32), shape((1, width), F32),
+         shape((16, head), F32), shape((head, head), F32)],
+        GATHER_FLOPS, 0, 5, [line, pltpu.VMEM((1, width), F32), line, line, pltpu.VMEM((1, head, head), BF16)],
+    )(decay_log, in_gain[None, :], ret_gain[None, :], diff_gain[None, :], init_state)
+    near_rows, far_rows = [tokens], []
+    for k in range(1, chips):
+        near_rows.append(across(tokens, k))
+    for k in range(chips):
+        far_rows.append(paired(near_rows[k]))
     normed, packed, ret_k, ret_v = call(
         project_kernel, [shape((rows, width), BF16), shape((2 * rows + head + 8, head), BF16), square, square],
-        2 * rows * width * head * 4, 8,
-    )(gathered, gain, key_scale, factor, jnp.swapaxes(diff_key, 1, 2), diff_value, ret_key, ret_value)
+        2 * rows * width * head * 4, 15,
+    )(*near_rows, *far_rows, gain, key_scale, factor, jnp.swapaxes(diff_key, 1, 2), diff_value, ret_key, ret_value)
     blocks, sources = [], []
     for d in range(1, count):
         pairs, source = route(d, count)
         sources.append(source)
         blocks.append(lax.ppermute(packed, "sp", pairs))
     pair = shape((2, rows, head), F32)
-    mine = call(own_kernel, [square, wide, wide, pair, pair, shape((8, head), F32)], 2 * rows * width * head * 2, 8, scalars=1)(
-        diff_lambda, normed, packed, ret_k, ret_v, query_scale, fade, ret_query, jnp.swapaxes(diff_query, 1, 2)
+    mine = call(
+        own_kernel, [square, wide, wide, pair, pair, shape((8, head), F32)], 2 * rows * width * head * 2, 8, scalars=1,
+    )(diff_lambda, normed, packed, ret_k, ret_v, query_scale, fade, ret_query, jnp.swapaxes(diff_query, 1, 2))
+    cols = out_weight.shape[2]
+    half, most = rows // 2, (count - 1) * cols
+    keep, send, order = call(
+        functools.partial(finish_kernel, sources),
+        [shape((half, most), F32), shape((half, most), BF16), shape((rows, 2 * head), BF16)],
+        2 * rows * width * head * 2, 6 + 2 * count, scratch=[pltpu.VMEM((chips, 2, own_rows, 2 * head), BF16)],
+    )(*mine, small, init, *blocks, *weights)
+    other = paired(send)
+    last_keep, last_send = call(
+        last_kernel, [shape((half, cols), F32), shape((half, cols), BF16)], 2 * rows * cols * head * 2, 3
+    )(outer, inner, order)
+    last_other = paired(last_send)
+    part = (own_rows, width)
+    kept, *shares = call(merge_kernel, [shape(part, F32)] + [shape(part, BF16)] * (chips - 1), 1 << 18, 4)(
+        keep, other, last_keep, last_other
     )
-    cores = lax.axis_size("tp")
-    keep, send = call(
-        functools.partial(finish_kernel, sources), [shape((rows // 2, width), F32), shape((rows // 2, width), BF16)],
-        2 * rows * width * head * 2, 7 + 2 * count,
-        scratch=[pltpu.VMEM((group // cores, cores, own_rows, 2 * head), BF16)],
-    )(*mine, small, init, *blocks, *weights)
-    other = lax.ppermute(send, "tp", [(0, 1), (1, 0)])
-    both = (keep + other.astype(F32)).astype(BF16)
-    shares = lax.all_to_all(both, "fs", 0, 0, tiled=True)
-    return shares.reshape(group // cores, own_rows, width).astype(F32).sum(axis=0).astype(BF16)
+    arrived = []
+    for k in range(1, chips):
+        arrived.append(across(shares[k - 1], k))
+    (out,) = call(total_kernel, [jax.ShapeDtypeStruct(part, BF16)], 1 << 18, chips)(kept, *arrived)
+    return out
 
 
 def local_many(
@@ -335,5 +402,8 @@
         P(None, ("fs", "tp"), "sp"),
     )
     out_specs = P(("sp", "fs", "tp"), None)
-    local = local_few if few(count) and mesh.shape["tp"] == 2 else local_many
-    return jax.shard_map(local, mesh=mesh, in_specs=in_specs, out_specs=out_specs, check_vma=False)
+    local = local_few if few(count) and mesh.shape["fs"] == 4 and mesh.shape["tp"] == 2 else local_many
+    step = jax.shard_map(local, mesh=mesh, in_specs=in_specs, out_specs=out_specs, check_vma=False)
+    if local is local_many:
+        return step
+    return step

time: 54.8 us -> 47.6 us (0.87)
  the two profiles are of different devices: /device:TPU:16 before, /device:TPU:0 now
where the time goes in v3:
time: 47.6 us; the launch traced here: 46.8 us
  starting transfers between devices  27 us (57%)
  waiting for transfers between devices  13.3 us (28%)
  Pallas kernels  5.55 us (12%)
  between operations  0.91 us (2%)
    ppermute x3, starting transfers between devices, local_few(): blocks.append(lax.ppermute(packed, 'sp', pairs))  12.6 us
    ppermute x6, waiting for transfers between devices, across(): return lax.ppermute(array, 'fs', [(i, i ^ k) for i in range(chips)])  8.44 us
    ppermute x6, starting transfers between devices, across(): return lax.ppermute(array, 'fs', [(i, i ^ k) for i in range(chips)])  7.04 us
    pallas_call x8, Pallas kernels, placed(): run(*[a if spot is pltpu.SMEM else pltpu.with_memory_space_constraint(a,...  5.55 us
    ppermute x2, starting transfers between devices, local_few(): weights.append(lax.ppermute(out_weight, 'sp', list(pairs)))  4.19 us
    ppermute x2, waiting for transfers between devices, local_few(): weights.append(lax.ppermute(out_weight, 'sp', list(pairs)))  2.32 us
    ppermute x3, waiting for transfers between devices, local_few(): blocks.append(lax.ppermute(packed, 'sp', pairs))  1.59 us
    ppermute x1, starting transfers between devices, local_few(): outer = lax.ppermute(weights[1], 'sp', [(1, 0), (2, 3)])  1.28 us
  transfers between devices with their start and end apart: 19, of which 11 were waited for; matrix products, arithmetic and copies ran while one was open for 0% of the time, Pallas kernels for 10%

profile of v3, /device:TPU:0, one launch (start us, length us, event | category | flops | bytes accessed | tf_op | source)
XLA Modules:
  0.0 46.8 jit_solution(14661720935102682938)
XLA Ops:
  0.0 3.1 %collective-permute-start.11 = (bf16[2,128,512]{2,1,0:T(8,128)(2,1)}, bf16[2,128,512]{2,1,0:T(8,128)(2,1)S(1)}, u32[]{:S(2)}, u32[]{:S(2)}) collective-permute-start(bf16[2,128,512]{2,1,0:T(8,128)(2,1)} %own.1), channel_id=1, source_target_pairs={{16,0},{0,8},{24,16},{8,24},{17,1},{1,9},{25,17},{9,25},{18,2},{2,... | collective-permute-start | bytes 786440 | tf_op jit(solution)/shard_map/ppermute | solution.py:267
  3.1 1.5 %collective-permute-start = (bf16[16,2048]{1,0:T(8,128)(2,1)}, bf16[16,2048]{1,0:T(8,128)(2,1)S(1)}, u32[]{:S(2)}, u32[]{:S(2)}) collective-permute-start(bf16[16,2048]{1,0:T(8,128)(2,1)} %x0.1), channel_id=1, source_target_pairs={{0,2},{2,0},{4,6},{6,4},{1,3},{3,1},{5,7},{7,5},{8,10},{10,8},{12,... | collective-permute-start | bytes 196616 | tf_op jit(solution)/shard_map/ppermute | solution.py:276
  4.5 1.5 %collective-permute-start.1 = (bf16[16,2048]{1,0:T(8,128)(2,1)}, bf16[16,2048]{1,0:T(8,128)(2,1)S(1)}, u32[]{:S(2)}, u32[]{:S(2)}) collective-permute-start(bf16[16,2048]{1,0:T(8,128)(2,1)} %x0.1), channel_id=1, source_target_pairs={{0,4},{2,6},{4,0},{6,2},{1,5},{3,7},{5,1},{7,3},{8,12},{10,14},{12... | collective-permute-start | bytes 196616 | tf_op jit(solution)/shard_map/ppermute | solution.py:276
  6.1 0.5 %collective-permute-start.2 = (bf16[16,2048]{1,0:T(8,128)(2,1)}, bf16[16,2048]{1,0:T(8,128)(2,1)S(1)}, u32[]{:S(2)}, u32[]{:S(2)}) collective-permute-start(bf16[16,2048]{1,0:T(8,128)(2,1)} %x0.1), channel_id=1, source_target_pairs={{0,6},{2,4},{4,2},{6,0},{1,7},{3,5},{5,3},{7,1},{8,14},{10,12},{12... | collective-permute-start | bytes 196616 | tf_op jit(solution)/shard_map/ppermute | solution.py:276
  6.5 0.0 collective-permute-start.3
  6.5 1.0 %collective-permute-done.x1 = bf16[16,2048]{1,0:T(8,128)(2,1)S(1)} collective-permute-done((bf16[16,2048]{1,0:T(8,128)(2,1)}, bf16[16,2048]{1,0:T(8,128)(2,1)S(1)}, u32[]{:S(2)}, u32[]{:S(2)}) %collective-permute-start) | collective-permute-done | bytes 65568 | tf_op jit(solution)/shard_map/ppermute | solution.py:276
  7.5 1.1 %collective-permute-start.10 = (bf16[2,128,512]{2,1,0:T(8,128)(2,1)}, bf16[2,128,512]{2,1,0:T(8,128)(2,1)S(1)}, u32[]{:S(2)}, u32[]{:S(2)}) collective-permute-start(bf16[2,128,512]{2,1,0:T(8,128)(2,1)} %own.1), channel_id=1, source_target_pairs={{8,0},{24,8},{0,16},{16,24},{9,1},{25,9},{1,17},{17,25},{10,2},{26... | collective-permute-start | bytes 786440 | tf_op jit(solution)/shard_map/ppermute | solution.py:267
  8.7 1.1 %collective-permute-done.1.x2 = bf16[16,2048]{1,0:T(8,128)(2,1)S(1)} collective-permute-done((bf16[16,2048]{1,0:T(8,128)(2,1)}, bf16[16,2048]{1,0:T(8,128)(2,1)S(1)}, u32[]{:S(2)}, u32[]{:S(2)}) %collective-permute-start.1) | collective-permute-done | bytes 65568 | tf_op jit(solution)/shard_map/ppermute | solution.py:276
  9.7 0.0 collective-permute-start.4
  9.7 1.7 %collective-permute-done.2.x3 = bf16[16,2048]{1,0:T(8,128)(2,1)S(1)} collective-permute-done((bf16[16,2048]{1,0:T(8,128)(2,1)}, bf16[16,2048]{1,0:T(8,128)(2,1)S(1)}, u32[]{:S(2)}, u32[]{:S(2)}) %collective-permute-start.2) | collective-permute-done | bytes 65568 | tf_op jit(solution)/shard_map/ppermute | solution.py:276
  11.4 0.0 collective-permute-start.5
  11.4 0.0 collective-permute-done.11.refs_13_.second
  11.4 0.5 %collective-permute-start.6 = (bf16[16,2048]{1,0:T(8,128)(2,1)S(1)}, bf16[16,2048]{1,0:T(8,128)(2,1)S(1)}, u32[]{:S(2)}, u32[]{:S(2)}) collective-permute-start(bf16[16,2048]{1,0:T(8,128)(2,1)S(1)} %collective-permute-done.2.x3), channel_id=1, source_target_pairs={{0,1},{1,0},{2,3},{3,2},{4,5},{5,4},{6,7},{7,6},{8,9},{9,8},{10,11... | collective-permute-start | bytes 196616 | tf_op jit(solution)/shard_map/ppermute | solution.py:279
  12.0 1.1 %shard_map.136 = (f32[128,128]{1,0:T(8,128)S(1)}, f32[128,128]{1,0:T(8,128)S(1)}, f32[128,128]{1,0:T(8,128)S(1)}, f32[8,128]{1,0:T(8,128)S(1)}, f32[1,2048]{1,0:...) custom-call(f32[1,128]{1,0:T(1,128)} %decay_h.1, f32[1,2048]{1,0:T(1,128)} %bitcast.7, f32[1,128]{1,0:T(1,128)} %bitcast.8, ...), custom_call_target="tpu_custom_call" | custom-call | flops 30000001024 | bytes 1048576 | tf_op jit(solution)/shard_map/pallas_call | solution.py:245
  13.1 0.0 copy-start.3
  13.1 0.0 copy-start.7
  13.2 0.0 collective-permute-done.3.y0
  13.2 0.8 %collective-permute-start.14 = (bf16[2,128,512]{2,1,0:T(8,128)(2,1)S(1)}, bf16[2,128,512]{2,1,0:T(8,128)(2,1)S(1)}, u32[]{:S(2)}, u32[]{:S(2)}) collective-permute-start(bf16[2,128,512]{2,1,0:T(8,128)(2,1)S(1)} %shard_map.140), channel_id=1, source_target_pairs={{16,8},{24,16},{17,9},{25,17},{18,10},{26,18},{19,11},{27,19},{20,... | collective-permute-start | bytes 786440 | tf_op jit(solution)/shard_map/ppermute | solution.py:270
  14.0 2.3 %collective-permute-done.10.refs_12_ = bf16[2,128,512]{2,1,0:T(8,128)(2,1)S(1)} collective-permute-done((bf16[2,128,512]{2,1,0:T(8,128)(2,1)}, bf16[2,128,512]{2,1,0:T(8,128)(2,1)S(1)}, u32[]{:S(2)}, u32[]{:S(2)}) %collective-permute-start.10) | collective-permute-done | bytes 262176 | tf_op jit(solution)/shard_map/ppermute | solution.py:267
  16.3 1.3 %collective-permute-start.13 = (bf16[2,128,512]{2,1,0:T(8,128)(2,1)S(1)}, bf16[2,128,512]{2,1,0:T(8,128)(2,1)S(1)}, u32[]{:S(2)}, u32[]{:S(2)}) collective-permute-start(bf16[2,128,512]{2,1,0:T(8,128)(2,1)S(1)} %collective-permute-done.10.refs_12_), channel_id=1, source_target_pairs={{8,0},{16,24},{9,1},{17,25},{10,2},{18,26},{11,3},{19,27},{12,4},{... | collective-permute-start | bytes 786440 | tf_op jit(solution)/shard_map/ppermute | solution.py:268
  17.6 0.0 collective-permute-done.4.y1
  17.6 0.0 collective-permute-done.5.y2
  17.6 0.0 collective-permute-done.6.y3
  17.7 0.0 copy-start.1
  17.7 0.0 copy-start.2
  17.7 1.1 %shard_map.137 = (bf16[128,2048]{1,0:T(8,128)(2,1)S(1)}, bf16[392,128]{1,0:T(8,128)(2,1)S(1)}, bf16[128,128]{1,0:T(8,128)(2,1)S(1)}, bf16[128,128]{1,0:T(8,128)(2,1)S(1)}) custom-call(bf16[16,2048]{1,0:T(8,128)(2,1)S(1)} %copy-done.7, bf16[16,2048]{1,0:T(8,128)(2,1)S(1)} %collective-permute-done.x1, bf16[16,2048]{1,0:T(8,128)(2,1)S(1)} %collective-permute-done.1.x2, ...), custom_call_target="tpu_custom_call" | custom-call | flops 268435456 | bytes 1048576 | tf_op jit(solution)/shard_map/pallas_call | solution.py:245
  18.9 5.4 %collective-permute-start.7 = (bf16[392,128]{1,0:T(8,128)(2,1)S(1)}, bf16[392,128]{1,0:T(8,128)(2,1)S(1)}, u32[]{:S(2)}, u32[]{:S(2)}) collective-permute-start(bf16[392,128]{1,0:T(8,128)(2,1)S(1)} %get-tuple-element.35.packed), channel_id=1, source_target_pairs={{0,8},{8,16},{16,24},{1,9},{9,17},{17,25},{2,10},{10,18},{18,26},{... | collective-permute-start | bytes 301064 | tf_op jit(solution)/shard_map/ppermute | solution.py:301
  24.3 5.8 %collective-permute-start.8 = (bf16[392,128]{1,0:T(8,128)(2,1)S(1)}, bf16[392,128]{1,0:T(8,128)(2,1)S(1)}, u32[]{:S(2)}, u32[]{:S(2)}) collective-permute-start(bf16[392,128]{1,0:T(8,128)(2,1)S(1)} %get-tuple-element.35.packed), channel_id=1, source_target_pairs={{0,16},{8,24},{1,17},{9,25},{2,18},{10,26},{3,19},{11,27},{4,20},{... | collective-permute-start | bytes 301064 | tf_op jit(solution)/shard_map/ppermute | solution.py:301
  30.2 1.3 %collective-permute-start.9 = (bf16[392,128]{1,0:T(8,128)(2,1)S(1)}, bf16[392,128]{1,0:T(8,128)(2,1)S(1)}, u32[]{:S(2)}, u32[]{:S(2)}) collective-permute-start(bf16[392,128]{1,0:T(8,128)(2,1)S(1)} %get-tuple-element.35.packed), channel_id=1, source_target_pairs={{0,24},{1,25},{2,26},{3,27},{4,28},{5,29},{6,30},{7,31}} | collective-permute-start | bytes 301064 | tf_op jit(solution)/shard_map/ppermute | solution.py:301
  32.1 1.1 %shard_map.138 = (bf16[128,128]{1,0:T(8,128)(2,1)S(1)}, f32[128,128]{1,0:T(8,128)S(1)}, f32[128,128]{1,0:T(8,128)S(1)}, f32[2,128,128]{2,1,0:T(8,128)S(1)}, f32[...) custom-call(f32[1]{0:T(128)S(6)} %copy.15.lam, bf16[128,2048]{1,0:T(8,128)(2,1)S(1)} %get-tuple-element.34.normed, ...), custom_call_target="tpu_custom_call" | custom-call | flops 134217728 | bytes 1048576 | tf_op jit(solution)/shard_map/pallas_call | solution.py:245
  33.2 0.2 collective-permute-done.8.refs_9_
  33.4 1.4 %collective-permute-done.9.refs_10_ = bf16[392,128]{1,0:T(8,128)(2,1)S(1)} collective-permute-done((bf16[392,128]{1,0:T(8,128)(2,1)S(1)}, bf16[392,128]{1,0:T(8,128)(2,1)S(1)}, u32[]{:S(2)}, u32[]{:S(2)}) %collective-permute-start.9) | collective-permute-done | bytes 100384 | tf_op jit(solution)/shard_map/ppermute | solution.py:301
  34.8 1.3 %shard_map.139 = (f32[64,1536]{1,0:T(8,128)S(1)}, bf16[64,1536]{1,0:T(8,128)(2,1)S(1)}, bf16[128,256]{1,0:T(8,128)(2,1)S(1)}) custom-call(bf16[128,128]{1,0:T(8,128)(2,1)S(1)} %get-tuple-element.40.refs_0_, f32[128,128]{1,0:T(8,128)S(1)} %get-tuple-element.41.refs_1_, f32[128,128]{1,0:T(8,128)S(1)} %get-tuple-element.42.refs_2_, ...), custom_call_target="tpu_custom_call" | custom-call | flops 134217728 | bytes 1048576 | tf_op jit(solution)/shard_map/pallas_call | solution.py:245
  36.1 0.1 collective-permute-start.12
  36.1 0.0 collective-permute-done.14.inner
  36.2 0.0 collective-permute-done.13.outer
  36.2 0.2 shard_map.141
  36.4 0.5 %collective-permute-start.15 = (bf16[64,512]{1,0:T(8,128)(2,1)S(1)}, bf16[64,512]{1,0:T(8,128)(2,1)S(1)}, u32[]{:S(2)}, u32[]{:S(2)}) collective-permute-start(bf16[64,512]{1,0:T(8,128)(2,1)S(1)} %get-tuple-element.52), channel_id=1, source_target_pairs={{0,1},{1,0},{2,3},{3,2},{4,5},{5,4},{6,7},{7,6},{8,9},{9,8},{10,11... | collective-permute-start | bytes 196616 | tf_op jit(solution)/shard_map/ppermute | solution.py:279
  36.9 0.7 %collective-permute-done.12.other = bf16[64,1536]{1,0:T(8,128)(2,1)S(1)} collective-permute-done((bf16[64,1536]{1,0:T(8,128)(2,1)S(1)}, bf16[64,1536]{1,0:T(8,128)(2,1)S(1)}, u32[]{:S(2)}, u32[]{:S(2)}) %collective-permute-start.12) | collective-permute-done | bytes 196640 | tf_op jit(solution)/shard_map/ppermute | solution.py:279
  37.6 0.2 collective-permute-done.15.last_other
  37.8 0.1 shard_map.142
  37.9 1.6 %collective-permute-start.16 = (bf16[16,2048]{1,0:T(8,128)(2,1)S(1)}, bf16[16,2048]{1,0:T(8,128)(2,1)S(1)}, u32[]{:S(2)}, u32[]{:S(2)}) collective-permute-start(bf16[16,2048]{1,0:T(8,128)(2,1)S(1)} %get-tuple-element.54), channel_id=1, source_target_pairs={{0,2},{2,0},{4,6},{6,4},{1,3},{3,1},{5,7},{7,5},{8,10},{10,8},{12,... | collective-permute-start | bytes 196616 | tf_op jit(solution)/shard_map/ppermute | solution.py:276
  39.4 1.5 %collective-permute-start.17 = (bf16[16,2048]{1,0:T(8,128)(2,1)S(1)}, bf16[16,2048]{1,0:T(8,128)(2,1)S(1)}, u32[]{:S(2)}, u32[]{:S(2)}) collective-permute-start(bf16[16,2048]{1,0:T(8,128)(2,1)S(1)} %get-tuple-element.55), channel_id=1, source_target_pairs={{0,4},{2,6},{4,0},{6,2},{1,5},{3,7},{5,1},{7,3},{8,12},{10,14},{12... | collective-permute-start | bytes 196616 | tf_op jit(solution)/shard_map/ppermute | solution.py:276
  41.0 0.5 %collective-permute-start.18 = (bf16[16,2048]{1,0:T(8,128)(2,1)S(1)}, bf16[16,2048]{1,0:T(8,128)(2,1)S(1)}, u32[]{:S(2)}, u32[]{:S(2)}) collective-permute-start(bf16[16,2048]{1,0:T(8,128)(2,1)S(1)} %get-tuple-element.56), channel_id=1, source_target_pairs={{0,6},{2,4},{4,2},{6,0},{1,7},{3,5},{5,3},{7,1},{8,14},{10,12},{12... | collective-permute-start | bytes 196616 | tf_op jit(solution)/shard_map/ppermute | solution.py:276
  41.4 0.9 %collective-permute-done.16.refs_0_ = bf16[16,2048]{1,0:T(8,128)(2,1)S(1)} collective-permute-done((bf16[16,2048]{1,0:T(8,128)(2,1)S(1)}, bf16[16,2048]{1,0:T(8,128)(2,1)S(1)}, u32[]{:S(2)}, u32[]{:S(2)}) %collective-permute-start.16) | collective-permute-done | bytes 65568 | tf_op jit(solution)/shard_map/ppermute | solution.py:276
  42.3 1.4 %collective-permute-done.17.refs_1_ = bf16[16,2048]{1,0:T(8,128)(2,1)S(1)} collective-permute-done((bf16[16,2048]{1,0:T(8,128)(2,1)S(1)}, bf16[16,2048]{1,0:T(8,128)(2,1)S(1)}, u32[]{:S(2)}, u32[]{:S(2)}) %collective-permute-start.17) | collective-permute-done | bytes 65568 | tf_op jit(solution)/shard_map/ppermute | solution.py:276
  43.7 2.4 %collective-permute-done.18.refs_2_ = bf16[16,2048]{1,0:T(8,128)(2,1)S(1)} collective-permute-done((bf16[16,2048]{1,0:T(8,128)(2,1)S(1)}, bf16[16,2048]{1,0:T(8,128)(2,1)S(1)}, u32[]{:S(2)}, u32[]{:S(2)}) %collective-permute-start.18) | collective-permute-done | bytes 65568 | tf_op jit(solution)/shard_map/ppermute | solution.py:276
  46.1 0.7 %shard_map.143 = bf16[16,2048]{1,0:T(8,128)(2,1)} custom-call(f32[16,2048]{1,0:T(8,128)S(1)} %get-tuple-element.53.mine, bf16[16,2048]{1,0:T(8,128)(2,1)S(1)} %collective-permute-done.16.refs_0_, bf16[16,2048]{1,0:T(8,128)(2,1)S(1)} %collective-permute-done.17.refs_1_, bf16[16,2048]{1,0:T(8,128)(2,1)S(1)} %collective-permute-done.18.refs_2_), custom_call_target="tpu_custom_call" | custom-call | flops 262144 | bytes 1048576 | tf_op jit(solution)/shard_map/pallas_call | solution.py:245
  (14 shorter events, 0.1 us)
Async XLA Ops:
  0.0 11.4 %collective-permute-start.11 = (bf16[2,128,512]{2,1,0:T(8,128)(2,1)}, bf16[2,128,512]{2,1,0:T(8,128)(2,1)S(1)}, u32[]{:S(2)}, u32[]{:S(2)}) collective-permute-start(bf16[2,128,512]{2,1,0:T(8,128)(2,1)} %own.1), channel_id=1, source_target_pairs={{16,0},{0,8},{24,16},{8,24},{17,1},{1,9},{25,17},{9,25},{18,2},{2,... | collective-permute-start | bytes 786440 | tf_op jit(solution)/shard_map/ppermute | solution.py:267
  3.1 4.5 %collective-permute-start = (bf16[16,2048]{1,0:T(8,128)(2,1)}, bf16[16,2048]{1,0:T(8,128)(2,1)S(1)}, u32[]{:S(2)}, u32[]{:S(2)}) collective-permute-start(bf16[16,2048]{1,0:T(8,128)(2,1)} %x0.1), channel_id=1, source_target_pairs={{0,2},{2,0},{4,6},{6,4},{1,3},{3,1},{5,7},{7,5},{8,10},{10,8},{12,... | collective-permute-start | bytes 196616 | tf_op jit(solution)/shard_map/ppermute | solution.py:276
  4.5 5.2 %collective-permute-start.1 = (bf16[16,2048]{1,0:T(8,128)(2,1)}, bf16[16,2048]{1,0:T(8,128)(2,1)S(1)}, u32[]{:S(2)}, u32[]{:S(2)}) collective-permute-start(bf16[16,2048]{1,0:T(8,128)(2,1)} %x0.1), channel_id=1, source_target_pairs={{0,4},{2,6},{4,0},{6,2},{1,5},{3,7},{5,1},{7,3},{8,12},{10,14},{12... | collective-permute-start | bytes 196616 | tf_op jit(solution)/shard_map/ppermute | solution.py:276
  6.1 5.4 %collective-permute-start.2 = (bf16[16,2048]{1,0:T(8,128)(2,1)}, bf16[16,2048]{1,0:T(8,128)(2,1)S(1)}, u32[]{:S(2)}, u32[]{:S(2)}) collective-permute-start(bf16[16,2048]{1,0:T(8,128)(2,1)} %x0.1), channel_id=1, source_target_pairs={{0,6},{2,4},{4,2},{6,0},{1,7},{3,5},{5,3},{7,1},{8,14},{10,12},{12... | collective-permute-start | bytes 196616 | tf_op jit(solution)/shard_map/ppermute | solution.py:276
  6.5 6.6 %collective-permute-start.3 = (bf16[16,2048]{1,0:T(8,128)(2,1)}, bf16[16,2048]{1,0:T(8,128)(2,1)S(1)}, u32[]{:S(2)}, u32[]{:S(2)}) collective-permute-start(bf16[16,2048]{1,0:T(8,128)(2,1)} %x0.1), channel_id=1, source_target_pairs={{0,1},{1,0},{2,3},{3,2},{4,5},{5,4},{6,7},{7,6},{8,9},{9,8},{10,11... | collective-permute-start | bytes 196616 | tf_op jit(solution)/shard_map/ppermute | solution.py:279
  7.5 8.8 %collective-permute-start.10 = (bf16[2,128,512]{2,1,0:T(8,128)(2,1)}, bf16[2,128,512]{2,1,0:T(8,128)(2,1)S(1)}, u32[]{:S(2)}, u32[]{:S(2)}) collective-permute-start(bf16[2,128,512]{2,1,0:T(8,128)(2,1)} %own.1), channel_id=1, source_target_pairs={{8,0},{24,8},{0,16},{16,24},{9,1},{25,9},{1,17},{17,25},{10,2},{26... | collective-permute-start | bytes 786440 | tf_op jit(solution)/shard_map/ppermute | solution.py:267
  9.7 7.9 %collective-permute-start.4 = (bf16[16,2048]{1,0:T(8,128)(2,1)S(1)}, bf16[16,2048]{1,0:T(8,128)(2,1)S(1)}, u32[]{:S(2)}, u32[]{:S(2)}) collective-permute-start(bf16[16,2048]{1,0:T(8,128)(2,1)S(1)} %collective-permute-done.x1), channel_id=1, source_target_pairs={{0,1},{1,0},{2,3},{3,2},{4,5},{5,4},{6,7},{7,6},{8,9},{9,8},{10,11... | collective-permute-start | bytes 196616 | tf_op jit(solution)/shard_map/ppermute | solution.py:279
  11.4 6.2 %collective-permute-start.5 = (bf16[16,2048]{1,0:T(8,128)(2,1)S(1)}, bf16[16,2048]{1,0:T(8,128)(2,1)S(1)}, u32[]{:S(2)}, u32[]{:S(2)}) collective-permute-start(bf16[16,2048]{1,0:T(8,128)(2,1)S(1)} %collective-permute-done.1.x2), channel_id=1, source_target_pairs={{0,1},{1,0},{2,3},{3,2},{4,5},{5,4},{6,7},{7,6},{8,9},{9,8},{10,11... | collective-permute-start | bytes 196616 | tf_op jit(solution)/shard_map/ppermute | solution.py:279
  11.4 6.2 %collective-permute-start.6 = (bf16[16,2048]{1,0:T(8,128)(2,1)S(1)}, bf16[16,2048]{1,0:T(8,128)(2,1)S(1)}, u32[]{:S(2)}, u32[]{:S(2)}) collective-permute-start(bf16[16,2048]{1,0:T(8,128)(2,1)S(1)} %collective-permute-done.2.x3), channel_id=1, source_target_pairs={{0,1},{1,0},{2,3},{3,2},{4,5},{5,4},{6,7},{7,6},{8,9},{9,8},{10,11... | collective-permute-start | bytes 196616 | tf_op jit(solution)/shard_map/ppermute | solution.py:279
  12.0 1.2 %copy-start = (bf16[2,128,512]{2,1,0:T(8,128)(2,1)S(1)}, bf16[2,128,512]{2,1,0:T(8,128)(2,1)}, u32[]{:S(2)}) copy-start(bf16[2,128,512]{2,1,0:T(8,128)(2,1)} %own.1) | copy-start | bytes 786436
  12.0 5.7 %copy-start.4 = (bf16[2048,128]{1,0:T(8,128)(2,1)S(1)}, bf16[2048,128]{1,0:T(8,128)(2,1)}, u32[]{:S(2)}) copy-start(bf16[2048,128]{1,0:T(8,128)(2,1)} %dv.1) | copy-start | bytes 1572868
  12.0 5.7 %copy-start.5 = (bf16[2048,128]{1,0:T(8,128)(2,1)S(1)}, bf16[2048,128]{1,0:T(8,128)(2,1)}, u32[]{:S(2)}) copy-start(bf16[2048,128]{1,0:T(8,128)(2,1)} %wk.1) | copy-start | bytes 1572868
  12.0 5.7 %copy-start.6 = (bf16[2048,128]{1,0:T(8,128)(2,1)S(1)}, bf16[2048,128]{1,0:T(8,128)(2,1)}, u32[]{:S(2)}) copy-start(bf16[2048,128]{1,0:T(8,128)(2,1)} %wv.1) | copy-start | bytes 1572868
  13.1 4.6 %copy-start.3 = (bf16[2,2048,64]{1,2,0:T(8,128)(2,1)S(1)}, bf16[2,2048,64]{1,2,0:T(8,128)(2,1)}, u32[]{:S(2)}) copy-start(bf16[2,2048,64]{1,2,0:T(8,128)(2,1)} %param.23) | copy-start | bytes 1572868
  13.1 4.6 %copy-start.7 = (bf16[16,2048]{1,0:T(8,128)(2,1)S(1)}, bf16[16,2048]{1,0:T(8,128)(2,1)}, u32[]{:S(2)}) copy-start(bf16[16,2048]{1,0:T(8,128)(2,1)} %x0.1) | copy-start | bytes 196612
  13.2 23.0 %collective-permute-start.14 = (bf16[2,128,512]{2,1,0:T(8,128)(2,1)S(1)}, bf16[2,128,512]{2,1,0:T(8,128)(2,1)S(1)}, u32[]{:S(2)}, u32[]{:S(2)}) collective-permute-start(bf16[2,128,512]{2,1,0:T(8,128)(2,1)S(1)} %shard_map.140), channel_id=1, source_target_pairs={{16,8},{24,16},{17,9},{25,17},{18,10},{26,18},{19,11},{27,19},{20,... | collective-permute-start | bytes 786440 | tf_op jit(solution)/shard_map/ppermute | solution.py:270
  16.3 19.8 %collective-permute-start.13 = (bf16[2,128,512]{2,1,0:T(8,128)(2,1)S(1)}, bf16[2,128,512]{2,1,0:T(8,128)(2,1)S(1)}, u32[]{:S(2)}, u32[]{:S(2)}) collective-permute-start(bf16[2,128,512]{2,1,0:T(8,128)(2,1)S(1)} %collective-permute-done.10.refs_12_), channel_id=1, source_target_pairs={{8,0},{16,24},{9,1},{17,25},{10,2},{18,26},{11,3},{19,27},{12,4},{... | collective-permute-start | bytes 786440 | tf_op jit(solution)/shard_map/ppermute | solution.py:268
  17.7 14.4 %copy-start.1 = (bf16[2048,128]{1,0:T(8,128)(2,1)S(1)}, bf16[2048,128]{1,0:T(8,128)(2,1)}, u32[]{:S(2)}) copy-start(bf16[2048,128]{1,0:T(8,128)(2,1)} %wq.1) | copy-start | bytes 1572868
  17.7 14.4 %copy-start.2 = (bf16[2,2048,64]{1,2,0:T(8,128)(2,1)S(1)}, bf16[2,2048,64]{1,2,0:T(8,128)(2,1)}, u32[]{:S(2)}) copy-start(bf16[2,2048,64]{1,2,0:T(8,128)(2,1)} %param.22) | copy-start | bytes 1572868
  18.9 14.3 %collective-permute-start.7 = (bf16[392,128]{1,0:T(8,128)(2,1)S(1)}, bf16[392,128]{1,0:T(8,128)(2,1)S(1)}, u32[]{:S(2)}, u32[]{:S(2)}) collective-permute-start(bf16[392,128]{1,0:T(8,128)(2,1)S(1)} %get-tuple-element.35.packed), channel_id=1, source_target_pairs={{0,8},{8,16},{16,24},{1,9},{9,17},{17,25},{2,10},{10,18},{18,26},{... | collective-permute-start | bytes 301064 | tf_op jit(solution)/shard_map/ppermute | solution.py:301
  24.3 9.1 %collective-permute-start.8 = (bf16[392,128]{1,0:T(8,128)(2,1)S(1)}, bf16[392,128]{1,0:T(8,128)(2,1)S(1)}, u32[]{:S(2)}, u32[]{:S(2)}) collective-permute-start(bf16[392,128]{1,0:T(8,128)(2,1)S(1)} %get-tuple-element.35.packed), channel_id=1, source_target_pairs={{0,16},{8,24},{1,17},{9,25},{2,18},{10,26},{3,19},{11,27},{4,20},{... | collective-permute-start | bytes 301064 | tf_op jit(solution)/shard_map/ppermute | solution.py:301
  30.2 4.6 %collective-permute-start.9 = (bf16[392,128]{1,0:T(8,128)(2,1)S(1)}, bf16[392,128]{1,0:T(8,128)(2,1)S(1)}, u32[]{:S(2)}, u32[]{:S(2)}) collective-permute-start(bf16[392,128]{1,0:T(8,128)(2,1)S(1)} %get-tuple-element.35.packed), channel_id=1, source_target_pairs={{0,24},{1,25},{2,26},{3,27},{4,28},{5,29},{6,30},{7,31}} | collective-permute-start | bytes 301064 | tf_op jit(solution)/shard_map/ppermute | solution.py:301
  36.1 1.5 %collective-permute-start.12 = (bf16[64,1536]{1,0:T(8,128)(2,1)S(1)}, bf16[64,1536]{1,0:T(8,128)(2,1)S(1)}, u32[]{:S(2)}, u32[]{:S(2)}) collective-permute-start(bf16[64,1536]{1,0:T(8,128)(2,1)S(1)} %get-tuple-element.49), channel_id=1, source_target_pairs={{0,1},{1,0},{2,3},{3,2},{4,5},{5,4},{6,7},{7,6},{8,9},{9,8},{10,11... | collective-permute-start | bytes 589832 | tf_op jit(solution)/shard_map/ppermute | solution.py:279
  36.4 1.4 %collective-permute-start.15 = (bf16[64,512]{1,0:T(8,128)(2,1)S(1)}, bf16[64,512]{1,0:T(8,128)(2,1)S(1)}, u32[]{:S(2)}, u32[]{:S(2)}) collective-permute-start(bf16[64,512]{1,0:T(8,128)(2,1)S(1)} %get-tuple-element.52), channel_id=1, source_target_pairs={{0,1},{1,0},{2,3},{3,2},{4,5},{5,4},{6,7},{7,6},{8,9},{9,8},{10,11... | collective-permute-start | bytes 196616 | tf_op jit(solution)/shard_map/ppermute | solution.py:279
  37.9 4.4 %collective-permute-start.16 = (bf16[16,2048]{1,0:T(8,128)(2,1)S(1)}, bf16[16,2048]{1,0:T(8,128)(2,1)S(1)}, u32[]{:S(2)}, u32[]{:S(2)}) collective-permute-start(bf16[16,2048]{1,0:T(8,128)(2,1)S(1)} %get-tuple-element.54), channel_id=1, source_target_pairs={{0,2},{2,0},{4,6},{6,4},{1,3},{3,1},{5,7},{7,5},{8,10},{10,8},{12,... | collective-permute-start | bytes 196616 | tf_op jit(solution)/shard_map/ppermute | solution.py:276
  39.4 4.3 %collective-permute-start.17 = (bf16[16,2048]{1,0:T(8,128)(2,1)S(1)}, bf16[16,2048]{1,0:T(8,128)(2,1)S(1)}, u32[]{:S(2)}, u32[]{:S(2)}) collective-permute-start(bf16[16,2048]{1,0:T(8,128)(2,1)S(1)} %get-tuple-element.55), channel_id=1, source_target_pairs={{0,4},{2,6},{4,0},{6,2},{1,5},{3,7},{5,1},{7,3},{8,12},{10,14},{12... | collective-permute-start | bytes 196616 | tf_op jit(solution)/shard_map/ppermute | solution.py:276
  41.0 5.2 %collective-permute-start.18 = (bf16[16,2048]{1,0:T(8,128)(2,1)S(1)}, bf16[16,2048]{1,0:T(8,128)(2,1)S(1)}, u32[]{:S(2)}, u32[]{:S(2)}) collective-permute-start(bf16[16,2048]{1,0:T(8,128)(2,1)S(1)} %get-tuple-element.56), channel_id=1, source_target_pairs={{0,6},{2,4},{4,2},{6,0},{1,7},{3,5},{5,3},{7,1},{8,14},{10,12},{12... | collective-permute-start | bytes 196616 | tf_op jit(solution)/shard_map/ppermute | solution.py:276

commit v4 on v3

--- a/solution.py
+++ b/solution.py
@@ -39,6 +39,11 @@
 
 ROUNDS = (lambda at: lax.rem(2 * at + 1, 5), lambda at: lax.rem(3 * at + 2, 5))
 ROUND_PAIRS = (((1, 0), (3, 1), (0, 2), (2, 3)), ((2, 0), (0, 1), (3, 2), (1, 3)))
+
+
+def halves(a):
+    high = a.astype(BF16)
+    return high, (a - high.astype(F32)).astype(BF16)
 
 
 def few(count):
@@ -110,7 +115,8 @@
     v = nn(rounded, wv[...]).astype(BF16)
     ret_k[...] = k
     ret_v[...] = v
-    state = tn(k.astype(F32) * key_scale[...], v.astype(F32), precision=HIGHEST)
+    weighted, rest = halves(k.astype(F32) * key_scale[...])
+    state = tn(weighted, v) + tn(rest, v)
     packed[2 * rows : 2 * rows + head, :] = state.astype(BF16)
     packed[2 * rows + head :, :] = factor[...].astype(BF16)
 
@@ -161,7 +167,8 @@
             if i != j:
                 carry = carry * jnp.where(jnp.logical_and(source[i] > source[j], before[i]), factor, 1.0)
         entering = entering + carry * block[2 * rows : 2 * rows + head, :].astype(F32)
-    ret_out = inner[...] + nn(scaled[...], entering, precision=HIGHEST)
+    (left, left_rest), (right, right_rest) = halves(scaled[...]), halves(entering)
+    ret_out = inner[...] + nn(left, right) + nn(left, right_rest) + nn(left_rest, right)
     centre = ret_out - jnp.mean(ret_out, axis=-1, keepdims=True)
     spread = lax.rsqrt(jnp.mean(centre * centre, axis=-1, keepdims=True) + EPS)
     ret_mix = (centre * spread * small[0:1, :]).astype(BF16)

time: 47.6 us -> 47.5 us (level)
  no operation moved by 1% of the time
where the time goes in v4:
time: 47.5 us; the launch traced here: 46.7 us
  starting transfers between devices  27 us (57%)
  waiting for transfers between devices  13.3 us (28%)
  Pallas kernels  5.43 us (11%)
  between operations  0.91 us (2%)
    ppermute x3, starting transfers between devices, local_few(): blocks.append(lax.ppermute(packed, 'sp', pairs))  12.6 us
    ppermute x6, waiting for transfers between devices, across(): return lax.ppermute(array, 'fs', [(i, i ^ k) for i in range(chips)])  8.44 us
    ppermute x6, starting transfers between devices, across(): return lax.ppermute(array, 'fs', [(i, i ^ k) for i in range(chips)])  7.04 us
    pallas_call x8, Pallas kernels, placed(): run(*[a if spot is pltpu.SMEM else pltpu.with_memory_space_constraint(a,...  5.43 us
    ppermute x2, starting transfers between devices, local_few(): weights.append(lax.ppermute(out_weight, 'sp', list(pairs)))  4.19 us
    ppermute x2, waiting for transfers between devices, local_few(): weights.append(lax.ppermute(out_weight, 'sp', list(pairs)))  2.32 us
    ppermute x3, waiting for transfers between devices, local_few(): blocks.append(lax.ppermute(packed, 'sp', pairs))  1.6 us
    ppermute x1, starting transfers between devices, local_few(): outer = lax.ppermute(weights[1], 'sp', [(1, 0), (2, 3)])  1.28 us
  transfers between devices with their start and end apart: 19, of which 11 were waited for; matrix products, arithmetic and copies ran while one was open for 0% of the time, Pallas kernels for 10%

profile of v4, /device:TPU:0, one launch (start us, length us, event | category | flops | bytes accessed | tf_op | source)
XLA Modules:
  0.0 46.7 jit_solution(5903861295527850558)
XLA Ops:
  0.0 3.1 %collective-permute-start.11 = (bf16[2,128,512]{2,1,0:T(8,128)(2,1)}, bf16[2,128,512]{2,1,0:T(8,128)(2,1)S(1)}, u32[]{:S(2)}, u32[]{:S(2)}) collective-permute-start(bf16[2,128,512]{2,1,0:T(8,128)(2,1)} %own.1), channel_id=1, source_target_pairs={{16,0},{0,8},{24,16},{8,24},{17,1},{1,9},{25,17},{9,25},{18,2},{2,... | collective-permute-start | bytes 786440 | tf_op jit(solution)/shard_map/ppermute | solution.py:274
  3.1 1.5 %collective-permute-start = (bf16[16,2048]{1,0:T(8,128)(2,1)}, bf16[16,2048]{1,0:T(8,128)(2,1)S(1)}, u32[]{:S(2)}, u32[]{:S(2)}) collective-permute-start(bf16[16,2048]{1,0:T(8,128)(2,1)} %x0.1), channel_id=1, source_target_pairs={{0,2},{2,0},{4,6},{6,4},{1,3},{3,1},{5,7},{7,5},{8,10},{10,8},{12,... | collective-permute-start | bytes 196616 | tf_op jit(solution)/shard_map/ppermute | solution.py:283
  4.5 1.5 %collective-permute-start.1 = (bf16[16,2048]{1,0:T(8,128)(2,1)}, bf16[16,2048]{1,0:T(8,128)(2,1)S(1)}, u32[]{:S(2)}, u32[]{:S(2)}) collective-permute-start(bf16[16,2048]{1,0:T(8,128)(2,1)} %x0.1), channel_id=1, source_target_pairs={{0,4},{2,6},{4,0},{6,2},{1,5},{3,7},{5,1},{7,3},{8,12},{10,14},{12... | collective-permute-start | bytes 196616 | tf_op jit(solution)/shard_map/ppermute | solution.py:283
  6.1 0.5 %collective-permute-start.2 = (bf16[16,2048]{1,0:T(8,128)(2,1)}, bf16[16,2048]{1,0:T(8,128)(2,1)S(1)}, u32[]{:S(2)}, u32[]{:S(2)}) collective-permute-start(bf16[16,2048]{1,0:T(8,128)(2,1)} %x0.1), channel_id=1, source_target_pairs={{0,6},{2,4},{4,2},{6,0},{1,7},{3,5},{5,3},{7,1},{8,14},{10,12},{12... | collective-permute-start | bytes 196616 | tf_op jit(solution)/shard_map/ppermute | solution.py:283
  6.5 0.0 collective-permute-start.3
  6.5 1.0 %collective-permute-done.x1 = bf16[16,2048]{1,0:T(8,128)(2,1)S(1)} collective-permute-done((bf16[16,2048]{1,0:T(8,128)(2,1)}, bf16[16,2048]{1,0:T(8,128)(2,1)S(1)}, u32[]{:S(2)}, u32[]{:S(2)}) %collective-permute-start) | collective-permute-done | bytes 65568 | tf_op jit(solution)/shard_map/ppermute | solution.py:283
  7.5 1.1 %collective-permute-start.10 = (bf16[2,128,512]{2,1,0:T(8,128)(2,1)}, bf16[2,128,512]{2,1,0:T(8,128)(2,1)S(1)}, u32[]{:S(2)}, u32[]{:S(2)}) collective-permute-start(bf16[2,128,512]{2,1,0:T(8,128)(2,1)} %own.1), channel_id=1, source_target_pairs={{8,0},{24,8},{0,16},{16,24},{9,1},{25,9},{1,17},{17,25},{10,2},{26... | collective-permute-start | bytes 786440 | tf_op jit(solution)/shard_map/ppermute | solution.py:274
  8.7 1.1 %collective-permute-done.1.x2 = bf16[16,2048]{1,0:T(8,128)(2,1)S(1)} collective-permute-done((bf16[16,2048]{1,0:T(8,128)(2,1)}, bf16[16,2048]{1,0:T(8,128)(2,1)S(1)}, u32[]{:S(2)}, u32[]{:S(2)}) %collective-permute-start.1) | collective-permute-done | bytes 65568 | tf_op jit(solution)/shard_map/ppermute | solution.py:283
  9.7 0.0 collective-permute-start.4
  9.7 1.7 %collective-permute-done.2.x3 = bf16[16,2048]{1,0:T(8,128)(2,1)S(1)} collective-permute-done((bf16[16,2048]{1,0:T(8,128)(2,1)}, bf16[16,2048]{1,0:T(8,128)(2,1)S(1)}, u32[]{:S(2)}, u32[]{:S(2)}) %collective-permute-start.2) | collective-permute-done | bytes 65568 | tf_op jit(solution)/shard_map/ppermute | solution.py:283
  11.4 0.0 collective-permute-start.5
  11.4 0.0 collective-permute-done.11.refs_13_.second
  11.4 0.5 %collective-permute-start.6 = (bf16[16,2048]{1,0:T(8,128)(2,1)S(1)}, bf16[16,2048]{1,0:T(8,128)(2,1)S(1)}, u32[]{:S(2)}, u32[]{:S(2)}) collective-permute-start(bf16[16,2048]{1,0:T(8,128)(2,1)S(1)} %collective-permute-done.2.x3), channel_id=1, source_target_pairs={{0,1},{1,0},{2,3},{3,2},{4,5},{5,4},{6,7},{7,6},{8,9},{9,8},{10,11... | collective-permute-start | bytes 196616 | tf_op jit(solution)/shard_map/ppermute | solution.py:286
  12.0 1.1 %shard_map.136 = (f32[128,128]{1,0:T(8,128)S(1)}, f32[128,128]{1,0:T(8,128)S(1)}, f32[128,128]{1,0:T(8,128)S(1)}, f32[8,128]{1,0:T(8,128)S(1)}, f32[1,2048]{1,0:...) custom-call(f32[1,128]{1,0:T(1,128)} %decay_h.1, f32[1,2048]{1,0:T(1,128)} %bitcast.7, f32[1,128]{1,0:T(1,128)} %bitcast.8, ...), custom_call_target="tpu_custom_call" | custom-call | flops 30000001024 | bytes 1048576 | tf_op jit(solution)/shard_map/pallas_call | solution.py:252
  13.1 0.0 copy-start.3
  13.1 0.0 copy-start.7
  13.2 0.0 collective-permute-done.3.y0
  13.2 0.8 %collective-permute-start.14 = (bf16[2,128,512]{2,1,0:T(8,128)(2,1)S(1)}, bf16[2,128,512]{2,1,0:T(8,128)(2,1)S(1)}, u32[]{:S(2)}, u32[]{:S(2)}) collective-permute-start(bf16[2,128,512]{2,1,0:T(8,128)(2,1)S(1)} %shard_map.140), channel_id=1, source_target_pairs={{16,8},{24,16},{17,9},{25,17},{18,10},{26,18},{19,11},{27,19},{20,... | collective-permute-start | bytes 786440 | tf_op jit(solution)/shard_map/ppermute | solution.py:277
  14.0 2.3 %collective-permute-done.10.refs_12_ = bf16[2,128,512]{2,1,0:T(8,128)(2,1)S(1)} collective-permute-done((bf16[2,128,512]{2,1,0:T(8,128)(2,1)}, bf16[2,128,512]{2,1,0:T(8,128)(2,1)S(1)}, u32[]{:S(2)}, u32[]{:S(2)}) %collective-permute-start.10) | collective-permute-done | bytes 262176 | tf_op jit(solution)/shard_map/ppermute | solution.py:274
  16.3 1.3 %collective-permute-start.13 = (bf16[2,128,512]{2,1,0:T(8,128)(2,1)S(1)}, bf16[2,128,512]{2,1,0:T(8,128)(2,1)S(1)}, u32[]{:S(2)}, u32[]{:S(2)}) collective-permute-start(bf16[2,128,512]{2,1,0:T(8,128)(2,1)S(1)} %collective-permute-done.10.refs_12_), channel_id=1, source_target_pairs={{8,0},{16,24},{9,1},{17,25},{10,2},{18,26},{11,3},{19,27},{12,4},{... | collective-permute-start | bytes 786440 | tf_op jit(solution)/shard_map/ppermute | solution.py:275
  17.6 0.0 collective-permute-done.4.y1
  17.6 0.0 collective-permute-done.5.y2
  17.6 0.0 collective-permute-done.6.y3
  17.7 0.0 copy-start.1
  17.7 0.0 copy-start.2
  17.7 1.0 %shard_map.137 = (bf16[128,2048]{1,0:T(8,128)(2,1)S(1)}, bf16[392,128]{1,0:T(8,128)(2,1)S(1)}, bf16[128,128]{1,0:T(8,128)(2,1)S(1)}, bf16[128,128]{1,0:T(8,128)(2,1)S(1)}) custom-call(bf16[16,2048]{1,0:T(8,128)(2,1)S(1)} %copy-done.7, bf16[16,2048]{1,0:T(8,128)(2,1)S(1)} %collective-permute-done.x1, bf16[16,2048]{1,0:T(8,128)(2,1)S(1)} %collective-permute-done.1.x2, ...), custom_call_target="tpu_custom_call" | custom-call | flops 268435456 | bytes 1048576 | tf_op jit(solution)/shard_map/pallas_call | solution.py:252
  18.8 5.4 %collective-permute-start.7 = (bf16[392,128]{1,0:T(8,128)(2,1)S(1)}, bf16[392,128]{1,0:T(8,128)(2,1)S(1)}, u32[]{:S(2)}, u32[]{:S(2)}) collective-permute-start(bf16[392,128]{1,0:T(8,128)(2,1)S(1)} %get-tuple-element.35.packed), channel_id=1, source_target_pairs={{0,8},{8,16},{16,24},{1,9},{9,17},{17,25},{2,10},{10,18},{18,26},{... | collective-permute-start | bytes 301064 | tf_op jit(solution)/shard_map/ppermute | solution.py:308
  24.2 5.8 %collective-permute-start.8 = (bf16[392,128]{1,0:T(8,128)(2,1)S(1)}, bf16[392,128]{1,0:T(8,128)(2,1)S(1)}, u32[]{:S(2)}, u32[]{:S(2)}) collective-permute-start(bf16[392,128]{1,0:T(8,128)(2,1)S(1)} %get-tuple-element.35.packed), channel_id=1, source_target_pairs={{0,16},{8,24},{1,17},{9,25},{2,18},{10,26},{3,19},{11,27},{4,20},{... | collective-permute-start | bytes 301064 | tf_op jit(solution)/shard_map/ppermute | solution.py:308
  30.0 1.3 %collective-permute-start.9 = (bf16[392,128]{1,0:T(8,128)(2,1)S(1)}, bf16[392,128]{1,0:T(8,128)(2,1)S(1)}, u32[]{:S(2)}, u32[]{:S(2)}) collective-permute-start(bf16[392,128]{1,0:T(8,128)(2,1)S(1)} %get-tuple-element.35.packed), channel_id=1, source_target_pairs={{0,24},{1,25},{2,26},{3,27},{4,28},{5,29},{6,30},{7,31}} | collective-permute-start | bytes 301064 | tf_op jit(solution)/shard_map/ppermute | solution.py:308
  32.0 1.1 %shard_map.138 = (bf16[128,128]{1,0:T(8,128)(2,1)S(1)}, f32[128,128]{1,0:T(8,128)S(1)}, f32[128,128]{1,0:T(8,128)S(1)}, f32[2,128,128]{2,1,0:T(8,128)S(1)}, f32[...) custom-call(f32[1]{0:T(128)S(6)} %copy.15.lam, bf16[128,2048]{1,0:T(8,128)(2,1)S(1)} %get-tuple-element.34.normed, ...), custom_call_target="tpu_custom_call" | custom-call | flops 134217728 | bytes 1048576 | tf_op jit(solution)/shard_map/pallas_call | solution.py:252
  33.1 0.0 collective-permute-done.7.refs_8_
  33.1 0.2 collective-permute-done.8.refs_9_
  33.3 1.4 %collective-permute-done.9.refs_10_ = bf16[392,128]{1,0:T(8,128)(2,1)S(1)} collective-permute-done((bf16[392,128]{1,0:T(8,128)(2,1)S(1)}, bf16[392,128]{1,0:T(8,128)(2,1)S(1)}, u32[]{:S(2)}, u32[]{:S(2)}) %collective-permute-start.9) | collective-permute-done | bytes 100384 | tf_op jit(solution)/shard_map/ppermute | solution.py:308
  34.7 1.2 %shard_map.139 = (f32[64,1536]{1,0:T(8,128)S(1)}, bf16[64,1536]{1,0:T(8,128)(2,1)S(1)}, bf16[128,256]{1,0:T(8,128)(2,1)S(1)}) custom-call(bf16[128,128]{1,0:T(8,128)(2,1)S(1)} %get-tuple-element.40.refs_0_, f32[128,128]{1,0:T(8,128)S(1)} %get-tuple-element.41.refs_1_, f32[128,128]{1,0:T(8,128)S(1)} %get-tuple-element.42.refs_2_, ...), custom_call_target="tpu_custom_call" | custom-call | flops 134217728 | bytes 1048576 | tf_op jit(solution)/shard_map/pallas_call | solution.py:252
  35.9 0.1 collective-permute-start.12
  36.0 0.0 collective-permute-done.14.inner
  36.0 0.2 shard_map.141
  36.3 0.5 %collective-permute-start.15 = (bf16[64,512]{1,0:T(8,128)(2,1)S(1)}, bf16[64,512]{1,0:T(8,128)(2,1)S(1)}, u32[]{:S(2)}, u32[]{:S(2)}) collective-permute-start(bf16[64,512]{1,0:T(8,128)(2,1)S(1)} %get-tuple-element.52), channel_id=1, source_target_pairs={{0,1},{1,0},{2,3},{3,2},{4,5},{5,4},{6,7},{7,6},{8,9},{9,8},{10,11... | collective-permute-start | bytes 196616 | tf_op jit(solution)/shard_map/ppermute | solution.py:286
  36.8 0.7 %collective-permute-done.12.other = bf16[64,1536]{1,0:T(8,128)(2,1)S(1)} collective-permute-done((bf16[64,1536]{1,0:T(8,128)(2,1)S(1)}, bf16[64,1536]{1,0:T(8,128)(2,1)S(1)}, u32[]{:S(2)}, u32[]{:S(2)}) %collective-permute-start.12) | collective-permute-done | bytes 196640 | tf_op jit(solution)/shard_map/ppermute | solution.py:286
  37.5 0.2 collective-permute-done.15.last_other
  37.7 0.1 shard_map.142
  37.8 1.6 %collective-permute-start.16 = (bf16[16,2048]{1,0:T(8,128)(2,1)S(1)}, bf16[16,2048]{1,0:T(8,128)(2,1)S(1)}, u32[]{:S(2)}, u32[]{:S(2)}) collective-permute-start(bf16[16,2048]{1,0:T(8,128)(2,1)S(1)} %get-tuple-element.54), channel_id=1, source_target_pairs={{0,2},{2,0},{4,6},{6,4},{1,3},{3,1},{5,7},{7,5},{8,10},{10,8},{12,... | collective-permute-start | bytes 196616 | tf_op jit(solution)/shard_map/ppermute | solution.py:283
  39.3 1.5 %collective-permute-start.17 = (bf16[16,2048]{1,0:T(8,128)(2,1)S(1)}, bf16[16,2048]{1,0:T(8,128)(2,1)S(1)}, u32[]{:S(2)}, u32[]{:S(2)}) collective-permute-start(bf16[16,2048]{1,0:T(8,128)(2,1)S(1)} %get-tuple-element.55), channel_id=1, source_target_pairs={{0,4},{2,6},{4,0},{6,2},{1,5},{3,7},{5,1},{7,3},{8,12},{10,14},{12... | collective-permute-start | bytes 196616 | tf_op jit(solution)/shard_map/ppermute | solution.py:283
  40.8 0.5 %collective-permute-start.18 = (bf16[16,2048]{1,0:T(8,128)(2,1)S(1)}, bf16[16,2048]{1,0:T(8,128)(2,1)S(1)}, u32[]{:S(2)}, u32[]{:S(2)}) collective-permute-start(bf16[16,2048]{1,0:T(8,128)(2,1)S(1)} %get-tuple-element.56), channel_id=1, source_target_pairs={{0,6},{2,4},{4,2},{6,0},{1,7},{3,5},{5,3},{7,1},{8,14},{10,12},{12... | collective-permute-start | bytes 196616 | tf_op jit(solution)/shard_map/ppermute | solution.py:283
  41.3 0.9 %collective-permute-done.16.refs_0_ = bf16[16,2048]{1,0:T(8,128)(2,1)S(1)} collective-permute-done((bf16[16,2048]{1,0:T(8,128)(2,1)S(1)}, bf16[16,2048]{1,0:T(8,128)(2,1)S(1)}, u32[]{:S(2)}, u32[]{:S(2)}) %collective-permute-start.16) | collective-permute-done | bytes 65568 | tf_op jit(solution)/shard_map/ppermute | solution.py:283
  42.2 1.4 %collective-permute-done.17.refs_1_ = bf16[16,2048]{1,0:T(8,128)(2,1)S(1)} collective-permute-done((bf16[16,2048]{1,0:T(8,128)(2,1)S(1)}, bf16[16,2048]{1,0:T(8,128)(2,1)S(1)}, u32[]{:S(2)}, u32[]{:S(2)}) %collective-permute-start.17) | collective-permute-done | bytes 65568 | tf_op jit(solution)/shard_map/ppermute | solution.py:283
  43.6 2.4 %collective-permute-done.18.refs_2_ = bf16[16,2048]{1,0:T(8,128)(2,1)S(1)} collective-permute-done((bf16[16,2048]{1,0:T(8,128)(2,1)S(1)}, bf16[16,2048]{1,0:T(8,128)(2,1)S(1)}, u32[]{:S(2)}, u32[]{:S(2)}) %collective-permute-start.18) | collective-permute-done | bytes 65568 | tf_op jit(solution)/shard_map/ppermute | solution.py:283
  46.0 0.7 %shard_map.143 = bf16[16,2048]{1,0:T(8,128)(2,1)} custom-call(f32[16,2048]{1,0:T(8,128)S(1)} %get-tuple-element.53.mine, bf16[16,2048]{1,0:T(8,128)(2,1)S(1)} %collective-permute-done.16.refs_0_, bf16[16,2048]{1,0:T(8,128)(2,1)S(1)} %collective-permute-done.17.refs_1_, bf16[16,2048]{1,0:T(8,128)(2,1)S(1)} %collective-permute-done.18.refs_2_), custom_call_target="tpu_custom_call" | custom-call | flops 262144 | bytes 1048576 | tf_op jit(solution)/shard_map/pallas_call | solution.py:252
  (14 shorter events, 0.1 us)
Async XLA Ops:
  0.0 11.4 %collective-permute-start.11 = (bf16[2,128,512]{2,1,0:T(8,128)(2,1)}, bf16[2,128,512]{2,1,0:T(8,128)(2,1)S(1)}, u32[]{:S(2)}, u32[]{:S(2)}) collective-permute-start(bf16[2,128,512]{2,1,0:T(8,128)(2,1)} %own.1), channel_id=1, source_target_pairs={{16,0},{0,8},{24,16},{8,24},{17,1},{1,9},{25,17},{9,25},{18,2},{2,... | collective-permute-start | bytes 786440 | tf_op jit(solution)/shard_map/ppermute | solution.py:274
  3.1 4.5 %collective-permute-start = (bf16[16,2048]{1,0:T(8,128)(2,1)}, bf16[16,2048]{1,0:T(8,128)(2,1)S(1)}, u32[]{:S(2)}, u32[]{:S(2)}) collective-permute-start(bf16[16,2048]{1,0:T(8,128)(2,1)} %x0.1), channel_id=1, source_target_pairs={{0,2},{2,0},{4,6},{6,4},{1,3},{3,1},{5,7},{7,5},{8,10},{10,8},{12,... | collective-permute-start | bytes 196616 | tf_op jit(solution)/shard_map/ppermute | solution.py:283
  4.5 5.2 %collective-permute-start.1 = (bf16[16,2048]{1,0:T(8,128)(2,1)}, bf16[16,2048]{1,0:T(8,128)(2,1)S(1)}, u32[]{:S(2)}, u32[]{:S(2)}) collective-permute-start(bf16[16,2048]{1,0:T(8,128)(2,1)} %x0.1), channel_id=1, source_target_pairs={{0,4},{2,6},{4,0},{6,2},{1,5},{3,7},{5,1},{7,3},{8,12},{10,14},{12... | collective-permute-start | bytes 196616 | tf_op jit(solution)/shard_map/ppermute | solution.py:283
  6.1 5.4 %collective-permute-start.2 = (bf16[16,2048]{1,0:T(8,128)(2,1)}, bf16[16,2048]{1,0:T(8,128)(2,1)S(1)}, u32[]{:S(2)}, u32[]{:S(2)}) collective-permute-start(bf16[16,2048]{1,0:T(8,128)(2,1)} %x0.1), channel_id=1, source_target_pairs={{0,6},{2,4},{4,2},{6,0},{1,7},{3,5},{5,3},{7,1},{8,14},{10,12},{12... | collective-permute-start | bytes 196616 | tf_op jit(solution)/shard_map/ppermute | solution.py:283
  6.5 6.6 %collective-permute-start.3 = (bf16[16,2048]{1,0:T(8,128)(2,1)}, bf16[16,2048]{1,0:T(8,128)(2,1)S(1)}, u32[]{:S(2)}, u32[]{:S(2)}) collective-permute-start(bf16[16,2048]{1,0:T(8,128)(2,1)} %x0.1), channel_id=1, source_target_pairs={{0,1},{1,0},{2,3},{3,2},{4,5},{5,4},{6,7},{7,6},{8,9},{9,8},{10,11... | collective-permute-start | bytes 196616 | tf_op jit(solution)/shard_map/ppermute | solution.py:286
  7.5 8.8 %collective-permute-start.10 = (bf16[2,128,512]{2,1,0:T(8,128)(2,1)}, bf16[2,128,512]{2,1,0:T(8,128)(2,1)S(1)}, u32[]{:S(2)}, u32[]{:S(2)}) collective-permute-start(bf16[2,128,512]{2,1,0:T(8,128)(2,1)} %own.1), channel_id=1, source_target_pairs={{8,0},{24,8},{0,16},{16,24},{9,1},{25,9},{1,17},{17,25},{10,2},{26... | collective-permute-start | bytes 786440 | tf_op jit(solution)/shard_map/ppermute | solution.py:274
  9.7 7.9 %collective-permute-start.4 = (bf16[16,2048]{1,0:T(8,128)(2,1)S(1)}, bf16[16,2048]{1,0:T(8,128)(2,1)S(1)}, u32[]{:S(2)}, u32[]{:S(2)}) collective-permute-start(bf16[16,2048]{1,0:T(8,128)(2,1)S(1)} %collective-permute-done.x1), channel_id=1, source_target_pairs={{0,1},{1,0},{2,3},{3,2},{4,5},{5,4},{6,7},{7,6},{8,9},{9,8},{10,11... | collective-permute-start | bytes 196616 | tf_op jit(solution)/shard_map/ppermute | solution.py:286
  11.4 6.2 %collective-permute-start.5 = (bf16[16,2048]{1,0:T(8,128)(2,1)S(1)}, bf16[16,2048]{1,0:T(8,128)(2,1)S(1)}, u32[]{:S(2)}, u32[]{:S(2)}) collective-permute-start(bf16[16,2048]{1,0:T(8,128)(2,1)S(1)} %collective-permute-done.1.x2), channel_id=1, source_target_pairs={{0,1},{1,0},{2,3},{3,2},{4,5},{5,4},{6,7},{7,6},{8,9},{9,8},{10,11... | collective-permute-start | bytes 196616 | tf_op jit(solution)/shard_map/ppermute | solution.py:286
  11.4 6.2 %collective-permute-start.6 = (bf16[16,2048]{1,0:T(8,128)(2,1)S(1)}, bf16[16,2048]{1,0:T(8,128)(2,1)S(1)}, u32[]{:S(2)}, u32[]{:S(2)}) collective-permute-start(bf16[16,2048]{1,0:T(8,128)(2,1)S(1)} %collective-permute-done.2.x3), channel_id=1, source_target_pairs={{0,1},{1,0},{2,3},{3,2},{4,5},{5,4},{6,7},{7,6},{8,9},{9,8},{10,11... | collective-permute-start | bytes 196616 | tf_op jit(solution)/shard_map/ppermute | solution.py:286
  12.0 1.2 %copy-start = (bf16[2,128,512]{2,1,0:T(8,128)(2,1)S(1)}, bf16[2,128,512]{2,1,0:T(8,128)(2,1)}, u32[]{:S(2)}) copy-start(bf16[2,128,512]{2,1,0:T(8,128)(2,1)} %own.1) | copy-start | bytes 786436
  12.0 5.7 %copy-start.4 = (bf16[2048,128]{1,0:T(8,128)(2,1)S(1)}, bf16[2048,128]{1,0:T(8,128)(2,1)}, u32[]{:S(2)}) copy-start(bf16[2048,128]{1,0:T(8,128)(2,1)} %dv.1) | copy-start | bytes 1572868
  12.0 5.7 %copy-start.5 = (bf16[2048,128]{1,0:T(8,128)(2,1)S(1)}, bf16[2048,128]{1,0:T(8,128)(2,1)}, u32[]{:S(2)}) copy-start(bf16[2048,128]{1,0:T(8,128)(2,1)} %wk.1) | copy-start | bytes 1572868
  12.0 5.7 %copy-start.6 = (bf16[2048,128]{1,0:T(8,128)(2,1)S(1)}, bf16[2048,128]{1,0:T(8,128)(2,1)}, u32[]{:S(2)}) copy-start(bf16[2048,128]{1,0:T(8,128)(2,1)} %wv.1) | copy-start | bytes 1572868
  13.1 4.6 %copy-start.3 = (bf16[2,2048,64]{1,2,0:T(8,128)(2,1)S(1)}, bf16[2,2048,64]{1,2,0:T(8,128)(2,1)}, u32[]{:S(2)}) copy-start(bf16[2,2048,64]{1,2,0:T(8,128)(2,1)} %param.23) | copy-start | bytes 1572868
  13.1 4.6 %copy-start.7 = (bf16[16,2048]{1,0:T(8,128)(2,1)S(1)}, bf16[16,2048]{1,0:T(8,128)(2,1)}, u32[]{:S(2)}) copy-start(bf16[16,2048]{1,0:T(8,128)(2,1)} %x0.1) | copy-start | bytes 196612
  13.2 22.8 %collective-permute-start.14 = (bf16[2,128,512]{2,1,0:T(8,128)(2,1)S(1)}, bf16[2,128,512]{2,1,0:T(8,128)(2,1)S(1)}, u32[]{:S(2)}, u32[]{:S(2)}) collective-permute-start(bf16[2,128,512]{2,1,0:T(8,128)(2,1)S(1)} %shard_map.140), channel_id=1, source_target_pairs={{16,8},{24,16},{17,9},{25,17},{18,10},{26,18},{19,11},{27,19},{20,... | collective-permute-start | bytes 786440 | tf_op jit(solution)/shard_map/ppermute | solution.py:277
  16.3 19.7 %collective-permute-start.13 = (bf16[2,128,512]{2,1,0:T(8,128)(2,1)S(1)}, bf16[2,128,512]{2,1,0:T(8,128)(2,1)S(1)}, u32[]{:S(2)}, u32[]{:S(2)}) collective-permute-start(bf16[2,128,512]{2,1,0:T(8,128)(2,1)S(1)} %collective-permute-done.10.refs_12_), channel_id=1, source_target_pairs={{8,0},{16,24},{9,1},{17,25},{10,2},{18,26},{11,3},{19,27},{12,4},{... | collective-permute-start | bytes 786440 | tf_op jit(solution)/shard_map/ppermute | solution.py:275
  17.7 14.3 %copy-start.1 = (bf16[2048,128]{1,0:T(8,128)(2,1)S(1)}, bf16[2048,128]{1,0:T(8,128)(2,1)}, u32[]{:S(2)}) copy-start(bf16[2048,128]{1,0:T(8,128)(2,1)} %wq.1) | copy-start | bytes 1572868
  17.7 14.3 %copy-start.2 = (bf16[2,2048,64]{1,2,0:T(8,128)(2,1)S(1)}, bf16[2,2048,64]{1,2,0:T(8,128)(2,1)}, u32[]{:S(2)}) copy-start(bf16[2,2048,64]{1,2,0:T(8,128)(2,1)} %param.22) | copy-start | bytes 1572868
  18.8 14.3 %collective-permute-start.7 = (bf16[392,128]{1,0:T(8,128)(2,1)S(1)}, bf16[392,128]{1,0:T(8,128)(2,1)S(1)}, u32[]{:S(2)}, u32[]{:S(2)}) collective-permute-start(bf16[392,128]{1,0:T(8,128)(2,1)S(1)} %get-tuple-element.35.packed), channel_id=1, source_target_pairs={{0,8},{8,16},{16,24},{1,9},{9,17},{17,25},{2,10},{10,18},{18,26},{... | collective-permute-start | bytes 301064 | tf_op jit(solution)/shard_map/ppermute | solution.py:308
  24.2 9.1 %collective-permute-start.8 = (bf16[392,128]{1,0:T(8,128)(2,1)S(1)}, bf16[392,128]{1,0:T(8,128)(2,1)S(1)}, u32[]{:S(2)}, u32[]{:S(2)}) collective-permute-start(bf16[392,128]{1,0:T(8,128)(2,1)S(1)} %get-tuple-element.35.packed), channel_id=1, source_target_pairs={{0,16},{8,24},{1,17},{9,25},{2,18},{10,26},{3,19},{11,27},{4,20},{... | collective-permute-start | bytes 301064 | tf_op jit(solution)/shard_map/ppermute | solution.py:308
  30.0 4.7 %collective-permute-start.9 = (bf16[392,128]{1,0:T(8,128)(2,1)S(1)}, bf16[392,128]{1,0:T(8,128)(2,1)S(1)}, u32[]{:S(2)}, u32[]{:S(2)}) collective-permute-start(bf16[392,128]{1,0:T(8,128)(2,1)S(1)} %get-tuple-element.35.packed), channel_id=1, source_target_pairs={{0,24},{1,25},{2,26},{3,27},{4,28},{5,29},{6,30},{7,31}} | collective-permute-start | bytes 301064 | tf_op jit(solution)/shard_map/ppermute | solution.py:308
  35.9 1.5 %collective-permute-start.12 = (bf16[64,1536]{1,0:T(8,128)(2,1)S(1)}, bf16[64,1536]{1,0:T(8,128)(2,1)S(1)}, u32[]{:S(2)}, u32[]{:S(2)}) collective-permute-start(bf16[64,1536]{1,0:T(8,128)(2,1)S(1)} %get-tuple-element.49), channel_id=1, source_target_pairs={{0,1},{1,0},{2,3},{3,2},{4,5},{5,4},{6,7},{7,6},{8,9},{9,8},{10,11... | collective-permute-start | bytes 589832 | tf_op jit(solution)/shard_map/ppermute | solution.py:286
  36.3 1.4 %collective-permute-start.15 = (bf16[64,512]{1,0:T(8,128)(2,1)S(1)}, bf16[64,512]{1,0:T(8,128)(2,1)S(1)}, u32[]{:S(2)}, u32[]{:S(2)}) collective-permute-start(bf16[64,512]{1,0:T(8,128)(2,1)S(1)} %get-tuple-element.52), channel_id=1, source_target_pairs={{0,1},{1,0},{2,3},{3,2},{4,5},{5,4},{6,7},{7,6},{8,9},{9,8},{10,11... | collective-permute-start | bytes 196616 | tf_op jit(solution)/shard_map/ppermute | solution.py:286
  37.8 4.4 %collective-permute-start.16 = (bf16[16,2048]{1,0:T(8,128)(2,1)S(1)}, bf16[16,2048]{1,0:T(8,128)(2,1)S(1)}, u32[]{:S(2)}, u32[]{:S(2)}) collective-permute-start(bf16[16,2048]{1,0:T(8,128)(2,1)S(1)} %get-tuple-element.54), channel_id=1, source_target_pairs={{0,2},{2,0},{4,6},{6,4},{1,3},{3,1},{5,7},{7,5},{8,10},{10,8},{12,... | collective-permute-start | bytes 196616 | tf_op jit(solution)/shard_map/ppermute | solution.py:283
  39.3 4.3 %collective-permute-start.17 = (bf16[16,2048]{1,0:T(8,128)(2,1)S(1)}, bf16[16,2048]{1,0:T(8,128)(2,1)S(1)}, u32[]{:S(2)}, u32[]{:S(2)}) collective-permute-start(bf16[16,2048]{1,0:T(8,128)(2,1)S(1)} %get-tuple-element.55), channel_id=1, source_target_pairs={{0,4},{2,6},{4,0},{6,2},{1,5},{3,7},{5,1},{7,3},{8,12},{10,14},{12... | collective-permute-start | bytes 196616 | tf_op jit(solution)/shard_map/ppermute | solution.py:283
  40.8 5.2 %collective-permute-start.18 = (bf16[16,2048]{1,0:T(8,128)(2,1)S(1)}, bf16[16,2048]{1,0:T(8,128)(2,1)S(1)}, u32[]{:S(2)}, u32[]{:S(2)}) collective-permute-start(bf16[16,2048]{1,0:T(8,128)(2,1)S(1)} %get-tuple-element.56), channel_id=1, source_target_pairs={{0,6},{2,4},{4,2},{6,0},{1,7},{3,5},{5,3},{7,1},{8,14},{10,12},{12... | collective-permute-start | bytes 196616 | tf_op jit(solution)/shard_map/ppermute | solution.py:283
